TPU v7x, 256 devices: a 4x2x16 block of a 4x16x16 slice. The times are simulated.
256 devices in a mesh: grp: 2 (over y), ep: 64 (over z, x), tp: 2 (over core).
Axes of the slice: x: 4, y: 2, z: 16, core: 2. Of those that a mesh axis runs over, the one named last changes fastest.
The devices are a block of a 4x16x16 slice.
Arguments:
- tokens: bfloat16 [32768, 2048], P(('grp', 'ep', 'tp')), parts along dimension 0, may hold values from -6 to 6
- norm_gain: float32 [2048], replicated, may hold values from 0.1 to 1.9
- expert_ids: int32 [32768, 2], P(('grp', 'ep', 'tp')), parts along dimension 0, may hold values from 0 to 31, all different within a row; in each aligned block of 128 rows (0 to 127, 128 to 255, ...) at most 10 rows name the same one
- route_weights: float32 [32768, 2], P(('grp', 'ep', 'tp')), parts along dimension 0, may hold values from 0.1 to 0.9
- w_gate: bfloat16 [2048, 114688], P(None, ('ep', 'tp')), may hold values from -0.125 to 0.125
- w_up: bfloat16 [2048, 114688], P(None, ('ep', 'tp')), may hold values from -0.125 to 0.125
- w_down: bfloat16 [114688, 2048], P(('ep', 'tp')), may hold values from -0.09375 to 0.09375
Outputs:
- mixed_out: bfloat16 [32768, 2048], P(('grp', 'ep', 'tp')), parts along dimension 0
There are 2 independent parts, one for each index of `grp`. A program takes and returns all parts, laid end to end along the dimension named above; an argument that names none is the same for every part. Nothing has to cross between parts.
Inputs may be any that keep to these rules, and one draw needn't show every extreme that they name: `expert_ids`: each row names 2 different experts. Among the rows of one device no expert is named more than 10 times, and in every draw some expert is named exactly 10 times by one device's rows.
All inputs are finite; a program needn't handle non-finite values.
Results may differ from a plain program's by a relative error of at most 0.01.
Values may be sent and summed in bfloat16 or wider, within the bound.
No kernel may reach another device: no remote copies, remote signals or barrier semaphores. Data moves between devices by JAX's collectives and lax.ppermute only.
A program may use at most 128 MiB of HBM per device.

v0:
```python
import jax
import jax.numpy as jnp
from jax import lax
from jax.sharding import PartitionSpec as P


def split_up(shard, dim, devices):
    before, after = (shard.shape[:dim], shard.shape[dim + 1 :])
    return jnp.moveaxis(shard.reshape(*before, devices, -1, *after), dim, 0)


def sum_at_owner(shard, axis, dim):
    devices = lax.axis_size(axis)
    blocks = lax.all_to_all(split_up(shard, dim, devices), axis, 0, 0, tiled=True)
    return jnp.sum(blocks.astype(jnp.float32), axis=0)


def partner_2(block, axis, apart):
    count = lax.axis_size(axis)
    route = []
    for low in range(count):
        high = low | 1 << apart
        if high != low and high < count:
            route += [(low, high), (high, low)]
    return lax.ppermute(block, axis, route)


def local(tokens, norm_gain, expert_ids, route_weights, w_gate, w_up, w_down):
    ep_count = lax.axis_size("ep")
    core_count = lax.axis_size("tp")
    expert_count = ep_count // 2
    tok_count = tokens.shape[0]
    model_width = tokens.shape[1]
    top_count = expert_ids.shape[1]
    capacity = 2 * max(1, 5 * tok_count * top_count // (8 * expert_count))
    source = lax.axis_index("ep") * core_count + lax.axis_index("tp")
    values = tokens.astype(jnp.float32)
    scale_rows = lax.rsqrt(jnp.mean(values * values, axis=1, keepdims=True) + 1e-06)
    normed = (values * scale_rows * norm_gain).astype(jnp.bfloat16)
    flat_ids = expert_ids.reshape(-1)
    route_count = flat_ids.shape[0]
    onehot = (flat_ids[:, None] == jnp.arange(expert_count, dtype=jnp.int32)[None, :]).astype(
        jnp.int32
    )
    earlier = jnp.cumsum(onehot, axis=0) - onehot
    slot_base = jnp.sum(earlier * onehot, axis=1)
    slot_index = jnp.remainder(slot_base + source, capacity)
    position = flat_ids * capacity + slot_index
    token_index = jnp.arange(route_count, dtype=jnp.int32) // top_count
    slot_table = (
        jnp.full((expert_count * capacity,), tok_count, jnp.int32).at[position].set(token_index)
    )
    padded = jnp.concatenate([normed, jnp.zeros((1, model_width), jnp.bfloat16)], axis=0)
    buffer = padded[slot_table].reshape(expert_count, capacity, model_width)
    half_slots = capacity // 2
    outgoing = buffer.reshape(ep_count, half_slots, model_width)
    arrived = lax.all_to_all(outgoing, "ep", split_axis=0, concat_axis=0, tiled=True).reshape(
        -1, model_width
    )
    partner = partner_2(arrived, "ep", 0)
    block_rows = lax.all_gather(
        jnp.concatenate([arrived, partner], axis=0), "tp", axis=0, tiled=True
    )
    gate_part = jnp.dot(block_rows, w_gate, preferred_element_type=jnp.float32)
    up_part = jnp.dot(block_rows, w_up, preferred_element_type=jnp.float32)
    hidden = (jax.nn.silu(gate_part) * up_part).astype(jnp.bfloat16)
    halves = sum_at_owner(
        jnp.dot(hidden, w_down, preferred_element_type=jnp.float32).astype(jnp.bfloat16), "tp", 0
    ).astype(jnp.bfloat16)
    own_rows = arrived.shape[0]
    partner_sums = partner_2(halves[own_rows:], "ep", 0)
    combined = (halves[:own_rows].astype(jnp.float32) + partner_sums.astype(jnp.float32)).astype(
        jnp.bfloat16
    )
    returned = lax.all_to_all(
        combined.reshape(ep_count, half_slots, model_width),
        "ep",
        split_axis=0,
        concat_axis=0,
        tiled=True,
    )
    summed = returned.reshape(expert_count, capacity, model_width).astype(jnp.float32)
    picked = summed.reshape(-1, model_width)[position].reshape(tok_count, top_count, model_width)
    mixed_out = jnp.sum(picked * route_weights[:, :, None], axis=1)
    return mixed_out.astype(jnp.bfloat16)


def solution(mesh):
    placed = (
        P(("grp", "ep", "tp"), None),
        P(),
        P(("grp", "ep", "tp"), None),
        P(("grp", "ep", "tp"), None),
        P(None, ("ep", "tp")),
        P(None, ("ep", "tp")),
        P(("ep", "tp"), None),
    )
    return jax.shard_map(
        local, mesh=mesh, in_specs=placed, out_specs=P(("grp", "ep", "tp"), None), check_vma=False
    )
```

profile of v0, /device:TPU:34, one launch (start us, length us, event | category | flops | bytes accessed | tf_op | source)
XLA Modules:
  0.0 411.0 jit_solution(868617568506192977)
XLA Ops:
  6.5 0.0 all-gather.2.cloned.1.call-start
  6.6 0.8 copy.10
  7.3 0.1 eq.31
  7.5 0.1 eq.27
  7.6 0.7 broadcast_multiply_fusion
  8.3 0.6 reduce-window.6
  8.9 0.2 slice_reduce_fusion
  9.1 0.1 copy.9
  9.3 0.1 mul.67
  9.4 0.1 fusion.6
  9.5 1.4 scatter_custom_fusion
  11.0 1.2 fusion.1
  12.2 1.2 fusion.3
  13.5 2.4 gather_fusion
  15.9 0.6 reshape_reshape.3
  16.5 127.6 %all_to_all.15 = bf16[64,5,2048]{2,1,0:T(8,128)(2,1)} all-to-all(bf16[64,5,2048]{2,1,0:T(8,128)(2,1)S(1)} %reshape_reshape.3), channel_id=1, replica_groups=mesh['grp'=2,'ep'=64,'tp'=2] {'ep'}, dimensions={0} | all-to-all | bytes 2621440 | tf_op jit(solution)/shard_map/all_to_all | solution.py:57
  144.1 2.6 reshape.99
  146.7 0.7 collective-permute-start
  147.4 26.9 %collective-permute-done = bf16[320,2048]{1,0:T(8,128)(2,1)S(1)} collective-permute-done((bf16[320,2048]{1,0:T(8,128)(2,1)S(1)}, bf16[320,2048]{1,0:T(8,128)(2,1)S(1)}, u32[]{:S(2)}, u32[]{:S(2)}) %collective-permute-start) | collective-permute-done | bytes 1310752 | tf_op jit(solution)/shard_map/ppermute | solution.py:25
  174.3 1.8 pad_maximum_fusion
  176.1 0.1 all-gather.2.cloned.1.call-update
  176.1 19.2 %all-gather.2.cloned.1.call-done = bf16[1280,2048]{1,0:T(8,128)(2,1)} async-done(((bf16[640,2048]{1,0:T(8,128)(2,1)}), bf16[1280,2048]{1,0:T(8,128)(2,1)}) %all-gather.2.cloned.1.call-update) | async-done | bytes 5242896 | tf_op jit(solution)/shard_map/all_gather | solution.py:61
  195.4 10.0 %fusion.14 = f32[1280,896]{1,0:T(8,128)} fusion(bf16[1280,2048]{1,0:T(8,128)(2,1)} %all-gather.2.cloned.1.call-done, bf16[2048,896]{1,0:T(8,128)(2,1)} %param.11), kind=kOutput, calls=%fused_computation.40 | convolution fusion | flops 4697620480 | bytes 13500416 | tf_op jit(solution)/shard_map/dot_general | solution.py:64
  205.4 17.6 %convolution_convert_fusion = bf16[1280,2048]{1,0:T(8,128)(2,1)} fusion(bf16[896,2048]{1,0:T(8,128)(2,1)} %param.13, f32[1280,896]{1,0:T(8,128)} %fusion.14, bf16[1280,2048]{1,0:T(8,128)(2,1)} %all-gather.2.cloned.1.call-done, bf16[2048,896]{1,0:T(8,128)(2,1)} %param.12), kind=kOutput, calls=%fused_computation.3 | convolution fusion | flops 9404743680 | bytes 22413312 | tf_op jit(solution)/shard_map/dot_general | solution.py:68
  222.9 13.8 %all_to_all.16 = bf16[2,640,2048]{2,1,0:T(8,128)(2,1)} all-to-all(bf16[2,640,2048]{2,1,0:T(8,128)(2,1)} %bitcast.27), channel_id=1, replica_groups=mesh['grp'=2,'ep'=64,'tp'=2] {'tp'}, dimensions={0} | all-to-all | bytes 10485760 | tf_op jit(solution)/shard_map/all_to_all | solution.py:14
  236.7 4.3 %reduce_sum.41 = bf16[640,2048]{1,0:T(8,128)(2,1)S(1)} reduce(bf16[2,640,2048]{2,1,0:T(8,128)(2,1)} %all_to_all.16, bf16[]{:T(256)} %constant.51.clone.1), dimensions={0}, to_apply=%region_5.6 | reduce | flops 1310720 | bytes 7864322 | tf_op jit(solution)/shard_map/reduce_sum | solution.py:15
  241.1 0.1 slice.22
  241.2 1.4 collective-permute-start.1
  242.5 29.6 %collective-permute-done.1 = bf16[320,2048]{1,0:T(8,128)(2,1)S(1)} collective-permute-done((bf16[320,2048]{1,0:T(8,128)(2,1)S(1)}, bf16[320,2048]{1,0:T(8,128)(2,1)S(1)}, u32[]{:S(2)}, u32[]{:S(2)}) %collective-permute-start.1) | collective-permute-done | bytes 1310752 | tf_op jit(solution)/shard_map/ppermute | solution.py:25
  272.1 1.5 add_convert_fusion
  273.6 0.0 copy-start
  273.6 3.4 reshape.101
  277.0 16.4 %all-to-all-start.2 = ((bf16[64,5,2048]{2,1,0:T(8,128)(2,1)}), bf16[64,5,2048]{2,1,0:T(8,128)(2,1)}, u32[]{:S(2)}, u32[]{:S(2)}) async-start(bf16[64,5,2048]{2,1,0:T(8,128)(2,1)} %reshape.101), calls=%async_computation.2 | async-start | bytes 4194304 | tf_op jit(solution)/shard_map/all_to_all | solution.py:75
  293.4 0.0 copy-done
  293.4 0.1 copy.13
  293.6 99.0 %all-to-all-done.2 = bf16[64,5,2048]{2,1,0:T(8,128)(2,1)} async-done(((bf16[64,5,2048]{2,1,0:T(8,128)(2,1)}), bf16[64,5,2048]{2,1,0:T(8,128)(2,1)}, u32[]{:S(2)}, u32[]{:S(2)}) %all-to-all-start.2) | async-done | bytes 1310752 | tf_op jit(solution)/shard_map/all_to_all | solution.py:75
  392.5 2.5 reshape.103
  395.0 2.7 gather_fusion.1
  397.7 2.5 reshape.102
  400.2 3.9 multiply_reduce_fusion
  (11 shorter events, 0.1 us)
Async XLA Ops:
  6.5 188.8 %all-gather.2.cloned.1.call-start = ((), (), s32[]{:S(2)}) async-start(), calls=%async_computation.3 | async-start | bytes 7864320 | tf_op jit(solution)/shard_map/all_gather | solution.py:61
  146.7 27.6 %collective-permute-start = (bf16[320,2048]{1,0:T(8,128)(2,1)S(1)}, bf16[320,2048]{1,0:T(8,128)(2,1)S(1)}, u32[]{:S(2)}, u32[]{:S(2)}) collective-permute-start(bf16[320,2048]{1,0:T(8,128)(2,1)S(1)} %reshape.99), channel_id=1, source_target_pairs={{0,2},{2,0},{4,6},{6,4},{8,10},{10,8},{12,14},{14,12},{16,18},{18,... | collective-permute-start | bytes 3932168 | tf_op jit(solution)/shard_map/ppermute | solution.py:25
  241.2 30.9 %collective-permute-start.1 = (bf16[320,2048]{1,0:T(8,128)(2,1)S(1)}, bf16[320,2048]{1,0:T(8,128)(2,1)S(1)}, u32[]{:S(2)}, u32[]{:S(2)}) collective-permute-start(bf16[320,2048]{1,0:T(8,128)(2,1)S(1)} %slice.22), channel_id=1, source_target_pairs={{0,2},{2,0},{4,6},{6,4},{8,10},{10,8},{12,14},{14,12},{16,18},{18,... | collective-permute-start | bytes 3932168 | tf_op jit(solution)/shard_map/ppermute | solution.py:25
  273.6 19.8 %copy-start = (f32[128,2]{0,1:T(2,128)S(1)}, f32[128,2]{0,1:T(2,128)}, u32[]{:S(2)}) copy-start(f32[128,2]{0,1:T(2,128)} %param.10) | copy-start | bytes 3076
  277.0 115.5 %all-to-all-start.2 = ((bf16[64,5,2048]{2,1,0:T(8,128)(2,1)}), bf16[64,5,2048]{2,1,0:T(8,128)(2,1)}, u32[]{:S(2)}, u32[]{:S(2)}) async-start(bf16[64,5,2048]{2,1,0:T(8,128)(2,1)} %reshape.101), calls=%async_computation.2 | async-start | bytes 4194304 | tf_op jit(solution)/shard_map/all_to_all | solution.py:75
Sparse Core Ops, SparseCore 0:
  176.3 19.0 all-gather.1
where the time goes:
time: 412 us; the launch traced here: 411 us
  waiting for transfers between devices  175 us (42%)
  blocking collectives  141 us (34%)
  matrix products  27.5 us (7%)
  local copies, waits for them, and re-layouts  19.8 us (5%)
  starting transfers between devices  18.4 us (4%)
  other arithmetic  15.5 us (4%)
  between operations  13.6 us (3%)
    all_to_all x1, blocking collectives, local(): lax.all_to_all(outgoing, 'ep', split_axis=0, concat_axis=0, tiled=True)  128 us
    all_to_all x1, waiting for transfers between devices, local(): lax.all_to_all(combined.reshape(ep_count, half_slots, model_width), 'ep',...  99 us
    ppermute x2, waiting for transfers between devices, partner_2(): return lax.ppermute(block, axis, route)  56.5 us
    all_gather x1, waiting for transfers between devices, local(): lax.all_gather(jnp.concatenate([arrived, partner], axis=0), 'tp', axis=0,...  19.2 us
    dot_general x1, matrix products, local(): jnp.dot(hidden, w_down, preferred_element_type=jnp.float32)  17.6 us
    all_to_all x1, starting transfers between devices, local(): lax.all_to_all(combined.reshape(ep_count, half_slots, model_width), 'ep',...  16.4 us
    all_to_all x1, blocking collectives, sum_at_owner(): lax.all_to_all(split_up(shard, dim, devices), axis, 0, 0, tiled=True)  13.8 us
    dot_general x1, matrix products, local(): gate_part = jnp.dot(block_rows, w_gate, preferred_element_type=jnp.float32)  9.98 us
  transfers between devices with their start and end apart: 4, of which 4 were waited for; matrix products, arithmetic and copies ran while one was open for 0% of the time, Pallas kernels for 0%

commit v1 on v0

v1 whole, which is shorter than its diff:
```python
import jax
import jax.numpy as jnp
from jax import lax
from jax.experimental import pallas as pl
from jax.experimental.pallas import tpu as pltpu
from jax.sharding import Mesh
from jax.sharding import PartitionSpec as P


ROW = 4
TILE = 128
COLUMNS = 512
SPLIT = 4


def swap(block, axis, mask):
    count = lax.axis_size(axis)
    return lax.ppermute(block, axis, [(i, i ^ mask) for i in range(count)])


def unpack(packed, capacity):
    rows, _, width = packed.shape
    pieces = packed.reshape(rows, SPLIT, capacity, width)
    return pieces.transpose(0, 2, 1, 3).reshape(rows * capacity, SPLIT * width)


def pack(block, rows):
    capacity, width = block.shape[0] // rows, block.shape[1] // SPLIT
    pieces = block.reshape(rows, capacity, SPLIT, width)
    return pieces.transpose(0, 2, 1, 3).reshape(rows, SPLIT * capacity, width)


def along_z(packed):
    return lax.all_to_all(packed, "z", split_axis=0, concat_axis=0, tiled=True)


def add(a, b):
    return (a.astype(jnp.float32) + b.astype(jnp.float32)).astype(jnp.bfloat16)


def expert_kernel(mine, other, w_gate, w_up, w_down, out_mine, out_other, rows, hidden, down, sem):
    step, steps = pl.program_id(0), pl.num_programs(0)
    count, tile = mine.shape[0], w_gate.shape[1]
    load = pltpu.make_async_copy(w_down, down, sem)

    @pl.when(step == 0)
    def _():
        load.start()
        rows[:count] = mine[...]
        rows[count:] = other[...]

    both = jnp.dot(
        rows[...],
        jnp.concatenate([w_gate[...], w_up[...]], axis=1),
        preferred_element_type=jnp.float32,
    )
    gate, up = both[:, :tile], both[:, tile:]
    hidden[step] = (gate / (1.0 + jnp.exp(-gate)) * up).astype(jnp.bfloat16)

    @pl.when(step == steps - 1)
    def _():
        load.wait()
        units = jnp.concatenate([hidden[i] for i in range(hidden.shape[0])], axis=1)
        for first in range(0, down.shape[1], COLUMNS):
            part = jnp.dot(
                units, down[:, first : first + COLUMNS], preferred_element_type=jnp.float32
            ).astype(jnp.bfloat16)
            out_mine[:, first : first + COLUMNS] = part[:count]
            out_other[:, first : first + COLUMNS] = part[count:]


def expert(mine, other, w_gate, w_up, w_down):
    count, model_width = mine.shape
    units = w_gate.shape[1]
    steps = units // TILE
    whole = pl.BlockSpec((count, model_width), lambda i: (0, 0))
    columns = pl.BlockSpec((model_width, TILE), lambda i: (0, i))
    out = jax.ShapeDtypeStruct((count, model_width), jnp.bfloat16)
    return pl.pallas_call(
        expert_kernel,
        grid=(steps,),
        in_specs=[whole, whole, columns, columns, pl.BlockSpec(memory_space=pl.ANY)],
        out_specs=[whole, whole],
        out_shape=[out, out],
        scratch_shapes=[
            pltpu.VMEM((2 * count, model_width), jnp.bfloat16),
            pltpu.VMEM((steps, 2 * count, TILE), jnp.bfloat16),
            pltpu.VMEM((units, model_width), jnp.bfloat16),
            pltpu.SemaphoreType.DMA,
        ],
        compiler_params=pltpu.CompilerParams(vmem_limit_bytes=40 * 2**20),
        cost_estimate=pl.CostEstimate(
            flops=12 * count * model_width * units,
            bytes_accessed=6 * model_width * units + 8 * count * model_width,
            transcendentals=2 * count * units,
        ),
    )(mine, other, w_gate, w_up, w_down)


def to_halves(packed, weights, capacity):
    rows = unpack(packed, capacity)
    theirs = swap(rows, "x", 1)
    mine = jnp.concatenate([rows, theirs], axis=0)
    other = swap(mine, "tp", 1)
    out_mine, out_other = expert(mine, other, *weights)
    return add(out_mine, swap(out_other, "tp", 1))


def to_outputs(half, nz):
    count = half.shape[0] // 2
    theirs = swap(half[count:], "x", 1)
    return pack(add(half[:count], theirs), nz)


def local(tokens, norm_gain, expert_ids, route_weights, w_gate, w_up, w_down):
    nz = lax.axis_size("z")
    expert_count = nz * ROW // 2
    tok_count, model_width = tokens.shape
    top_count = expert_ids.shape[1]
    capacity = 2 * max(1, 5 * tok_count * top_count // (8 * expert_count))
    width = model_width // SPLIT
    weights = (w_gate, w_up, w_down)
    pair = lax.axis_index("x") // 2

    values = tokens.astype(jnp.float32)
    scale_rows = lax.rsqrt(jnp.mean(values * values, axis=1, keepdims=True) + 1e-06)
    normed = (values * scale_rows * norm_gain).astype(jnp.bfloat16)
    stacked = jnp.concatenate(
        [normed[:, q * width : (q + 1) * width] for q in range(SPLIT)], axis=0
    )

    before = jnp.arange(tok_count)[:, None] > jnp.arange(tok_count)[None, :]
    places, parts = [], []
    for k in range(top_count):
        mine = expert_ids[:, k]
        same = sum((mine[:, None] == expert_ids[:, j][None, :]).astype(jnp.int32) for j in range(top_count))
        rank = jnp.sum(jnp.where(before, same, 0), axis=1)
        places.append((mine // 2) * capacity + rank)
        parts.append((mine % 2) ^ pair)

    line = jnp.arange(nz * SPLIT * capacity, dtype=jnp.int32)
    line_piece = (line // capacity) % SPLIT
    line_place = (line // (SPLIT * capacity)) * capacity + line % capacity
    piece = jnp.repeat(jnp.arange(SPLIT, dtype=jnp.int32), tok_count)

    def chosen(part, k):
        place = jnp.tile(jnp.where(parts[k] == part, places[k], -1), SPLIT)
        return (line_piece[:, None] == piece[None, :]) & (line_place[:, None] == place[None, :])

    def outgoing(part):
        select = chosen(part, 0)
        for k in range(1, top_count):
            select = select | chosen(part, k)
        message = jnp.dot(select.astype(jnp.bfloat16), stacked, preferred_element_type=jnp.float32)
        return message.astype(jnp.bfloat16).reshape(nz, SPLIT * capacity, width)

    near = along_z(outgoing(0))
    crossed = swap(outgoing(1), "x", 3)
    near, crossed = lax.optimization_barrier((near, crossed))
    far = along_z(crossed)
    near_half = to_halves(near, weights, capacity)
    far, near_half = lax.optimization_barrier((far, near_half))
    near_out = to_outputs(near_half, nz)
    near_back = along_z(near_out)
    far_out = to_outputs(to_halves(far, weights, capacity), nz)
    near_back, far_out = lax.optimization_barrier((near_back, far_out))
    far_back = along_z(far_out)
    far_back = swap(far_back, "x", 3)

    mixed = jnp.zeros((SPLIT * tok_count, width), jnp.float32)
    for k in range(top_count):
        picked = jnp.zeros((SPLIT * tok_count, width), jnp.float32)
        for part, back in ((0, near_back), (1, far_back)):
            select = chosen(part, k).T.astype(jnp.bfloat16)
            picked = picked + jnp.dot(
                select, back.reshape(-1, width), preferred_element_type=jnp.float32
            )
        mixed = mixed + picked * jnp.tile(route_weights[:, k], SPLIT)[:, None]
    mixed = mixed.astype(jnp.bfloat16)
    return jnp.concatenate(
        [mixed[q * tok_count : (q + 1) * tok_count] for q in range(SPLIT)], axis=1
    )


def solution(mesh):
    groups, ep, cores = (mesh.shape[name] for name in ("grp", "ep", "tp"))
    grid = Mesh(mesh.devices.reshape(groups, ep // ROW, ROW, cores), ("grp", "z", "x", "tp"))
    tok = P(("grp", "z", "x", "tp"), None)
    placed = (
        tok,
        P(),
        tok,
        tok,
        P(None, ("z", "x", "tp")),
        P(None, ("z", "x", "tp")),
        P(("z", "x", "tp"), None),
    )

    return jax.shard_map(local, mesh=grid, in_specs=placed, out_specs=tok, check_vma=False)
```

time: 412 us -> 262 us (0.64)
  blocking collectives: 141 us -> 0 us
  starting transfers between devices: 18.4 us -> 63.1 us
  waiting for transfers between devices: 175 us -> 150 us
  matrix products: 27.5 us -> 5.41 us
  Pallas kernels: 0 us -> 20.9 us
  between operations: 13.6 us -> 0.39 us
  other arithmetic: 15.5 us -> 7.01 us
  local copies, waits for them, and re-layouts: 19.8 us -> 13.3 us
    all_to_all x2 -> x0, blocking collectives: 141 us -> none  [the longest x1 128 us: local(): lax.all_to_all(outgoing, 'ep', split_axis=0, concat_axis=0, tiled=True)]
    all_to_all x1 -> x4, starting transfers between devices: 16.4 us -> 56.6 us  [along_z(): return lax.all_to_all(packed, 'z', split_axis=0, concat_axis=0, tiled=True)]
    dot_general x2 -> x6, matrix products: 27.5 us -> 5.41 us  [the longest x4 3.18 us: local(): jnp.dot(select, back.reshape(-1, width), preferred_element_type=jnp.float32)]
    pallas_call x0 -> x2, Pallas kernels: none -> 20.9 us  [expert(): pl.pallas_call(expert_kernel, grid=(steps,), in_specs=[whole, whole, colu...]
    all_gather x1 -> x0, waiting for transfers between devices: 19.2 us -> none  [local(): lax.all_gather(jnp.concatenate([arrived, partner], axis=0), 'tp', axis=0,...]
    all_to_all x1 -> x4, waiting for transfers between devices: 99 us -> 81.6 us  [along_z(): return lax.all_to_all(packed, 'z', split_axis=0, concat_axis=0, tiled=True)]
    ppermute x2 -> x10, waiting for transfers between devices: 56.5 us -> 68.3 us  [swap(): return lax.ppermute(block, axis, [(i, i ^ mask) for i in range(count)])]
    reduce_sum x3 -> x1, other arithmetic: 8.35 us -> 0.18 us  [local(): rank = jnp.sum(jnp.where(before, same, 0), axis=1)]
  transfers between devices with their start and end apart: 4 -> 14, of which waited for: 4 -> 12; matrix products, arithmetic and copies ran while one was open for 0% -> 4% of each run, Pallas kernels for 0% -> 8%
where the time goes in v1:
time: 262 us; the launch traced here: 260 us
  waiting for transfers between devices  150 us (57%)
  starting transfers between devices  63.1 us (24%)
  Pallas kernels  20.9 us (8%)
  local copies, waits for them, and re-layouts  13.3 us (5%)
  other arithmetic  7.01 us (3%)
  matrix products  5.41 us (2%)
    all_to_all x4, waiting for transfers between devices, along_z(): return lax.all_to_all(packed, 'z', split_axis=0, concat_axis=0, tiled=True)  81.6 us
    ppermute x10, waiting for transfers between devices, swap(): return lax.ppermute(block, axis, [(i, i ^ mask) for i in range(count)])  68.3 us
    all_to_all x4, starting transfers between devices, along_z(): return lax.all_to_all(packed, 'z', split_axis=0, concat_axis=0, tiled=True)  56.6 us
    pallas_call x2, Pallas kernels, expert(): pl.pallas_call(expert_kernel, grid=(steps,), in_specs=[whole, whole, colu...  20.9 us
    ppermute x10, starting transfers between devices, swap(): return lax.ppermute(block, axis, [(i, i ^ mask) for i in range(count)])  6.51 us
  transfers between devices with their start and end apart: 14, of which 12 were waited for; matrix products, arithmetic and copies ran while one was open for 4% of the time, Pallas kernels for 8%

profile of v1, /device:TPU:34, one launch (start us, length us, event | category | flops | bytes accessed | tf_op | source)
XLA Modules:
  0.0 260.0 jit_solution(16471016235506154848)
XLA Ops:
  0.0 0.8 slice_bitcast_fusion.3
  1.0 0.8 compare_select_fusion.1
  1.8 1.2 fusion.6
  3.0 1.2 fusion.8
  4.3 1.6 convolution_convert_fusion.1
  5.9 24.0 %all-to-all-start = ((bf16[16,40,512]{2,1,0:T(8,128)(2,1)}), bf16[16,40,512]{2,1,0:T(8,128)(2,1)S(1)}, u32[]{:S(2)}, u32[]{:S(2)}) async-start(bf16[16,40,512]{2,1,0:T(8,128)(2,1)} %bitcast.5), calls=%async_computation | async-start | bytes 1310720 | tf_op jit(solution)/shard_map/all_to_all | solution.py:34
  29.9 0.7 convolution_convert_fusion
  30.5 1.8 collective-permute-start
  32.3 14.6 %collective-permute-done = bf16[16,40,512]{2,1,0:T(8,128)(2,1)S(1)} collective-permute-done((bf16[16,40,512]{2,1,0:T(8,128)(2,1)S(1)}, bf16[16,40,512]{2,1,0:T(8,128)(2,1)S(1)}, u32[]{:S(2)}, u32[]{:S(2)}) %collective-permute-start) | collective-permute-done | bytes 655392 | tf_op jit(solution)/shard_map/ppermute | solution.py:18
  46.9 16.6 %all-to-all-done = bf16[16,40,512]{2,1,0:T(8,128)(2,1)S(1)} async-done(((bf16[16,40,512]{2,1,0:T(8,128)(2,1)}), bf16[16,40,512]{2,1,0:T(8,128)(2,1)S(1)}, u32[]{:S(2)}, u32[]{:S(2)}) %all-to-all-start) | async-done | bytes 655392 | tf_op jit(solution)/shard_map/all_to_all | solution.py:34
  63.7 0.5 copy.35
  64.3 0.5 collective-permute-start.1
  64.9 10.9 %collective-permute-done.1 = bf16[160,2048]{1,0:T(8,128)(2,1)S(1)} collective-permute-done((bf16[160,2048]{1,0:T(8,128)(2,1)S(1)}, bf16[160,2048]{1,0:T(8,128)(2,1)S(1)}, u32[]{:S(2)}, u32[]{:S(2)}) %collective-permute-start.1) | collective-permute-done | bytes 655392 | tf_op jit(solution)/shard_map/ppermute | solution.py:18
  76.0 12.8 %all-to-all-start.1 = ((bf16[16,40,512]{2,1,0:T(8,128)(2,1)}), bf16[16,40,512]{2,1,0:T(8,128)(2,1)S(1)}, u32[]{:S(2)}, u32[]{:S(2)}) async-start(bf16[16,40,512]{2,1,0:T(8,128)(2,1)} %copy-done.6), calls=%async_computation.1 | async-start | bytes 1310720 | tf_op jit(solution)/shard_map/all_to_all | solution.py:34
  88.8 2.0 copy-done
  90.8 2.0 copy-done.2
  92.9 10.5 %shard_map.73 = (bf16[320,2048]{1,0:T(8,128)(2,1)S(1)}, bf16[320,2048]{1,0:T(8,128)(2,1)S(1)}) custom-call(bf16[320,2048]{1,0:T(8,128)(2,1)S(1)} %constant_dynamic-update-slice_fusion.mine, bf16[320,2048]{1,0:T(8,128)(2,1)S(1)} %collective-permute-done.2.other, bf16[2048,896]{1,0:T(8,128)(2,1)S(1)} %copy-done, bf16[2048,896]{1,0:T(8,128)(2,1)S(1)} %copy-done.2, ...), custom_call_target="tpu_custom_call" | custom-call | flops 7046430720 | bytes 16252928 | tf_op jit(solution)/shard_map/pallas_call | solution.py:79
  103.4 0.3 collective-permute-start.3
  103.7 2.8 %collective-permute-done.3 = bf16[320,2048]{1,0:T(8,128)(2,1)S(1)} collective-permute-done((bf16[320,2048]{1,0:T(8,128)(2,1)S(1)}, bf16[320,2048]{1,0:T(8,128)(2,1)S(1)}, u32[]{:S(2)}, u32[]{:S(2)}) %collective-permute-start.3) | collective-permute-done | bytes 1310752 | tf_op jit(solution)/shard_map/ppermute | solution.py:18
  106.5 0.5 add_convert_fusion.1
  107.0 17.3 %all-to-all-done.1 = bf16[16,40,512]{2,1,0:T(8,128)(2,1)S(1)} async-done(((bf16[16,40,512]{2,1,0:T(8,128)(2,1)}), bf16[16,40,512]{2,1,0:T(8,128)(2,1)S(1)}, u32[]{:S(2)}, u32[]{:S(2)}) %all-to-all-start.1) | async-done | bytes 655392 | tf_op jit(solution)/shard_map/all_to_all | solution.py:34
  124.5 0.5 copy.39
  125.2 0.5 collective-permute-start.5
  125.8 10.1 %collective-permute-done.5 = bf16[160,2048]{1,0:T(8,128)(2,1)S(1)} collective-permute-done((bf16[160,2048]{1,0:T(8,128)(2,1)S(1)}, bf16[160,2048]{1,0:T(8,128)(2,1)S(1)}, u32[]{:S(2)}, u32[]{:S(2)}) %collective-permute-start.5) | collective-permute-done | bytes 655392 | tf_op jit(solution)/shard_map/ppermute | solution.py:18
  136.2 0.7 collective-permute-start.4
  136.9 2.2 collective-permute-done.6.other
  139.1 10.5 %shard_map.74 = (bf16[320,2048]{1,0:T(8,128)(2,1)S(1)}, bf16[320,2048]{1,0:T(8,128)(2,1)S(1)}) custom-call(bf16[320,2048]{1,0:T(8,128)(2,1)S(1)} %constant_dynamic-update-slice_fusion.2.mine, bf16[320,2048]{1,0:T(8,128)(2,1)S(1)} %collective-permute-done.6.other, bf16[2048,896]{1,0:T(8,128)(2,1)S(1)} %copy-done.1, bf16[2048,896]{1,0:T(8,128)(2,1)S(1)} %copy-done.3, ...), custom_call_target="tpu_custom_call" | custom-call | flops 7046430720 | bytes 16252928 | tf_op jit(solution)/shard_map/pallas_call | solution.py:79
  149.6 0.3 collective-permute-start.7
  149.9 3.7 %collective-permute-done.4 = bf16[160,2048]{1,0:T(8,128)(2,1)S(1)} collective-permute-done((bf16[160,2048]{1,0:T(8,128)(2,1)S(1)}, bf16[160,2048]{1,0:T(8,128)(2,1)S(1)}, u32[]{:S(2)}, u32[]{:S(2)}) %collective-permute-start.4) | collective-permute-done | bytes 655392 | tf_op jit(solution)/shard_map/ppermute | solution.py:18
  153.6 1.1 add_convert_fusion.3
  154.7 2.1 reshape.251
  157.0 1.2 copy.37
  158.2 12.2 %all-to-all-start.2 = ((bf16[16,40,512]{2,1,0:T(8,128)(2,1)}), bf16[16,40,512]{2,1,0:T(8,128)(2,1)S(1)}, u32[]{:S(2)}, u32[]{:S(2)}) async-start(bf16[16,40,512]{2,1,0:T(8,128)(2,1)} %copy.37), calls=%async_computation.2 | async-start | bytes 1310720 | tf_op jit(solution)/shard_map/all_to_all | solution.py:34
  170.4 1.8 add_convert_fusion
  172.2 0.5 collective-permute-start.8
  172.8 15.6 %collective-permute-done.8 = bf16[160,2048]{1,0:T(8,128)(2,1)S(1)} collective-permute-done((bf16[160,2048]{1,0:T(8,128)(2,1)S(1)}, bf16[160,2048]{1,0:T(8,128)(2,1)S(1)}, u32[]{:S(2)}, u32[]{:S(2)}) %collective-permute-start.8) | collective-permute-done | bytes 655392 | tf_op jit(solution)/shard_map/ppermute | solution.py:18
  188.5 0.5 reshape.255
  189.2 14.3 %all-to-all-done.2 = bf16[16,40,512]{2,1,0:T(8,128)(2,1)S(1)} async-done(((bf16[16,40,512]{2,1,0:T(8,128)(2,1)}), bf16[16,40,512]{2,1,0:T(8,128)(2,1)S(1)}, u32[]{:S(2)}, u32[]{:S(2)}) %all-to-all-start.2) | async-done | bytes 655392 | tf_op jit(solution)/shard_map/all_to_all | solution.py:34
  203.6 1.2 copy.41
  204.8 7.6 %all-to-all-start.3 = ((bf16[16,40,512]{2,1,0:T(8,128)(2,1)}), bf16[16,40,512]{2,1,0:T(8,128)(2,1)S(1)}, u32[]{:S(2)}, u32[]{:S(2)}) async-start(bf16[16,40,512]{2,1,0:T(8,128)(2,1)} %copy.41), calls=%async_computation.3 | async-start | bytes 1310720 | tf_op jit(solution)/shard_map/all_to_all | solution.py:34
  212.4 33.4 %all-to-all-done.3 = bf16[16,40,512]{2,1,0:T(8,128)(2,1)S(1)} async-done(((bf16[16,40,512]{2,1,0:T(8,128)(2,1)}), bf16[16,40,512]{2,1,0:T(8,128)(2,1)S(1)}, u32[]{:S(2)}, u32[]{:S(2)}) %all-to-all-start.3) | async-done | bytes 655392 | tf_op jit(solution)/shard_map/all_to_all | solution.py:34
  245.8 1.6 collective-permute-start.9
  247.4 0.8 fusion.9
  248.2 0.8 fusion.10
  249.0 8.2 %collective-permute-done.9 = bf16[16,40,512]{2,1,0:T(8,128)(2,1)S(1)} collective-permute-done((bf16[16,40,512]{2,1,0:T(8,128)(2,1)S(1)}, bf16[16,40,512]{2,1,0:T(8,128)(2,1)S(1)}, u32[]{:S(2)}, u32[]{:S(2)}) %collective-permute-start.9) | collective-permute-done | bytes 655392 | tf_op jit(solution)/shard_map/ppermute | solution.py:18
  257.2 0.8 fusion.2
  258.0 0.8 fusion.5
  259.0 1.0 copy.42
  (44 shorter events, 2.2 us)
Async XLA Ops:
  5.9 57.6 %all-to-all-start = ((bf16[16,40,512]{2,1,0:T(8,128)(2,1)}), bf16[16,40,512]{2,1,0:T(8,128)(2,1)S(1)}, u32[]{:S(2)}, u32[]{:S(2)}) async-start(bf16[16,40,512]{2,1,0:T(8,128)(2,1)} %bitcast.5), calls=%async_computation | async-start | bytes 1310720 | tf_op jit(solution)/shard_map/all_to_all | solution.py:34
  30.5 16.4 %collective-permute-start = (bf16[16,40,512]{2,1,0:T(8,128)(2,1)S(1)}, bf16[16,40,512]{2,1,0:T(8,128)(2,1)S(1)}, u32[]{:S(2)}, u32[]{:S(2)}) collective-permute-start(bf16[16,40,512]{2,1,0:T(8,128)(2,1)S(1)} %bitcast.82), channel_id=1, source_target_pairs={{0,6},{2,4},{4,2},{6,0},{1,7},{3,5},{5,3},{7,1},{8,14},{10,12},{12... | collective-permute-start | bytes 1966088 | tf_op jit(solution)/shard_map/ppermute | solution.py:18
  46.9 17.3 %copy-start.6 = (bf16[16,40,512]{2,1,0:T(8,128)(2,1)}, bf16[16,40,512]{2,1,0:T(8,128)(2,1)S(1)}, u32[]{:S(2)}) copy-start(bf16[16,40,512]{2,1,0:T(8,128)(2,1)S(1)} %collective-permute-done) | copy-start | bytes 1966084
  64.3 11.5 %collective-permute-start.1 = (bf16[160,2048]{1,0:T(8,128)(2,1)S(1)}, bf16[160,2048]{1,0:T(8,128)(2,1)S(1)}, u32[]{:S(2)}, u32[]{:S(2)}) collective-permute-start(bf16[160,2048]{1,0:T(8,128)(2,1)S(1)} %bitcast.69), channel_id=1, source_target_pairs={{0,2},{2,0},{4,6},{6,4},{1,3},{3,1},{5,7},{7,5},{8,10},{10,8},{12,... | collective-permute-start | bytes 1966088 | tf_op jit(solution)/shard_map/ppermute | solution.py:18
  75.9 12.9 %collective-permute-start.2 = (bf16[320,2048]{1,0:T(8,128)(2,1)S(1)}, bf16[320,2048]{1,0:T(8,128)(2,1)S(1)}, u32[]{:S(2)}, u32[]{:S(2)}) collective-permute-start(bf16[320,2048]{1,0:T(8,128)(2,1)S(1)} %constant_dynamic-update-slice_fusion.mine), channel_id=1, source_target_pairs={{0,1},{1,0},{2,3},{3,2},{4,5},{5,4},{6,7},{7,6},{8,9},{9,8},{10,11... | collective-permute-start | bytes 3932168 | tf_op jit(solution)/shard_map/ppermute | solution.py:18
  76.0 48.3 %all-to-all-start.1 = ((bf16[16,40,512]{2,1,0:T(8,128)(2,1)}), bf16[16,40,512]{2,1,0:T(8,128)(2,1)S(1)}, u32[]{:S(2)}, u32[]{:S(2)}) async-start(bf16[16,40,512]{2,1,0:T(8,128)(2,1)} %copy-done.6), calls=%async_computation.1 | async-start | bytes 1310720 | tf_op jit(solution)/shard_map/all_to_all | solution.py:34
  88.8 2.0 copy-start
  90.8 2.0 copy-start.2
  103.4 3.2 %collective-permute-start.3 = (bf16[320,2048]{1,0:T(8,128)(2,1)S(1)}, bf16[320,2048]{1,0:T(8,128)(2,1)S(1)}, u32[]{:S(2)}, u32[]{:S(2)}) collective-permute-start(bf16[320,2048]{1,0:T(8,128)(2,1)S(1)} %get-tuple-element.18), channel_id=1, source_target_pairs={{0,1},{1,0},{2,3},{3,2},{4,5},{5,4},{6,7},{7,6},{8,9},{9,8},{10,11... | collective-permute-start | bytes 3932168 | tf_op jit(solution)/shard_map/ppermute | solution.py:18
  107.0 29.1 %copy-start.4 = (bf16[320,2048]{1,0:T(8,128)(2,1)}, bf16[320,2048]{1,0:T(8,128)(2,1)S(1)}, u32[]{:S(2)}) copy-start(bf16[320,2048]{1,0:T(8,128)(2,1)S(1)} %add_convert_fusion.1) | copy-start | bytes 3932164
  124.3 14.8 %copy-start.3 = (bf16[2048,896]{1,0:T(8,128)(2,1)S(1)}, bf16[2048,896]{1,0:T(8,128)(2,1)}, u32[]{:S(2)}) copy-start(bf16[2048,896]{1,0:T(8,128)(2,1)} %w_up.3) | copy-start | bytes 11010052
  125.2 10.7 %collective-permute-start.5 = (bf16[160,2048]{1,0:T(8,128)(2,1)S(1)}, bf16[160,2048]{1,0:T(8,128)(2,1)S(1)}, u32[]{:S(2)}, u32[]{:S(2)}) collective-permute-start(bf16[160,2048]{1,0:T(8,128)(2,1)S(1)} %bitcast.71), channel_id=1, source_target_pairs={{0,2},{2,0},{4,6},{6,4},{1,3},{3,1},{5,7},{7,5},{8,10},{10,8},{12,... | collective-permute-start | bytes 1966088 | tf_op jit(solution)/shard_map/ppermute | solution.py:18
  125.7 13.4 %copy-start.1 = (bf16[2048,896]{1,0:T(8,128)(2,1)S(1)}, bf16[2048,896]{1,0:T(8,128)(2,1)}, u32[]{:S(2)}) copy-start(bf16[2048,896]{1,0:T(8,128)(2,1)} %w_gate.3) | copy-start | bytes 11010052
  136.0 3.2 %collective-permute-start.6 = (bf16[320,2048]{1,0:T(8,128)(2,1)S(1)}, bf16[320,2048]{1,0:T(8,128)(2,1)S(1)}, u32[]{:S(2)}, u32[]{:S(2)}) collective-permute-start(bf16[320,2048]{1,0:T(8,128)(2,1)S(1)} %constant_dynamic-update-slice_fusion.2.mine), channel_id=1, source_target_pairs={{0,1},{1,0},{2,3},{3,2},{4,5},{5,4},{6,7},{7,6},{8,9},{9,8},{10,11... | collective-permute-start | bytes 3932168 | tf_op jit(solution)/shard_map/ppermute | solution.py:18
  136.2 17.4 %copy-start.5 = (bf16[320,2048]{1,0:T(8,128)(2,1)S(1)}, bf16[320,2048]{1,0:T(8,128)(2,1)}, u32[]{:S(2)}) copy-start(bf16[320,2048]{1,0:T(8,128)(2,1)} %copy-done.4) | copy-start | bytes 3932164
  136.2 17.4 %collective-permute-start.4 = (bf16[160,2048]{1,0:T(8,128)(2,1)S(1)}, bf16[160,2048]{1,0:T(8,128)(2,1)S(1)}, u32[]{:S(2)}, u32[]{:S(2)}) collective-permute-start(bf16[160,2048]{1,0:T(8,128)(2,1)S(1)} %slice.59), channel_id=1, source_target_pairs={{0,2},{2,0},{4,6},{6,4},{1,3},{3,1},{5,7},{7,5},{8,10},{10,8},{12,... | collective-permute-start | bytes 1966088 | tf_op jit(solution)/shard_map/ppermute | solution.py:18
  149.6 20.8 %collective-permute-start.7 = (bf16[320,2048]{1,0:T(8,128)(2,1)S(1)}, bf16[320,2048]{1,0:T(8,128)(2,1)}, u32[]{:S(2)}, u32[]{:S(2)}) collective-permute-start(bf16[320,2048]{1,0:T(8,128)(2,1)S(1)} %get-tuple-element.22), channel_id=1, source_target_pairs={{0,1},{1,0},{2,3},{3,2},{4,5},{5,4},{6,7},{7,6},{8,9},{9,8},{10,11... | collective-permute-start | bytes 3932168 | tf_op jit(solution)/shard_map/ppermute | solution.py:18
  158.2 45.4 %all-to-all-start.2 = ((bf16[16,40,512]{2,1,0:T(8,128)(2,1)}), bf16[16,40,512]{2,1,0:T(8,128)(2,1)S(1)}, u32[]{:S(2)}, u32[]{:S(2)}) async-start(bf16[16,40,512]{2,1,0:T(8,128)(2,1)} %copy.37), calls=%async_computation.2 | async-start | bytes 1310720 | tf_op jit(solution)/shard_map/all_to_all | solution.py:34
  172.2 16.1 %collective-permute-start.8 = (bf16[160,2048]{1,0:T(8,128)(2,1)S(1)}, bf16[160,2048]{1,0:T(8,128)(2,1)S(1)}, u32[]{:S(2)}, u32[]{:S(2)}) collective-permute-start(bf16[160,2048]{1,0:T(8,128)(2,1)S(1)} %slice.73), channel_id=1, source_target_pairs={{0,2},{2,0},{4,6},{6,4},{1,3},{3,1},{5,7},{7,5},{8,10},{10,8},{12,... | collective-permute-start | bytes 1966088 | tf_op jit(solution)/shard_map/ppermute | solution.py:18
  203.6 8.8 %copy-start.7 = (f32[128,2]{0,1:T(2,128)S(1)}, f32[128,2]{0,1:T(2,128)}, u32[]{:S(2)}) copy-start(f32[128,2]{0,1:T(2,128)} %param.10) | copy-start | bytes 3076
  204.8 41.0 %all-to-all-start.3 = ((bf16[16,40,512]{2,1,0:T(8,128)(2,1)}), bf16[16,40,512]{2,1,0:T(8,128)(2,1)S(1)}, u32[]{:S(2)}, u32[]{:S(2)}) async-start(bf16[16,40,512]{2,1,0:T(8,128)(2,1)} %copy.41), calls=%async_computation.3 | async-start | bytes 1310720 | tf_op jit(solution)/shard_map/all_to_all | solution.py:34
  245.8 11.5 %collective-permute-start.9 = (bf16[16,40,512]{2,1,0:T(8,128)(2,1)S(1)}, bf16[16,40,512]{2,1,0:T(8,128)(2,1)S(1)}, u32[]{:S(2)}, u32[]{:S(2)}) collective-permute-start(bf16[16,40,512]{2,1,0:T(8,128)(2,1)S(1)} %all-to-all-done.3), channel_id=1, source_target_pairs={{0,6},{2,4},{4,2},{6,0},{1,7},{3,5},{5,3},{7,1},{8,14},{10,12},{12... | collective-permute-start | bytes 1966088 | tf_op jit(solution)/shard_map/ppermute | solution.py:18

commit v2 on v1

--- a/solution.py
+++ b/solution.py
@@ -22,12 +22,6 @@
     rows, _, width = packed.shape
     pieces = packed.reshape(rows, SPLIT, capacity, width)
     return pieces.transpose(0, 2, 1, 3).reshape(rows * capacity, SPLIT * width)
-
-
-def pack(block, rows):
-    capacity, width = block.shape[0] // rows, block.shape[1] // SPLIT
-    pieces = block.reshape(rows, capacity, SPLIT, width)
-    return pieces.transpose(0, 2, 1, 3).reshape(rows, SPLIT * capacity, width)
 
 
 def along_z(packed):
@@ -88,7 +82,7 @@
             pltpu.VMEM((units, model_width), jnp.bfloat16),
             pltpu.SemaphoreType.DMA,
         ],
-        compiler_params=pltpu.CompilerParams(vmem_limit_bytes=40 * 2**20),
+        compiler_params=pltpu.CompilerParams(vmem_limit_bytes=50 * 2**20),
         cost_estimate=pl.CostEstimate(
             flops=12 * count * model_width * units,
             bytes_accessed=6 * model_width * units + 8 * count * model_width,
@@ -97,19 +91,35 @@
     )(mine, other, w_gate, w_up, w_down)
 
 
-def to_halves(packed, weights, capacity):
-    rows = unpack(packed, capacity)
-    theirs = swap(rows, "x", 1)
-    mine = jnp.concatenate([rows, theirs], axis=0)
-    other = swap(mine, "tp", 1)
-    out_mine, out_other = expert(mine, other, *weights)
+def merge_kernel(own, theirs, order, out):
+    total = (own[...].astype(jnp.float32) + theirs[...].astype(jnp.float32)).astype(jnp.bfloat16)
+    width = out.shape[1]
+    stacked = jnp.concatenate(
+        [total[:, first : first + width] for first in range(0, total.shape[1], width)], axis=0
+    )
+    out[...] = jnp.dot(order[...], stacked, preferred_element_type=jnp.float32).astype(jnp.bfloat16)
+
+
+def merge(own, theirs, order, nz):
+    count, model_width = own.shape
+    width = model_width // SPLIT
+    packed = pl.pallas_call(
+        merge_kernel,
+        out_shape=jax.ShapeDtypeStruct((count * SPLIT, width), jnp.bfloat16),
+        in_specs=[pl.BlockSpec(memory_space=pltpu.VMEM)] * 3,
+        out_specs=pl.BlockSpec(memory_space=pltpu.VMEM),
+        compiler_params=pltpu.CompilerParams(vmem_limit_bytes=12 * 2**20),
+        cost_estimate=pl.CostEstimate(
+            flops=2 * (count * SPLIT) ** 2 * width, bytes_accessed=8 * count * model_width, transcendentals=0
+        ),
+    )(own, theirs, order)
+    return packed.reshape(nz, -1, width)
+
+
+def core_sums(rows, weights):
+    other = swap(rows, "tp", 1)
+    out_mine, out_other = expert(rows, other, *weights)
     return add(out_mine, swap(out_other, "tp", 1))
-
-
-def to_outputs(half, nz):
-    count = half.shape[0] // 2
-    theirs = swap(half[count:], "x", 1)
-    return pack(add(half[:count], theirs), nz)
 
 
 def local(tokens, norm_gain, expert_ids, route_weights, w_gate, w_up, w_down):
@@ -154,15 +164,32 @@
         message = jnp.dot(select.astype(jnp.bfloat16), stacked, preferred_element_type=jnp.float32)
         return message.astype(jnp.bfloat16).reshape(nz, SPLIT * capacity, width)
 
+    stacked_piece = jnp.repeat(jnp.arange(SPLIT, dtype=jnp.int32), nz * capacity)
+    stacked_place = jnp.tile(jnp.arange(nz * capacity, dtype=jnp.int32), SPLIT)
+    order = (
+        (line_piece[:, None] == stacked_piece[None, :]) & (line_place[:, None] == stacked_place[None, :])
+    ).astype(jnp.bfloat16)
+
     near = along_z(outgoing(0))
     crossed = swap(outgoing(1), "x", 3)
-    near, crossed = lax.optimization_barrier((near, crossed))
+    near, crossed, order = lax.optimization_barrier((near, crossed, order))
     far = along_z(crossed)
-    near_half = to_halves(near, weights, capacity)
-    far, near_half = lax.optimization_barrier((far, near_half))
-    near_out = to_outputs(near_half, nz)
+
+    rows = unpack(near, capacity)
+    theirs = swap(rows, "x", 1)
+    own_half = core_sums(rows, weights)
+    their_half = core_sums(theirs, weights)
+    theirs = swap(their_half, "x", 1)
+    near_out = merge(own_half, theirs, order, nz)
+    far, near_out = lax.optimization_barrier((far, near_out))
     near_back = along_z(near_out)
-    far_out = to_outputs(to_halves(far, weights, capacity), nz)
+
+    rows = unpack(far, capacity)
+    theirs = swap(rows, "x", 1)
+    own_half = core_sums(rows, weights)
+    their_half = core_sums(theirs, weights)
+    theirs = swap(their_half, "x", 1)
+    far_out = merge(own_half, theirs, order, nz)
     near_back, far_out = lax.optimization_barrier((near_back, far_out))
     far_back = along_z(far_out)
     far_back = swap(far_back, "x", 3)

time: 262 us -> 256 us (0.977)
  Pallas kernels: 20.9 us -> 40.1 us
  waiting for transfers between devices: 150 us -> 131 us
  local copies, waits for them, and re-layouts: 13.3 us -> 3.78 us
  starting transfers between devices: 63.1 us -> 68.8 us
  other arithmetic: 7.01 us -> 3.85 us
    all_to_all x4, waiting for transfers between devices: 81.6 us -> 49.7 us  [along_z(): return lax.all_to_all(packed, 'z', split_axis=0, concat_axis=0, tiled=True)]
    pallas_call x2 -> x4, Pallas kernels: 20.9 us -> 37 us  [expert(): pl.pallas_call(expert_kernel, grid=(steps,), in_specs=[whole, whole, colu...]
    ppermute x10 -> x14, waiting for transfers between devices: 68.3 us -> 81.6 us  [swap(): return lax.ppermute(block, axis, [(i, i ^ mask) for i in range(count)])]
    all_to_all x4, starting transfers between devices: 56.6 us -> 60.9 us  [along_z(): return lax.all_to_all(packed, 'z', split_axis=0, concat_axis=0, tiled=True)]
    unnamed x20 -> x8, local copies, waits for them, and re-layouts: 4.46 us -> 0.28 us
    reshape x5 -> x0, local copies, waits for them, and re-layouts: 4.18 us -> none  [the longest x4 2.95 us: pack(): pieces = block.reshape(rows, capacity, SPLIT, width)]
    pallas_call x0 -> x2, Pallas kernels: none -> 3.16 us  [merge(): pl.pallas_call(merge_kernel, out_shape=jax.ShapeDtypeStruct((count * SPLI...]
    convert_element_type x4, other arithmetic: 3.52 us -> 0.79 us  [add(): return (a.astype(jnp.float32) + b.astype(jnp.float32)).astype(jnp.bfloat16)]
  transfers between devices with their start and end apart: 14 -> 18, of which waited for: 12 -> 10; matrix products, arithmetic and copies ran while one was open for 4% -> 1% of each run, Pallas kernels for 8% -> 16%
where the time goes in v2:
time: 256 us; the launch traced here: 254 us
  waiting for transfers between devices  131 us (51%)
  starting transfers between devices  68.8 us (27%)
  Pallas kernels  40.1 us (16%)
  matrix products  5.39 us (2%)
  other arithmetic  3.85 us (2%)
  local copies, waits for them, and re-layouts  3.78 us (1%)
    ppermute x14, waiting for transfers between devices, swap(): return lax.ppermute(block, axis, [(i, i ^ mask) for i in range(count)])  81.6 us
    all_to_all x4, starting transfers between devices, along_z(): return lax.all_to_all(packed, 'z', split_axis=0, concat_axis=0, tiled=True)  60.9 us
    all_to_all x4, waiting for transfers between devices, along_z(): return lax.all_to_all(packed, 'z', split_axis=0, concat_axis=0, tiled=True)  49.7 us
    pallas_call x4, Pallas kernels, expert(): pl.pallas_call(expert_kernel, grid=(steps,), in_specs=[whole, whole, colu...  37 us
    ppermute x14, starting transfers between devices, swap(): return lax.ppermute(block, axis, [(i, i ^ mask) for i in range(count)])  7.89 us
  transfers between devices with their start and end apart: 18, of which 10 were waited for; matrix products, arithmetic and copies ran while one was open for 1% of the time, Pallas kernels for 16%

profile of v2, /device:TPU:34, one launch (start us, length us, event | category | flops | bytes accessed | tf_op | source)
XLA Modules:
  0.0 253.5 jit_solution(3273457410360691638)
XLA Ops:
  0.0 0.8 slice_bitcast_fusion.3
  0.8 1.2 fusion.6
  2.0 1.2 fusion.8
  3.6 1.5 convolution_convert_fusion.1
  5.1 24.0 %all-to-all-start = ((bf16[16,40,512]{2,1,0:T(8,128)(2,1)}), bf16[16,40,512]{2,1,0:T(8,128)(2,1)S(1)}, u32[]{:S(2)}, u32[]{:S(2)}) async-start(bf16[16,40,512]{2,1,0:T(8,128)(2,1)} %bitcast.5), calls=%async_computation | async-start | bytes 1310720 | tf_op jit(solution)/shard_map/all_to_all | solution.py:28
  29.1 0.7 convolution_convert_fusion
  29.8 1.8 collective-permute-start
  31.7 0.3 and_convert_fusion.order
  32.0 14.1 %collective-permute-done = bf16[16,40,512]{2,1,0:T(8,128)(2,1)S(1)} collective-permute-done((bf16[16,40,512]{2,1,0:T(8,128)(2,1)S(1)}, bf16[16,40,512]{2,1,0:T(8,128)(2,1)S(1)}, u32[]{:S(2)}, u32[]{:S(2)}) %collective-permute-start) | collective-permute-done | bytes 655392 | tf_op jit(solution)/shard_map/ppermute | solution.py:18
  46.2 16.6 %all-to-all-done = bf16[16,40,512]{2,1,0:T(8,128)(2,1)S(1)} async-done(((bf16[16,40,512]{2,1,0:T(8,128)(2,1)}), bf16[16,40,512]{2,1,0:T(8,128)(2,1)S(1)}, u32[]{:S(2)}, u32[]{:S(2)}) %all-to-all-start) | async-done | bytes 655392 | tf_op jit(solution)/shard_map/all_to_all | solution.py:28
  62.9 0.5 copy.20
  63.6 0.5 collective-permute-start.3
  64.1 11.0 %collective-permute-done.3.mine = bf16[160,2048]{1,0:T(8,128)(2,1)S(1)} collective-permute-done((bf16[160,2048]{1,0:T(8,128)(2,1)S(1)}, bf16[160,2048]{1,0:T(8,128)(2,1)S(1)}, u32[]{:S(2)}, u32[]{:S(2)}) %collective-permute-start.3) | collective-permute-done | bytes 655392 | tf_op jit(solution)/shard_map/ppermute | solution.py:18
  75.1 12.7 %all-to-all-start.1 = ((bf16[16,40,512]{2,1,0:T(8,128)(2,1)}), bf16[16,40,512]{2,1,0:T(8,128)(2,1)S(1)}, u32[]{:S(2)}, u32[]{:S(2)}) async-start(bf16[16,40,512]{2,1,0:T(8,128)(2,1)} %copy-done), calls=%async_computation.1 | async-start | bytes 1310720 | tf_op jit(solution)/shard_map/all_to_all | solution.py:28
  87.8 0.3 collective-permute-start.1
  88.2 9.2 %shard_map.74 = (bf16[160,2048]{1,0:T(8,128)(2,1)S(1)}, bf16[160,2048]{1,0:T(8,128)(2,1)S(1)}) custom-call(bf16[160,2048]{1,0:T(8,128)(2,1)S(1)} %collective-permute-done.3.mine, bf16[160,2048]{1,0:T(8,128)(2,1)S(1)} %collective-permute-done.4.other, bf16[2048,896]{1,0:T(8,128)(2,1)} %w_gate.7, bf16[2048,896]{1,0:T(8,128)(2,1)} %w_up.7, bf16[896,2048]{1,0:T(8,128)(2,1)} %w_down.7), custom_call_target="tpu_custom_call" | custom-call | flops 3523215360 | bytes 13631488 | tf_op jit(solution)/shard_map/pallas_call | solution.py:73
  97.4 0.4 collective-permute-start.5
  97.8 9.2 %shard_map.73 = (bf16[160,2048]{1,0:T(8,128)(2,1)S(1)}, bf16[160,2048]{1,0:T(8,128)(2,1)S(1)}) custom-call(bf16[160,2048]{1,0:T(8,128)(2,1)S(1)} %bitcast.66, bf16[160,2048]{1,0:T(8,128)(2,1)S(1)} %collective-permute-done.1.other, bf16[2048,896]{1,0:T(8,128)(2,1)} %w_gate.7, bf16[2048,896]{1,0:T(8,128)(2,1)} %w_up.7, bf16[896,2048]{1,0:T(8,128)(2,1)} %w_down.7), custom_call_target="tpu_custom_call" | custom-call | flops 3523215360 | bytes 13631488 | tf_op jit(solution)/shard_map/pallas_call | solution.py:73
  107.1 0.3 collective-permute-start.2
  107.5 0.2 add_convert_fusion.2
  107.7 0.7 collective-permute-start.6
  108.4 1.0 collective-permute-done.2
  109.5 15.4 %collective-permute-done.6.theirs = bf16[160,2048]{1,0:T(8,128)(2,1)S(1)} collective-permute-done((bf16[160,2048]{1,0:T(8,128)(2,1)S(1)}, bf16[160,2048]{1,0:T(8,128)(2,1)S(1)}, u32[]{:S(2)}, u32[]{:S(2)}) %collective-permute-start.6) | collective-permute-done | bytes 655392 | tf_op jit(solution)/shard_map/ppermute | solution.py:18
  124.9 1.6 shard_map.75
  126.6 0.5 copy.22
  127.3 0.5 collective-permute-start.9
  127.8 15.7 %collective-permute-done.9.mine = bf16[160,2048]{1,0:T(8,128)(2,1)S(1)} collective-permute-done((bf16[160,2048]{1,0:T(8,128)(2,1)S(1)}, bf16[160,2048]{1,0:T(8,128)(2,1)S(1)}, u32[]{:S(2)}, u32[]{:S(2)}) %collective-permute-start.9) | collective-permute-done | bytes 655392 | tf_op jit(solution)/shard_map/ppermute | solution.py:18
  143.5 12.1 %all-to-all-start.2 = ((bf16[16,40,512]{2,1,0:T(8,128)(2,1)}), bf16[16,40,512]{2,1,0:T(8,128)(2,1)S(1)}, u32[]{:S(2)}, u32[]{:S(2)}) async-start(bf16[16,40,512]{2,1,0:T(8,128)(2,1)} %bitcast.11), calls=%async_computation.2 | async-start | bytes 1310720 | tf_op jit(solution)/shard_map/all_to_all | solution.py:28
  155.6 0.3 collective-permute-start.7
  155.9 9.2 %shard_map.77 = (bf16[160,2048]{1,0:T(8,128)(2,1)S(1)}, bf16[160,2048]{1,0:T(8,128)(2,1)S(1)}) custom-call(bf16[160,2048]{1,0:T(8,128)(2,1)S(1)} %collective-permute-done.9.mine, bf16[160,2048]{1,0:T(8,128)(2,1)S(1)} %collective-permute-done.10.other, bf16[2048,896]{1,0:T(8,128)(2,1)} %w_gate.7, bf16[2048,896]{1,0:T(8,128)(2,1)} %w_up.7, ...), custom_call_target="tpu_custom_call" | custom-call | flops 3523215360 | bytes 13631488 | tf_op jit(solution)/shard_map/pallas_call | solution.py:73
  165.2 0.4 collective-permute-start.11
  165.6 9.2 %shard_map.76 = (bf16[160,2048]{1,0:T(8,128)(2,1)S(1)}, bf16[160,2048]{1,0:T(8,128)(2,1)S(1)}) custom-call(bf16[160,2048]{1,0:T(8,128)(2,1)S(1)} %bitcast.69, bf16[160,2048]{1,0:T(8,128)(2,1)S(1)} %collective-permute-done.7.other, bf16[2048,896]{1,0:T(8,128)(2,1)} %w_gate.7, bf16[2048,896]{1,0:T(8,128)(2,1)} %w_up.7, bf16[896,2048]{1,0:T(8,128)(2,1)} %w_down.7), custom_call_target="tpu_custom_call" | custom-call | flops 3523215360 | bytes 13631488 | tf_op jit(solution)/shard_map/pallas_call | solution.py:73
  174.9 0.4 collective-permute-start.8
  175.2 0.2 add_convert_fusion
  175.4 0.5 collective-permute-start.12
  175.9 1.1 collective-permute-done.8
  177.1 0.2 add_convert_fusion.1.own
  177.3 15.2 %collective-permute-done.12.theirs = bf16[160,2048]{1,0:T(8,128)(2,1)S(1)} collective-permute-done((bf16[160,2048]{1,0:T(8,128)(2,1)S(1)}, bf16[160,2048]{1,0:T(8,128)(2,1)S(1)}, u32[]{:S(2)}, u32[]{:S(2)}) %collective-permute-start.12) | collective-permute-done | bytes 655392 | tf_op jit(solution)/shard_map/ppermute | solution.py:18
  192.5 1.6 shard_map.78
  194.1 12.1 %all-to-all-start.3 = ((bf16[16,40,512]{2,1,0:T(8,128)(2,1)}), bf16[16,40,512]{2,1,0:T(8,128)(2,1)S(1)}, u32[]{:S(2)}, u32[]{:S(2)}) async-start(bf16[16,40,512]{2,1,0:T(8,128)(2,1)} %bitcast.14), calls=%async_computation.3 | async-start | bytes 1310720 | tf_op jit(solution)/shard_map/all_to_all | solution.py:28
  206.2 33.1 %all-to-all-done.3 = bf16[16,40,512]{2,1,0:T(8,128)(2,1)S(1)} async-done(((bf16[16,40,512]{2,1,0:T(8,128)(2,1)}), bf16[16,40,512]{2,1,0:T(8,128)(2,1)S(1)}, u32[]{:S(2)}, u32[]{:S(2)}) %all-to-all-start.3) | async-done | bytes 655392 | tf_op jit(solution)/shard_map/all_to_all | solution.py:28
  239.3 1.7 collective-permute-start.13
  241.0 0.8 fusion.9
  241.8 0.8 fusion.10
  242.6 8.2 %collective-permute-done.13 = bf16[16,40,512]{2,1,0:T(8,128)(2,1)S(1)} collective-permute-done((bf16[16,40,512]{2,1,0:T(8,128)(2,1)S(1)}, bf16[16,40,512]{2,1,0:T(8,128)(2,1)S(1)}, u32[]{:S(2)}, u32[]{:S(2)}) %collective-permute-start.13) | collective-permute-done | bytes 655392 | tf_op jit(solution)/shard_map/ppermute | solution.py:18
  250.8 0.8 fusion.2
  251.6 0.8 fusion.5
  252.5 1.0 copy.23
  (39 shorter events, 1.5 us)
Async XLA Ops:
  0.8 2.7 %copy-start.1 = (s32[128,2]{0,1:T(2,128)S(1)}, s32[128,2]{0,1:T(2,128)}, u32[]{:S(2)}) copy-start(s32[128,2]{0,1:T(2,128)} %param.9) | copy-start | bytes 3076
  5.1 57.6 %all-to-all-start = ((bf16[16,40,512]{2,1,0:T(8,128)(2,1)}), bf16[16,40,512]{2,1,0:T(8,128)(2,1)S(1)}, u32[]{:S(2)}, u32[]{:S(2)}) async-start(bf16[16,40,512]{2,1,0:T(8,128)(2,1)} %bitcast.5), calls=%async_computation | async-start | bytes 1310720 | tf_op jit(solution)/shard_map/all_to_all | solution.py:28
  29.8 16.4 %collective-permute-start = (bf16[16,40,512]{2,1,0:T(8,128)(2,1)S(1)}, bf16[16,40,512]{2,1,0:T(8,128)(2,1)S(1)}, u32[]{:S(2)}, u32[]{:S(2)}) collective-permute-start(bf16[16,40,512]{2,1,0:T(8,128)(2,1)S(1)} %bitcast.78), channel_id=1, source_target_pairs={{0,6},{2,4},{4,2},{6,0},{1,7},{3,5},{5,3},{7,1},{8,14},{10,12},{12... | collective-permute-start | bytes 1966088 | tf_op jit(solution)/shard_map/ppermute | solution.py:18
  46.2 17.3 %copy-start = (bf16[16,40,512]{2,1,0:T(8,128)(2,1)}, bf16[16,40,512]{2,1,0:T(8,128)(2,1)S(1)}, u32[]{:S(2)}) copy-start(bf16[16,40,512]{2,1,0:T(8,128)(2,1)S(1)} %collective-permute-done) | copy-start | bytes 1966084
  63.6 11.5 %collective-permute-start.3 = (bf16[160,2048]{1,0:T(8,128)(2,1)S(1)}, bf16[160,2048]{1,0:T(8,128)(2,1)S(1)}, u32[]{:S(2)}, u32[]{:S(2)}) collective-permute-start(bf16[160,2048]{1,0:T(8,128)(2,1)S(1)} %bitcast.64), channel_id=1, source_target_pairs={{0,2},{2,0},{4,6},{6,4},{1,3},{3,1},{5,7},{7,5},{8,10},{10,8},{12,... | collective-permute-start | bytes 1966088 | tf_op jit(solution)/shard_map/ppermute | solution.py:18
  75.1 13.1 %collective-permute-start.4 = (bf16[160,2048]{1,0:T(8,128)(2,1)S(1)}, bf16[160,2048]{1,0:T(8,128)(2,1)S(1)}, u32[]{:S(2)}, u32[]{:S(2)}) collective-permute-start(bf16[160,2048]{1,0:T(8,128)(2,1)S(1)} %collective-permute-done.3.mine), channel_id=1, source_target_pairs={{0,1},{1,0},{2,3},{3,2},{4,5},{5,4},{6,7},{7,6},{8,9},{9,8},{10,11... | collective-permute-start | bytes 1966088 | tf_op jit(solution)/shard_map/ppermute | solution.py:18
  75.1 51.4 %all-to-all-start.1 = ((bf16[16,40,512]{2,1,0:T(8,128)(2,1)}), bf16[16,40,512]{2,1,0:T(8,128)(2,1)S(1)}, u32[]{:S(2)}, u32[]{:S(2)}) async-start(bf16[16,40,512]{2,1,0:T(8,128)(2,1)} %copy-done), calls=%async_computation.1 | async-start | bytes 1310720 | tf_op jit(solution)/shard_map/all_to_all | solution.py:28
  87.8 10.0 %collective-permute-start.1 = (bf16[160,2048]{1,0:T(8,128)(2,1)S(1)}, bf16[160,2048]{1,0:T(8,128)(2,1)S(1)}, u32[]{:S(2)}, u32[]{:S(2)}) collective-permute-start(bf16[160,2048]{1,0:T(8,128)(2,1)S(1)} %bitcast.65), channel_id=1, source_target_pairs={{0,1},{1,0},{2,3},{3,2},{4,5},{5,4},{6,7},{7,6},{8,9},{9,8},{10,11... | collective-permute-start | bytes 1966088 | tf_op jit(solution)/shard_map/ppermute | solution.py:18
  97.4 10.0 %collective-permute-start.5 = (bf16[160,2048]{1,0:T(8,128)(2,1)S(1)}, bf16[160,2048]{1,0:T(8,128)(2,1)S(1)}, u32[]{:S(2)}, u32[]{:S(2)}) collective-permute-start(bf16[160,2048]{1,0:T(8,128)(2,1)S(1)} %get-tuple-element.25), channel_id=1, source_target_pairs={{0,1},{1,0},{2,3},{3,2},{4,5},{5,4},{6,7},{7,6},{8,9},{9,8},{10,11... | collective-permute-start | bytes 1966088 | tf_op jit(solution)/shard_map/ppermute | solution.py:18
  107.1 2.2 collective-permute-start.2
  107.7 17.2 %collective-permute-start.6 = (bf16[160,2048]{1,0:T(8,128)(2,1)S(1)}, bf16[160,2048]{1,0:T(8,128)(2,1)S(1)}, u32[]{:S(2)}, u32[]{:S(2)}) collective-permute-start(bf16[160,2048]{1,0:T(8,128)(2,1)S(1)} %add_convert_fusion.2), channel_id=1, source_target_pairs={{0,2},{2,0},{4,6},{6,4},{1,3},{3,1},{5,7},{7,5},{8,10},{10,8},{12,... | collective-permute-start | bytes 1966088 | tf_op jit(solution)/shard_map/ppermute | solution.py:18
  127.3 16.2 %collective-permute-start.9 = (bf16[160,2048]{1,0:T(8,128)(2,1)S(1)}, bf16[160,2048]{1,0:T(8,128)(2,1)S(1)}, u32[]{:S(2)}, u32[]{:S(2)}) collective-permute-start(bf16[160,2048]{1,0:T(8,128)(2,1)S(1)} %bitcast.67), channel_id=1, source_target_pairs={{0,2},{2,0},{4,6},{6,4},{1,3},{3,1},{5,7},{7,5},{8,10},{10,8},{12,... | collective-permute-start | bytes 1966088 | tf_op jit(solution)/shard_map/ppermute | solution.py:18
  143.5 12.5 %collective-permute-start.10 = (bf16[160,2048]{1,0:T(8,128)(2,1)S(1)}, bf16[160,2048]{1,0:T(8,128)(2,1)S(1)}, u32[]{:S(2)}, u32[]{:S(2)}) collective-permute-start(bf16[160,2048]{1,0:T(8,128)(2,1)S(1)} %collective-permute-done.9.mine), channel_id=1, source_target_pairs={{0,1},{1,0},{2,3},{3,2},{4,5},{5,4},{6,7},{7,6},{8,9},{9,8},{10,11... | collective-permute-start | bytes 1966088 | tf_op jit(solution)/shard_map/ppermute | solution.py:18
  143.5 50.6 %all-to-all-start.2 = ((bf16[16,40,512]{2,1,0:T(8,128)(2,1)}), bf16[16,40,512]{2,1,0:T(8,128)(2,1)S(1)}, u32[]{:S(2)}, u32[]{:S(2)}) async-start(bf16[16,40,512]{2,1,0:T(8,128)(2,1)} %bitcast.11), calls=%async_computation.2 | async-start | bytes 1310720 | tf_op jit(solution)/shard_map/all_to_all | solution.py:28
  155.6 10.0 %collective-permute-start.7 = (bf16[160,2048]{1,0:T(8,128)(2,1)S(1)}, bf16[160,2048]{1,0:T(8,128)(2,1)S(1)}, u32[]{:S(2)}, u32[]{:S(2)}) collective-permute-start(bf16[160,2048]{1,0:T(8,128)(2,1)S(1)} %bitcast.68), channel_id=1, source_target_pairs={{0,1},{1,0},{2,3},{3,2},{4,5},{5,4},{6,7},{7,6},{8,9},{9,8},{10,11... | collective-permute-start | bytes 1966088 | tf_op jit(solution)/shard_map/ppermute | solution.py:18
  165.2 10.0 %collective-permute-start.11 = (bf16[160,2048]{1,0:T(8,128)(2,1)S(1)}, bf16[160,2048]{1,0:T(8,128)(2,1)S(1)}, u32[]{:S(2)}, u32[]{:S(2)}) collective-permute-start(bf16[160,2048]{1,0:T(8,128)(2,1)S(1)} %get-tuple-element.32), channel_id=1, source_target_pairs={{0,1},{1,0},{2,3},{3,2},{4,5},{5,4},{6,7},{7,6},{8,9},{9,8},{10,11... | collective-permute-start | bytes 1966088 | tf_op jit(solution)/shard_map/ppermute | solution.py:18
  174.9 2.2 collective-permute-start.8
  175.4 17.0 %collective-permute-start.12 = (bf16[160,2048]{1,0:T(8,128)(2,1)S(1)}, bf16[160,2048]{1,0:T(8,128)(2,1)S(1)}, u32[]{:S(2)}, u32[]{:S(2)}) collective-permute-start(bf16[160,2048]{1,0:T(8,128)(2,1)S(1)} %add_convert_fusion), channel_id=1, source_target_pairs={{0,2},{2,0},{4,6},{6,4},{1,3},{3,1},{5,7},{7,5},{8,10},{10,8},{12,... | collective-permute-start | bytes 1966088 | tf_op jit(solution)/shard_map/ppermute | solution.py:18
  194.1 12.1 %copy-start.2 = (f32[128,2]{0,1:T(2,128)S(1)}, f32[128,2]{0,1:T(2,128)}, u32[]{:S(2)}) copy-start(f32[128,2]{0,1:T(2,128)} %param.10) | copy-start | bytes 3076
  194.1 45.2 %all-to-all-start.3 = ((bf16[16,40,512]{2,1,0:T(8,128)(2,1)}), bf16[16,40,512]{2,1,0:T(8,128)(2,1)S(1)}, u32[]{:S(2)}, u32[]{:S(2)}) async-start(bf16[16,40,512]{2,1,0:T(8,128)(2,1)} %bitcast.14), calls=%async_computation.3 | async-start | bytes 1310720 | tf_op jit(solution)/shard_map/all_to_all | solution.py:28
  239.3 11.5 %collective-permute-start.13 = (bf16[16,40,512]{2,1,0:T(8,128)(2,1)S(1)}, bf16[16,40,512]{2,1,0:T(8,128)(2,1)S(1)}, u32[]{:S(2)}, u32[]{:S(2)}) collective-permute-start(bf16[16,40,512]{2,1,0:T(8,128)(2,1)S(1)} %all-to-all-done.3), channel_id=1, source_target_pairs={{0,6},{2,4},{4,2},{6,0},{1,7},{3,5},{5,3},{7,1},{8,14},{10,12},{12... | collective-permute-start | bytes 1966088 | tf_op jit(solution)/shard_map/ppermute | solution.py:18

commit v3 on v2

--- a/solution.py
+++ b/solution.py
@@ -9,7 +9,8 @@
 
 ROW = 4
 TILE = 128
-COLUMNS = 512
+FFN_LIMIT = 20
+COLUMNS = 256
 SPLIT = 4
 
 
@@ -32,60 +33,48 @@
     return (a.astype(jnp.float32) + b.astype(jnp.float32)).astype(jnp.bfloat16)
 
 
-def expert_kernel(mine, other, w_gate, w_up, w_down, out_mine, out_other, rows, hidden, down, sem):
-    step, steps = pl.program_id(0), pl.num_programs(0)
-    count, tile = mine.shape[0], w_gate.shape[1]
-    load = pltpu.make_async_copy(w_down, down, sem)
-
-    @pl.when(step == 0)
-    def _():
-        load.start()
-        rows[:count] = mine[...]
-        rows[count:] = other[...]
-
-    both = jnp.dot(
-        rows[...],
-        jnp.concatenate([w_gate[...], w_up[...]], axis=1),
-        preferred_element_type=jnp.float32,
-    )
-    gate, up = both[:, :tile], both[:, tile:]
-    hidden[step] = (gate / (1.0 + jnp.exp(-gate)) * up).astype(jnp.bfloat16)
-
-    @pl.when(step == steps - 1)
-    def _():
-        load.wait()
-        units = jnp.concatenate([hidden[i] for i in range(hidden.shape[0])], axis=1)
-        for first in range(0, down.shape[1], COLUMNS):
-            part = jnp.dot(
-                units, down[:, first : first + COLUMNS], preferred_element_type=jnp.float32
-            ).astype(jnp.bfloat16)
-            out_mine[:, first : first + COLUMNS] = part[:count]
-            out_other[:, first : first + COLUMNS] = part[count:]
+def expert_kernel(mine, other, w_gate, w_up, w_down, out_mine, out_other, hidden):
+    count, model_width = mine.shape
+    units = w_gate.shape[1]
+
+    def gated(i, carry):
+        tile = pl.ds(pl.multiple_of(i * TILE, TILE), TILE)
+        both = jnp.dot(
+            jnp.concatenate([mine[...], other[...]], axis=0),
+            jnp.concatenate([w_gate[:, tile], w_up[:, tile]], axis=1),
+            preferred_element_type=jnp.float32,
+        )
+        gate, up = both[:, :TILE], both[:, TILE:]
+        hidden[:, tile] = (gate / (1.0 + jnp.exp(-gate)) * up).astype(jnp.bfloat16)
+        return carry
+
+    lax.fori_loop(0, units // TILE, gated, 0)
+
+    def down(i, carry):
+        tile = pl.ds(pl.multiple_of(i * COLUMNS, COLUMNS), COLUMNS)
+        part = jnp.dot(hidden[...], w_down[:, tile], preferred_element_type=jnp.float32)
+        out_mine[:, tile] = part[:count].astype(jnp.bfloat16)
+        out_other[:, tile] = part[count:].astype(jnp.bfloat16)
+        return carry
+
+    lax.fori_loop(0, model_width // COLUMNS, down, 0)
 
 
 def expert(mine, other, w_gate, w_up, w_down):
     count, model_width = mine.shape
     units = w_gate.shape[1]
-    steps = units // TILE
-    whole = pl.BlockSpec((count, model_width), lambda i: (0, 0))
-    columns = pl.BlockSpec((model_width, TILE), lambda i: (0, i))
+    vmem = pl.BlockSpec(memory_space=pltpu.VMEM)
     out = jax.ShapeDtypeStruct((count, model_width), jnp.bfloat16)
     return pl.pallas_call(
         expert_kernel,
-        grid=(steps,),
-        in_specs=[whole, whole, columns, columns, pl.BlockSpec(memory_space=pl.ANY)],
-        out_specs=[whole, whole],
+        in_specs=[vmem] * 5,
+        out_specs=[vmem, vmem],
         out_shape=[out, out],
-        scratch_shapes=[
-            pltpu.VMEM((2 * count, model_width), jnp.bfloat16),
-            pltpu.VMEM((steps, 2 * count, TILE), jnp.bfloat16),
-            pltpu.VMEM((units, model_width), jnp.bfloat16),
-            pltpu.SemaphoreType.DMA,
-        ],
-        compiler_params=pltpu.CompilerParams(vmem_limit_bytes=50 * 2**20),
+        scratch_shapes=[pltpu.VMEM((2 * count, units), jnp.bfloat16)],
+        compiler_params=pltpu.CompilerParams(vmem_limit_bytes=FFN_LIMIT * 2**20),
         cost_estimate=pl.CostEstimate(
             flops=12 * count * model_width * units,
-            bytes_accessed=6 * model_width * units + 8 * count * model_width,
+            bytes_accessed=8 * count * model_width,
             transcendentals=2 * count * units,
         ),
     )(mine, other, w_gate, w_up, w_down)

time: 256 us -> 257 us (level)
  local copies, waits for them, and re-layouts: 3.78 us -> 16 us
  Pallas kernels: 40.1 us -> 29.2 us
    unnamed x8 -> x22, local copies, waits for them, and re-layouts: 0.28 us -> 12.5 us
    pallas_call x4, Pallas kernels: 37 us -> 26.1 us  [expert(): pl.pallas_call(expert_kernel, in_specs=[vmem] * 5, out_specs=[vmem, vmem]...]
  transfers between devices with their start and end apart: 18 -> 18, of which waited for: 10 -> 10; matrix products, arithmetic and copies ran while one was open for 1% -> 1% of each run, Pallas kernels for 16% -> 11%
where the time goes in v3:
time: 257 us; the launch traced here: 255 us
  waiting for transfers between devices  131 us (51%)
  starting transfers between devices  68.6 us (27%)
  Pallas kernels  29.2 us (11%)
  local copies, waits for them, and re-layouts  16 us (6%)
  matrix products  5.39 us (2%)
  other arithmetic  3.85 us (1%)
    ppermute x14, waiting for transfers between devices, swap(): return lax.ppermute(block, axis, [(i, i ^ mask) for i in range(count)])  81.6 us
    all_to_all x4, starting transfers between devices, along_z(): return lax.all_to_all(packed, 'z', split_axis=0, concat_axis=0, tiled=True)  60.9 us
    all_to_all x4, waiting for transfers between devices, along_z(): return lax.all_to_all(packed, 'z', split_axis=0, concat_axis=0, tiled=True)  49.7 us
    pallas_call x4, Pallas kernels, expert(): pl.pallas_call(expert_kernel, in_specs=[vmem] * 5, out_specs=[vmem, vmem]...  26.1 us
    unnamed x22, local copies, waits for them, and re-layouts  12.5 us
    ppermute x14, starting transfers between devices, swap(): return lax.ppermute(block, axis, [(i, i ^ mask) for i in range(count)])  7.68 us
  transfers between devices with their start and end apart: 18, of which 10 were waited for; matrix products, arithmetic and copies ran while one was open for 1% of the time, Pallas kernels for 11%

profile of v3, /device:TPU:34, one launch (start us, length us, event | category | flops | bytes accessed | tf_op | source)
XLA Modules:
  0.0 254.7 jit_solution(15708330162256576975)
XLA Ops:
  0.0 0.8 slice_bitcast_fusion.3
  0.8 1.2 fusion.6
  2.0 1.2 fusion.8
  3.6 1.5 convolution_convert_fusion.1
  5.1 24.0 %all-to-all-start = ((bf16[16,40,512]{2,1,0:T(8,128)(2,1)}), bf16[16,40,512]{2,1,0:T(8,128)(2,1)S(1)}, u32[]{:S(2)}, u32[]{:S(2)}) async-start(bf16[16,40,512]{2,1,0:T(8,128)(2,1)} %bitcast.5), calls=%async_computation | async-start | bytes 1310720 | tf_op jit(solution)/shard_map/all_to_all | solution.py:29
  29.1 0.7 convolution_convert_fusion
  29.8 1.7 collective-permute-start
  32.0 14.1 %collective-permute-done = bf16[16,40,512]{2,1,0:T(8,128)(2,1)S(1)} collective-permute-done((bf16[16,40,512]{2,1,0:T(8,128)(2,1)S(1)}, bf16[16,40,512]{2,1,0:T(8,128)(2,1)S(1)}, u32[]{:S(2)}, u32[]{:S(2)}) %collective-permute-start) | collective-permute-done | bytes 655392 | tf_op jit(solution)/shard_map/ppermute | solution.py:19
  46.2 16.6 %all-to-all-done = bf16[16,40,512]{2,1,0:T(8,128)(2,1)S(1)} async-done(((bf16[16,40,512]{2,1,0:T(8,128)(2,1)}), bf16[16,40,512]{2,1,0:T(8,128)(2,1)S(1)}, u32[]{:S(2)}, u32[]{:S(2)}) %all-to-all-start) | async-done | bytes 655392 | tf_op jit(solution)/shard_map/all_to_all | solution.py:29
  62.9 0.5 copy.20
  63.6 0.5 collective-permute-start.3
  64.1 11.0 %collective-permute-done.3.mine = bf16[160,2048]{1,0:T(8,128)(2,1)S(1)} collective-permute-done((bf16[160,2048]{1,0:T(8,128)(2,1)S(1)}, bf16[160,2048]{1,0:T(8,128)(2,1)S(1)}, u32[]{:S(2)}, u32[]{:S(2)}) %collective-permute-start.3) | collective-permute-done | bytes 655392 | tf_op jit(solution)/shard_map/ppermute | solution.py:19
  75.1 12.7 %all-to-all-start.1 = ((bf16[16,40,512]{2,1,0:T(8,128)(2,1)}), bf16[16,40,512]{2,1,0:T(8,128)(2,1)S(1)}, u32[]{:S(2)}, u32[]{:S(2)}) async-start(bf16[16,40,512]{2,1,0:T(8,128)(2,1)} %copy-done.7), calls=%async_computation.1 | async-start | bytes 1310720 | tf_op jit(solution)/shard_map/all_to_all | solution.py:29
  88.2 2.0 copy-done
  90.2 2.0 copy-done.3
  92.3 2.0 copy-done.5
  94.3 6.5 %shard_map.74 = (bf16[160,2048]{1,0:T(8,128)(2,1)S(1)}, bf16[160,2048]{1,0:T(8,128)(2,1)S(1)}) custom-call(bf16[160,2048]{1,0:T(8,128)(2,1)S(1)} %collective-permute-done.3.mine, bf16[160,2048]{1,0:T(8,128)(2,1)S(1)} %collective-permute-done.4.other, bf16[2048,896]{1,0:T(8,128)(2,1)S(1)} %copy-done, bf16[2048,896]{1,0:T(8,128)(2,1)S(1)} %copy-done.3, ...), custom_call_target="tpu_custom_call" | custom-call | flops 3523215360 | bytes 2621440 | tf_op jit(solution)/shard_map/pallas_call | solution.py:68
  100.8 0.4 collective-permute-start.5
  101.2 6.5 %shard_map.73 = (bf16[160,2048]{1,0:T(8,128)(2,1)S(1)}, bf16[160,2048]{1,0:T(8,128)(2,1)S(1)}) custom-call(bf16[160,2048]{1,0:T(8,128)(2,1)S(1)} %bitcast.66, bf16[160,2048]{1,0:T(8,128)(2,1)S(1)} %collective-permute-done.1.other, bf16[2048,896]{1,0:T(8,128)(2,1)S(1)} %copy-done.1, bf16[2048,896]{1,0:T(8,128)(2,1)S(1)} %copy-done.3, ...), custom_call_target="tpu_custom_call" | custom-call | flops 3523215360 | bytes 2621440 | tf_op jit(solution)/shard_map/pallas_call | solution.py:68
  107.8 0.4 collective-permute-start.2
  108.3 0.5 collective-permute-start.6
  108.9 1.1 collective-permute-done.2
  110.2 15.2 %collective-permute-done.6.theirs = bf16[160,2048]{1,0:T(8,128)(2,1)S(1)} collective-permute-done((bf16[160,2048]{1,0:T(8,128)(2,1)S(1)}, bf16[160,2048]{1,0:T(8,128)(2,1)S(1)}, u32[]{:S(2)}, u32[]{:S(2)}) %collective-permute-start.6) | collective-permute-done | bytes 655392 | tf_op jit(solution)/shard_map/ppermute | solution.py:19
  125.4 1.6 shard_map.75
  127.1 0.5 copy.22
  127.8 0.5 collective-permute-start.9
  128.3 15.6 %collective-permute-done.9.mine = bf16[160,2048]{1,0:T(8,128)(2,1)S(1)} collective-permute-done((bf16[160,2048]{1,0:T(8,128)(2,1)S(1)}, bf16[160,2048]{1,0:T(8,128)(2,1)S(1)}, u32[]{:S(2)}, u32[]{:S(2)}) %collective-permute-start.9) | collective-permute-done | bytes 655392 | tf_op jit(solution)/shard_map/ppermute | solution.py:19
  144.0 12.1 %all-to-all-start.2 = ((bf16[16,40,512]{2,1,0:T(8,128)(2,1)}), bf16[16,40,512]{2,1,0:T(8,128)(2,1)S(1)}, u32[]{:S(2)}, u32[]{:S(2)}) async-start(bf16[16,40,512]{2,1,0:T(8,128)(2,1)} %bitcast.11), calls=%async_computation.2 | async-start | bytes 1310720 | tf_op jit(solution)/shard_map/all_to_all | solution.py:29
  156.5 2.0 copy-done.2
  158.5 2.0 copy-done.4
  160.5 2.0 copy-done.6
  162.6 6.5 %shard_map.77 = (bf16[160,2048]{1,0:T(8,128)(2,1)S(1)}, bf16[160,2048]{1,0:T(8,128)(2,1)S(1)}) custom-call(bf16[160,2048]{1,0:T(8,128)(2,1)S(1)} %collective-permute-done.9.mine, bf16[160,2048]{1,0:T(8,128)(2,1)S(1)} %collective-permute-done.10.other, bf16[2048,896]{1,0:T(8,128)(2,1)S(1)} %copy-done.2, bf16[2048,896]{1,0:T(8,128)(2,1)S(1)} %copy-done.4, ...), custom_call_target="tpu_custom_call" | custom-call | flops 3523215360 | bytes 2621440 | tf_op jit(solution)/shard_map/pallas_call | solution.py:68
  169.1 0.4 collective-permute-start.11
  169.5 6.5 %shard_map.76 = (bf16[160,2048]{1,0:T(8,128)(2,1)S(1)}, bf16[160,2048]{1,0:T(8,128)(2,1)S(1)}) custom-call(bf16[160,2048]{1,0:T(8,128)(2,1)S(1)} %bitcast.69, bf16[160,2048]{1,0:T(8,128)(2,1)S(1)} %collective-permute-done.7.other, bf16[2048,896]{1,0:T(8,128)(2,1)S(1)} %copy-done.2, bf16[2048,896]{1,0:T(8,128)(2,1)S(1)} %copy-done.4, ...), custom_call_target="tpu_custom_call" | custom-call | flops 3523215360 | bytes 2621440 | tf_op jit(solution)/shard_map/pallas_call | solution.py:68
  176.0 0.4 collective-permute-start.8
  176.6 0.5 collective-permute-start.12
  177.1 1.2 collective-permute-done.8
  178.4 15.2 %collective-permute-done.12.theirs = bf16[160,2048]{1,0:T(8,128)(2,1)S(1)} collective-permute-done((bf16[160,2048]{1,0:T(8,128)(2,1)S(1)}, bf16[160,2048]{1,0:T(8,128)(2,1)S(1)}, u32[]{:S(2)}, u32[]{:S(2)}) %collective-permute-start.12) | collective-permute-done | bytes 655392 | tf_op jit(solution)/shard_map/ppermute | solution.py:19
  193.6 1.6 shard_map.78
  195.2 12.1 %all-to-all-start.3 = ((bf16[16,40,512]{2,1,0:T(8,128)(2,1)}), bf16[16,40,512]{2,1,0:T(8,128)(2,1)S(1)}, u32[]{:S(2)}, u32[]{:S(2)}) async-start(bf16[16,40,512]{2,1,0:T(8,128)(2,1)} %bitcast.14), calls=%async_computation.3 | async-start | bytes 1310720 | tf_op jit(solution)/shard_map/all_to_all | solution.py:29
  207.3 33.2 %all-to-all-done.3 = bf16[16,40,512]{2,1,0:T(8,128)(2,1)S(1)} async-done(((bf16[16,40,512]{2,1,0:T(8,128)(2,1)}), bf16[16,40,512]{2,1,0:T(8,128)(2,1)S(1)}, u32[]{:S(2)}, u32[]{:S(2)}) %all-to-all-start.3) | async-done | bytes 655392 | tf_op jit(solution)/shard_map/all_to_all | solution.py:29
  240.5 1.6 collective-permute-start.13
  242.1 0.8 fusion.9
  242.9 0.8 fusion.10
  243.7 8.2 %collective-permute-done.13 = bf16[16,40,512]{2,1,0:T(8,128)(2,1)S(1)} collective-permute-done((bf16[16,40,512]{2,1,0:T(8,128)(2,1)S(1)}, bf16[16,40,512]{2,1,0:T(8,128)(2,1)S(1)}, u32[]{:S(2)}, u32[]{:S(2)}) %collective-permute-start.13) | collective-permute-done | bytes 655392 | tf_op jit(solution)/shard_map/ppermute | solution.py:19
  251.9 0.8 fusion.2
  252.7 0.8 fusion.5
  253.7 1.0 copy.23
  (53 shorter events, 3.1 us)
Async XLA Ops:
  0.8 2.7 %copy-start.8 = (s32[128,2]{0,1:T(2,128)S(1)}, s32[128,2]{0,1:T(2,128)}, u32[]{:S(2)}) copy-start(s32[128,2]{0,1:T(2,128)} %param.9) | copy-start | bytes 3076
  5.1 57.6 %all-to-all-start = ((bf16[16,40,512]{2,1,0:T(8,128)(2,1)}), bf16[16,40,512]{2,1,0:T(8,128)(2,1)S(1)}, u32[]{:S(2)}, u32[]{:S(2)}) async-start(bf16[16,40,512]{2,1,0:T(8,128)(2,1)} %bitcast.5), calls=%async_computation | async-start | bytes 1310720 | tf_op jit(solution)/shard_map/all_to_all | solution.py:29
  29.8 16.4 %collective-permute-start = (bf16[16,40,512]{2,1,0:T(8,128)(2,1)S(1)}, bf16[16,40,512]{2,1,0:T(8,128)(2,1)S(1)}, u32[]{:S(2)}, u32[]{:S(2)}) collective-permute-start(bf16[16,40,512]{2,1,0:T(8,128)(2,1)S(1)} %bitcast.78), channel_id=1, source_target_pairs={{0,6},{2,4},{4,2},{6,0},{1,7},{3,5},{5,3},{7,1},{8,14},{10,12},{12... | collective-permute-start | bytes 1966088 | tf_op jit(solution)/shard_map/ppermute | solution.py:19
  46.2 17.3 %copy-start.7 = (bf16[16,40,512]{2,1,0:T(8,128)(2,1)}, bf16[16,40,512]{2,1,0:T(8,128)(2,1)S(1)}, u32[]{:S(2)}) copy-start(bf16[16,40,512]{2,1,0:T(8,128)(2,1)S(1)} %collective-permute-done) | copy-start | bytes 1966084
  63.6 11.5 %collective-permute-start.3 = (bf16[160,2048]{1,0:T(8,128)(2,1)S(1)}, bf16[160,2048]{1,0:T(8,128)(2,1)S(1)}, u32[]{:S(2)}, u32[]{:S(2)}) collective-permute-start(bf16[160,2048]{1,0:T(8,128)(2,1)S(1)} %bitcast.64), channel_id=1, source_target_pairs={{0,2},{2,0},{4,6},{6,4},{1,3},{3,1},{5,7},{7,5},{8,10},{10,8},{12,... | collective-permute-start | bytes 1966088 | tf_op jit(solution)/shard_map/ppermute | solution.py:19
  75.1 13.1 %collective-permute-start.4 = (bf16[160,2048]{1,0:T(8,128)(2,1)S(1)}, bf16[160,2048]{1,0:T(8,128)(2,1)S(1)}, u32[]{:S(2)}, u32[]{:S(2)}) collective-permute-start(bf16[160,2048]{1,0:T(8,128)(2,1)S(1)} %collective-permute-done.3.mine), channel_id=1, source_target_pairs={{0,1},{1,0},{2,3},{3,2},{4,5},{5,4},{6,7},{7,6},{8,9},{9,8},{10,11... | collective-permute-start | bytes 1966088 | tf_op jit(solution)/shard_map/ppermute | solution.py:19
  75.1 51.8 %all-to-all-start.1 = ((bf16[16,40,512]{2,1,0:T(8,128)(2,1)}), bf16[16,40,512]{2,1,0:T(8,128)(2,1)S(1)}, u32[]{:S(2)}, u32[]{:S(2)}) async-start(bf16[16,40,512]{2,1,0:T(8,128)(2,1)} %copy-done.7), calls=%async_computation.1 | async-start | bytes 1310720 | tf_op jit(solution)/shard_map/all_to_all | solution.py:29
  87.8 13.4 %collective-permute-start.1 = (bf16[160,2048]{1,0:T(8,128)(2,1)S(1)}, bf16[160,2048]{1,0:T(8,128)(2,1)S(1)}, u32[]{:S(2)}, u32[]{:S(2)}) collective-permute-start(bf16[160,2048]{1,0:T(8,128)(2,1)S(1)} %bitcast.65), channel_id=1, source_target_pairs={{0,1},{1,0},{2,3},{3,2},{4,5},{5,4},{6,7},{7,6},{8,9},{9,8},{10,11... | collective-permute-start | bytes 1966088 | tf_op jit(solution)/shard_map/ppermute | solution.py:19
  88.2 2.0 copy-start
  90.2 2.0 copy-start.3
  92.3 2.0 copy-start.5
  94.3 6.9 %copy-start.1 = (bf16[2048,896]{1,0:T(8,128)(2,1)S(1)}, bf16[2048,896]{1,0:T(8,128)(2,1)}, u32[]{:S(2)}) copy-start(bf16[2048,896]{1,0:T(8,128)(2,1)} %w_gate.7) | copy-start | bytes 11010052
  100.8 7.3 %collective-permute-start.5 = (bf16[160,2048]{1,0:T(8,128)(2,1)S(1)}, bf16[160,2048]{1,0:T(8,128)(2,1)S(1)}, u32[]{:S(2)}, u32[]{:S(2)}) collective-permute-start(bf16[160,2048]{1,0:T(8,128)(2,1)S(1)} %get-tuple-element.25), channel_id=1, source_target_pairs={{0,1},{1,0},{2,3},{3,2},{4,5},{5,4},{6,7},{7,6},{8,9},{9,8},{10,11... | collective-permute-start | bytes 1966088 | tf_op jit(solution)/shard_map/ppermute | solution.py:19
  107.8 2.2 collective-permute-start.2
  108.3 17.0 %collective-permute-start.6 = (bf16[160,2048]{1,0:T(8,128)(2,1)S(1)}, bf16[160,2048]{1,0:T(8,128)(2,1)S(1)}, u32[]{:S(2)}, u32[]{:S(2)}) collective-permute-start(bf16[160,2048]{1,0:T(8,128)(2,1)S(1)} %add_convert_fusion.2), channel_id=1, source_target_pairs={{0,2},{2,0},{4,6},{6,4},{1,3},{3,1},{5,7},{7,5},{8,10},{10,8},{12,... | collective-permute-start | bytes 1966088 | tf_op jit(solution)/shard_map/ppermute | solution.py:19
  127.8 16.2 %collective-permute-start.9 = (bf16[160,2048]{1,0:T(8,128)(2,1)S(1)}, bf16[160,2048]{1,0:T(8,128)(2,1)S(1)}, u32[]{:S(2)}, u32[]{:S(2)}) collective-permute-start(bf16[160,2048]{1,0:T(8,128)(2,1)S(1)} %bitcast.67), channel_id=1, source_target_pairs={{0,2},{2,0},{4,6},{6,4},{1,3},{3,1},{5,7},{7,5},{8,10},{10,8},{12,... | collective-permute-start | bytes 1966088 | tf_op jit(solution)/shard_map/ppermute | solution.py:19
  144.0 12.5 %collective-permute-start.10 = (bf16[160,2048]{1,0:T(8,128)(2,1)S(1)}, bf16[160,2048]{1,0:T(8,128)(2,1)S(1)}, u32[]{:S(2)}, u32[]{:S(2)}) collective-permute-start(bf16[160,2048]{1,0:T(8,128)(2,1)S(1)} %collective-permute-done.9.mine), channel_id=1, source_target_pairs={{0,1},{1,0},{2,3},{3,2},{4,5},{5,4},{6,7},{7,6},{8,9},{9,8},{10,11... | collective-permute-start | bytes 1966088 | tf_op jit(solution)/shard_map/ppermute | solution.py:19
  144.0 51.2 %all-to-all-start.2 = ((bf16[16,40,512]{2,1,0:T(8,128)(2,1)}), bf16[16,40,512]{2,1,0:T(8,128)(2,1)S(1)}, u32[]{:S(2)}, u32[]{:S(2)}) async-start(bf16[16,40,512]{2,1,0:T(8,128)(2,1)} %bitcast.11), calls=%async_computation.2 | async-start | bytes 1310720 | tf_op jit(solution)/shard_map/all_to_all | solution.py:29
  156.1 13.4 %collective-permute-start.7 = (bf16[160,2048]{1,0:T(8,128)(2,1)S(1)}, bf16[160,2048]{1,0:T(8,128)(2,1)S(1)}, u32[]{:S(2)}, u32[]{:S(2)}) collective-permute-start(bf16[160,2048]{1,0:T(8,128)(2,1)S(1)} %bitcast.68), channel_id=1, source_target_pairs={{0,1},{1,0},{2,3},{3,2},{4,5},{5,4},{6,7},{7,6},{8,9},{9,8},{10,11... | collective-permute-start | bytes 1966088 | tf_op jit(solution)/shard_map/ppermute | solution.py:19
  156.5 2.0 copy-start.2
  158.5 2.0 copy-start.4
  160.5 2.0 copy-start.6
  169.1 7.3 %collective-permute-start.11 = (bf16[160,2048]{1,0:T(8,128)(2,1)S(1)}, bf16[160,2048]{1,0:T(8,128)(2,1)S(1)}, u32[]{:S(2)}, u32[]{:S(2)}) collective-permute-start(bf16[160,2048]{1,0:T(8,128)(2,1)S(1)} %get-tuple-element.32), channel_id=1, source_target_pairs={{0,1},{1,0},{2,3},{3,2},{4,5},{5,4},{6,7},{7,6},{8,9},{9,8},{10,11... | collective-permute-start | bytes 1966088 | tf_op jit(solution)/shard_map/ppermute | solution.py:19
  176.0 2.2 collective-permute-start.8
  176.6 17.0 %collective-permute-start.12 = (bf16[160,2048]{1,0:T(8,128)(2,1)S(1)}, bf16[160,2048]{1,0:T(8,128)(2,1)S(1)}, u32[]{:S(2)}, u32[]{:S(2)}) collective-permute-start(bf16[160,2048]{1,0:T(8,128)(2,1)S(1)} %add_convert_fusion), channel_id=1, source_target_pairs={{0,2},{2,0},{4,6},{6,4},{1,3},{3,1},{5,7},{7,5},{8,10},{10,8},{12,... | collective-permute-start | bytes 1966088 | tf_op jit(solution)/shard_map/ppermute | solution.py:19
  195.2 12.1 %copy-start.9 = (f32[128,2]{0,1:T(2,128)S(1)}, f32[128,2]{0,1:T(2,128)}, u32[]{:S(2)}) copy-start(f32[128,2]{0,1:T(2,128)} %param.10) | copy-start | bytes 3076
  195.2 45.2 %all-to-all-start.3 = ((bf16[16,40,512]{2,1,0:T(8,128)(2,1)}), bf16[16,40,512]{2,1,0:T(8,128)(2,1)S(1)}, u32[]{:S(2)}, u32[]{:S(2)}) async-start(bf16[16,40,512]{2,1,0:T(8,128)(2,1)} %bitcast.14), calls=%async_computation.3 | async-start | bytes 1310720 | tf_op jit(solution)/shard_map/all_to_all | solution.py:29
  240.5 11.5 %collective-permute-start.13 = (bf16[16,40,512]{2,1,0:T(8,128)(2,1)S(1)}, bf16[16,40,512]{2,1,0:T(8,128)(2,1)S(1)}, u32[]{:S(2)}, u32[]{:S(2)}) collective-permute-start(bf16[16,40,512]{2,1,0:T(8,128)(2,1)S(1)} %all-to-all-done.3), channel_id=1, source_target_pairs={{0,6},{2,4},{4,2},{6,0},{1,7},{3,5},{5,3},{7,1},{8,14},{10,12},{12... | collective-permute-start | bytes 1966088 | tf_op jit(solution)/shard_map/ppermute | solution.py:19

commit v4 on v2

--- a/solution.py
+++ b/solution.py
@@ -9,6 +9,7 @@
 
 ROW = 4
 TILE = 128
+FFN_LIMIT = 50
 COLUMNS = 512
 SPLIT = 4
 
@@ -32,16 +33,18 @@
     return (a.astype(jnp.float32) + b.astype(jnp.float32)).astype(jnp.bfloat16)
 
 
-def expert_kernel(mine, other, w_gate, w_up, w_down, out_mine, out_other, rows, hidden, down, sem):
+def expert_kernel(*refs):
+    ins, (w_gate, w_up, w_down), outs = refs[:4], refs[4:7], refs[7:11]
+    rows, hidden, down, sem = refs[11:]
     step, steps = pl.program_id(0), pl.num_programs(0)
-    count, tile = mine.shape[0], w_gate.shape[1]
+    count, tile = ins[0].shape[0], w_gate.shape[1]
     load = pltpu.make_async_copy(w_down, down, sem)
 
     @pl.when(step == 0)
     def _():
         load.start()
-        rows[:count] = mine[...]
-        rows[count:] = other[...]
+        for i, source in enumerate(ins):
+            rows[i * count : (i + 1) * count] = source[...]
 
     both = jnp.dot(
         rows[...],
@@ -59,41 +62,48 @@
             part = jnp.dot(
                 units, down[:, first : first + COLUMNS], preferred_element_type=jnp.float32
             ).astype(jnp.bfloat16)
-            out_mine[:, first : first + COLUMNS] = part[:count]
-            out_other[:, first : first + COLUMNS] = part[count:]
-
-
-def expert(mine, other, w_gate, w_up, w_down):
-    count, model_width = mine.shape
+            for i, target in enumerate(outs):
+                target[:, first : first + COLUMNS] = part[i * count : (i + 1) * count]
+
+
+def expert(blocks, w_gate, w_up, w_down):
+    count, model_width = blocks[0].shape
     units = w_gate.shape[1]
     steps = units // TILE
+    total = len(blocks) * count
     whole = pl.BlockSpec((count, model_width), lambda i: (0, 0))
     columns = pl.BlockSpec((model_width, TILE), lambda i: (0, i))
     out = jax.ShapeDtypeStruct((count, model_width), jnp.bfloat16)
     return pl.pallas_call(
         expert_kernel,
         grid=(steps,),
-        in_specs=[whole, whole, columns, columns, pl.BlockSpec(memory_space=pl.ANY)],
-        out_specs=[whole, whole],
-        out_shape=[out, out],
+        in_specs=[whole] * 4 + [columns, columns, pl.BlockSpec(memory_space=pl.ANY)],
+        out_specs=[whole] * 4,
+        out_shape=[out] * 4,
         scratch_shapes=[
-            pltpu.VMEM((2 * count, model_width), jnp.bfloat16),
-            pltpu.VMEM((steps, 2 * count, TILE), jnp.bfloat16),
+            pltpu.VMEM((total, model_width), jnp.bfloat16),
+            pltpu.VMEM((steps, total, TILE), jnp.bfloat16),
             pltpu.VMEM((units, model_width), jnp.bfloat16),
             pltpu.SemaphoreType.DMA,
         ],
-        compiler_params=pltpu.CompilerParams(vmem_limit_bytes=50 * 2**20),
+        compiler_params=pltpu.CompilerParams(vmem_limit_bytes=FFN_LIMIT * 2**20),
         cost_estimate=pl.CostEstimate(
-            flops=12 * count * model_width * units,
-            bytes_accessed=6 * model_width * units + 8 * count * model_width,
-            transcendentals=2 * count * units,
+            flops=6 * total * model_width * units,
+            bytes_accessed=6 * model_width * units + 4 * total * model_width,
+            transcendentals=total * units,
         ),
-    )(mine, other, w_gate, w_up, w_down)
-
-
-def merge_kernel(own, theirs, order, out):
-    total = (own[...].astype(jnp.float32) + theirs[...].astype(jnp.float32)).astype(jnp.bfloat16)
+    )(*blocks, w_gate, w_up, w_down)
+
+
+def merge_kernel(*refs):
+    parts, order, out = refs[:-2], refs[-2], refs[-1]
+    half = len(parts) // 2
     width = out.shape[1]
+    own, theirs = (
+        jnp.concatenate([part[...] for part in some], axis=0).astype(jnp.float32)
+        for some in (parts[:half], parts[half:])
+    )
+    total = (own + theirs).astype(jnp.bfloat16)
     stacked = jnp.concatenate(
         [total[:, first : first + width] for first in range(0, total.shape[1], width)], axis=0
     )
@@ -101,25 +111,37 @@
 
 
 def merge(own, theirs, order, nz):
-    count, model_width = own.shape
+    count = sum(part.shape[0] for part in own)
+    model_width = own[0].shape[1]
     width = model_width // SPLIT
+    vmem = pl.BlockSpec(memory_space=pltpu.VMEM)
     packed = pl.pallas_call(
         merge_kernel,
         out_shape=jax.ShapeDtypeStruct((count * SPLIT, width), jnp.bfloat16),
-        in_specs=[pl.BlockSpec(memory_space=pltpu.VMEM)] * 3,
-        out_specs=pl.BlockSpec(memory_space=pltpu.VMEM),
+        in_specs=[vmem] * (2 * len(own) + 1),
+        out_specs=vmem,
         compiler_params=pltpu.CompilerParams(vmem_limit_bytes=12 * 2**20),
         cost_estimate=pl.CostEstimate(
             flops=2 * (count * SPLIT) ** 2 * width, bytes_accessed=8 * count * model_width, transcendentals=0
         ),
-    )(own, theirs, order)
+    )(*own, *theirs, order)
     return packed.reshape(nz, -1, width)
 
 
-def core_sums(rows, weights):
-    other = swap(rows, "tp", 1)
-    out_mine, out_other = expert(rows, other, *weights)
-    return add(out_mine, swap(out_other, "tp", 1))
+def through_row(packed, weights, capacity, pieces):
+    rows = unpack(packed, capacity)
+    size = rows.shape[0] // pieces
+    cut = [rows[i * size : (i + 1) * size] for i in range(pieces)]
+    own, theirs = [], []
+    for mine in cut:
+        partner = swap(mine, "x", 1)
+        mine_other = swap(mine, "tp", 1)
+        partner_other = swap(partner, "tp", 1)
+        sums = expert((mine, partner, mine_other, partner_other), *weights)
+        partner_half = add(sums[1], swap(sums[3], "tp", 1))
+        own.append(add(sums[0], swap(sums[2], "tp", 1)))
+        theirs.append(swap(partner_half, "x", 1))
+    return own, theirs
 
 
 def local(tokens, norm_gain, expert_ids, route_weights, w_gate, w_up, w_down):
@@ -175,21 +197,12 @@
     near, crossed, order = lax.optimization_barrier((near, crossed, order))
     far = along_z(crossed)
 
-    rows = unpack(near, capacity)
-    theirs = swap(rows, "x", 1)
-    own_half = core_sums(rows, weights)
-    their_half = core_sums(theirs, weights)
-    theirs = swap(their_half, "x", 1)
-    near_out = merge(own_half, theirs, order, nz)
+    own, theirs = through_row(near, weights, capacity, 2)
+    near_out = merge(own, theirs, order, nz)
     far, near_out = lax.optimization_barrier((far, near_out))
     near_back = along_z(near_out)
-
-    rows = unpack(far, capacity)
-    theirs = swap(rows, "x", 1)
-    own_half = core_sums(rows, weights)
-    their_half = core_sums(theirs, weights)
-    theirs = swap(their_half, "x", 1)
-    far_out = merge(own_half, theirs, order, nz)
+    own, theirs = through_row(far, weights, capacity, 1)
+    far_out = merge(own, theirs, order, nz)
     near_back, far_out = lax.optimization_barrier((near_back, far_out))
     far_back = along_z(far_out)
     far_back = swap(far_back, "x", 3)

time: 256 us -> 246 us (0.961)
  Pallas kernels: 40.1 us -> 33.8 us
  waiting for transfers between devices: 131 us -> 128 us
    pallas_call x4 -> x3, Pallas kernels: 37 us -> 30.7 us  [expert(): pl.pallas_call(expert_kernel, grid=(steps,), in_specs=[whole] * 4 + [colu...]
    ppermute x14 -> x20, waiting for transfers between devices: 81.6 us -> 76.6 us  [swap(): return lax.ppermute(block, axis, [(i, i ^ mask) for i in range(count)])]
    all_to_all x4, starting transfers between devices: 60.9 us -> 56 us  [along_z(): return lax.all_to_all(packed, 'z', split_axis=0, concat_axis=0, tiled=True)]
    ppermute x14 -> x20, starting transfers between devices: 7.89 us -> 11 us  [swap(): return lax.ppermute(block, axis, [(i, i ^ mask) for i in range(count)])]
  transfers between devices with their start and end apart: 18 -> 24, of which waited for: 10 -> 12; matrix products, arithmetic and copies ran while one was open for 1% -> 2% of each run, Pallas kernels for 16% -> 14%
where the time goes in v4:
time: 246 us; the launch traced here: 244 us
  waiting for transfers between devices  128 us (52%)
  starting transfers between devices  67.1 us (27%)
  Pallas kernels  33.8 us (14%)
  matrix products  5.38 us (2%)
  local copies, waits for them, and re-layouts  4.92 us (2%)
  other arithmetic  4.51 us (2%)
    ppermute x20, waiting for transfers between devices, swap(): return lax.ppermute(block, axis, [(i, i ^ mask) for i in range(count)])  76.6 us
    all_to_all x4, starting transfers between devices, along_z(): return lax.all_to_all(packed, 'z', split_axis=0, concat_axis=0, tiled=True)  56 us
    all_to_all x4, waiting for transfers between devices, along_z(): return lax.all_to_all(packed, 'z', split_axis=0, concat_axis=0, tiled=True)  51.5 us
    pallas_call x3, Pallas kernels, expert(): pl.pallas_call(expert_kernel, grid=(steps,), in_specs=[whole] * 4 + [colu...  30.7 us
    ppermute x20, starting transfers between devices, swap(): return lax.ppermute(block, axis, [(i, i ^ mask) for i in range(count)])  11 us
  transfers between devices with their start and end apart: 24, of which 12 were waited for; matrix products, arithmetic and copies ran while one was open for 2% of the time, Pallas kernels for 14%

profile of v4, /device:TPU:34, one launch (start us, length us, event | category | flops | bytes accessed | tf_op | source)
XLA Modules:
  0.0 244.1 jit_solution(3745465371811344234)
XLA Ops:
  0.0 0.8 slice_bitcast_fusion.3
  1.0 0.8 compare_select_fusion.1
  1.8 1.2 fusion.6
  3.0 1.2 fusion.8
  4.3 1.5 convolution_convert_fusion.1
  5.8 24.0 %all-to-all-start = ((bf16[16,40,512]{2,1,0:T(8,128)(2,1)}), bf16[16,40,512]{2,1,0:T(8,128)(2,1)S(1)}, u32[]{:S(2)}, u32[]{:S(2)}) async-start(bf16[16,40,512]{2,1,0:T(8,128)(2,1)} %bitcast.5), calls=%async_computation | async-start | bytes 1310720 | tf_op jit(solution)/shard_map/all_to_all | solution.py:29
  29.8 0.7 convolution_convert_fusion
  30.5 1.8 collective-permute-start
  32.4 0.3 and_convert_fusion.refs_4_.refs_2_
  32.7 14.1 %collective-permute-done = bf16[16,40,512]{2,1,0:T(8,128)(2,1)S(1)} collective-permute-done((bf16[16,40,512]{2,1,0:T(8,128)(2,1)S(1)}, bf16[16,40,512]{2,1,0:T(8,128)(2,1)S(1)}, u32[]{:S(2)}, u32[]{:S(2)}) %collective-permute-start) | collective-permute-done | bytes 655392 | tf_op jit(solution)/shard_map/ppermute | solution.py:19
  46.9 16.6 %all-to-all-done = bf16[16,40,512]{2,1,0:T(8,128)(2,1)S(1)} async-done(((bf16[16,40,512]{2,1,0:T(8,128)(2,1)}), bf16[16,40,512]{2,1,0:T(8,128)(2,1)S(1)}, u32[]{:S(2)}, u32[]{:S(2)}) %all-to-all-start) | async-done | bytes 655392 | tf_op jit(solution)/shard_map/all_to_all | solution.py:29
  64.0 0.5 collective-permute-start.1
  64.9 1.7 collective-permute-start.5
  66.6 5.4 %collective-permute-done.1.refs_1_ = bf16[80,2048]{1,0:T(8,128)(2,1)S(1)} collective-permute-done((bf16[80,2048]{1,0:T(8,128)(2,1)S(1)}, bf16[80,2048]{1,0:T(8,128)(2,1)S(1)}, u32[]{:S(2)}, u32[]{:S(2)}) %collective-permute-start.1) | collective-permute-done | bytes 327712 | tf_op jit(solution)/shard_map/ppermute | solution.py:19
  72.0 0.5 collective-permute-start.6
  72.5 10.2 %all-to-all-start.1 = ((bf16[16,40,512]{2,1,0:T(8,128)(2,1)}), bf16[16,40,512]{2,1,0:T(8,128)(2,1)}, u32[]{:S(2)}, u32[]{:S(2)}) async-start(bf16[16,40,512]{2,1,0:T(8,128)(2,1)} %copy-done), calls=%async_computation.1 | async-start | bytes 1310720 | tf_op jit(solution)/shard_map/all_to_all | solution.py:29
  82.9 9.3 %shard_map.73 = (bf16[80,2048]{1,0:T(8,128)(2,1)S(1)}, bf16[80,2048]{1,0:T(8,128)(2,1)S(1)}, bf16[80,2048]{1,0:T(8,128)(2,1)S(1)}, bf16[80,2048]{1,0:T(8,128)(2,1)S(1)}) custom-call(bf16[80,2048]{1,0:T(8,128)(2,1)S(1)} %bitcast.75, bf16[80,2048]{1,0:T(8,128)(2,1)S(1)} %collective-permute-done.1.refs_1_, bf16[80,2048]{1,0:T(8,128)(2,1)S(1)} %collective-permute-done.2.refs_2_, ...), custom_call_target="tpu_custom_call" | custom-call | flops 3523215360 | bytes 13631488 | tf_op jit(solution)/shard_map/pallas_call | solution.py:77
  92.2 0.6 collective-permute-start.4
  92.8 0.3 collective-permute-start.9
  93.1 9.3 %shard_map.74 = (bf16[80,2048]{1,0:T(8,128)(2,1)S(1)}, bf16[80,2048]{1,0:T(8,128)(2,1)S(1)}, bf16[80,2048]{1,0:T(8,128)(2,1)S(1)}, bf16[80,2048]{1,0:T(8,128)(2,1)S(1)}) custom-call(bf16[80,2048]{1,0:T(8,128)(2,1)S(1)} %bitcast.72, bf16[80,2048]{1,0:T(8,128)(2,1)S(1)} %collective-permute-done.5.refs_1_, bf16[80,2048]{1,0:T(8,128)(2,1)S(1)} %collective-permute-done.6.refs_2_, ...), custom_call_target="tpu_custom_call" | custom-call | flops 3523215360 | bytes 13631488 | tf_op jit(solution)/shard_map/pallas_call | solution.py:77
  102.7 0.3 collective-permute-start.11
  103.1 0.5 collective-permute-start.10
  103.6 1.0 collective-permute-done.11
  104.7 0.8 collective-permute-start.12
  105.6 8.2 %collective-permute-done.10.refs_2_ = bf16[80,2048]{1,0:T(8,128)(2,1)S(1)} collective-permute-done((bf16[80,2048]{1,0:T(8,128)(2,1)S(1)}, bf16[80,2048]{1,0:T(8,128)(2,1)S(1)}, u32[]{:S(2)}, u32[]{:S(2)}) %collective-permute-start.10) | collective-permute-done | bytes 327712 | tf_op jit(solution)/shard_map/ppermute | solution.py:19
  113.8 6.2 %collective-permute-done.12.refs_3_ = bf16[80,2048]{1,0:T(8,128)(2,1)S(1)} collective-permute-done((bf16[80,2048]{1,0:T(8,128)(2,1)S(1)}, bf16[80,2048]{1,0:T(8,128)(2,1)S(1)}, u32[]{:S(2)}, u32[]{:S(2)}) %collective-permute-start.12) | collective-permute-done | bytes 327712 | tf_op jit(solution)/shard_map/ppermute | solution.py:19
  120.0 1.6 shard_map.75
  121.6 1.3 copy.24
  122.9 0.5 copy.25
  123.6 0.5 collective-permute-start.13
  124.1 15.6 %collective-permute-done.13.refs_1_ = bf16[160,2048]{1,0:T(8,128)(2,1)S(1)} collective-permute-done((bf16[160,2048]{1,0:T(8,128)(2,1)S(1)}, bf16[160,2048]{1,0:T(8,128)(2,1)S(1)}, u32[]{:S(2)}, u32[]{:S(2)}) %collective-permute-start.13) | collective-permute-done | bytes 655392 | tf_op jit(solution)/shard_map/ppermute | solution.py:19
  139.6 12.0 %all-to-all-start.2 = ((bf16[16,40,512]{2,1,0:T(8,128)(2,1)}), bf16[16,40,512]{2,1,0:T(8,128)(2,1)S(1)}, u32[]{:S(2)}, u32[]{:S(2)}) async-start(bf16[16,40,512]{2,1,0:T(8,128)(2,1)} %bitcast.12), calls=%async_computation.2 | async-start | bytes 1310720 | tf_op jit(solution)/shard_map/all_to_all | solution.py:29
  151.7 12.2 %shard_map.76 = (bf16[160,2048]{1,0:T(8,128)(2,1)S(1)}, bf16[160,2048]{1,0:T(8,128)(2,1)S(1)}, bf16[160,2048]{1,0:T(8,128)(2,1)S(1)}, bf16[160,2048]{1,0:T(8,128)(2,1)S(1)}) custom-call(bf16[160,2048]{1,0:T(8,128)(2,1)S(1)} %bitcast.69, bf16[160,2048]{1,0:T(8,128)(2,1)S(1)} %collective-permute-done.13.refs_1_, ...), custom_call_target="tpu_custom_call" | custom-call | flops 7046430720 | bytes 16252928 | tf_op jit(solution)/shard_map/pallas_call | solution.py:77
  163.9 0.3 collective-permute-start.17
  164.5 1.6 collective-permute-done.17
  166.3 0.7 collective-permute-start.18
  167.3 16.2 %collective-permute-done.18.refs_1_ = bf16[160,2048]{1,0:T(8,128)(2,1)S(1)} collective-permute-done((bf16[160,2048]{1,0:T(8,128)(2,1)S(1)}, bf16[160,2048]{1,0:T(8,128)(2,1)S(1)}, u32[]{:S(2)}, u32[]{:S(2)}) %collective-permute-start.18) | collective-permute-done | bytes 655392 | tf_op jit(solution)/shard_map/ppermute | solution.py:19
  183.5 1.6 shard_map.77
  185.1 2.3 all-to-all-done.2
  187.3 9.8 %all-to-all-start.3 = ((bf16[16,40,512]{2,1,0:T(8,128)(2,1)}), bf16[16,40,512]{2,1,0:T(8,128)(2,1)S(1)}, u32[]{:S(2)}, u32[]{:S(2)}) async-start(bf16[16,40,512]{2,1,0:T(8,128)(2,1)} %bitcast.15), calls=%async_computation.3 | async-start | bytes 1310720 | tf_op jit(solution)/shard_map/all_to_all | solution.py:29
  197.2 32.6 %all-to-all-done.3 = bf16[16,40,512]{2,1,0:T(8,128)(2,1)S(1)} async-done(((bf16[16,40,512]{2,1,0:T(8,128)(2,1)}), bf16[16,40,512]{2,1,0:T(8,128)(2,1)S(1)}, u32[]{:S(2)}, u32[]{:S(2)}) %all-to-all-start.3) | async-done | bytes 655392 | tf_op jit(solution)/shard_map/all_to_all | solution.py:29
  229.8 1.6 collective-permute-start.19
  231.5 0.8 fusion.9
  232.3 0.8 fusion.10
  233.1 8.3 %collective-permute-done.19 = bf16[16,40,512]{2,1,0:T(8,128)(2,1)S(1)} collective-permute-done((bf16[16,40,512]{2,1,0:T(8,128)(2,1)S(1)}, bf16[16,40,512]{2,1,0:T(8,128)(2,1)S(1)}, u32[]{:S(2)}, u32[]{:S(2)}) %collective-permute-start.19) | collective-permute-done | bytes 655392 | tf_op jit(solution)/shard_map/ppermute | solution.py:19
  241.3 0.8 fusion.2
  242.1 0.8 fusion.5
  243.1 1.0 copy.26
  (53 shorter events, 3.1 us)
Async XLA Ops:
  5.8 57.6 %all-to-all-start = ((bf16[16,40,512]{2,1,0:T(8,128)(2,1)}), bf16[16,40,512]{2,1,0:T(8,128)(2,1)S(1)}, u32[]{:S(2)}, u32[]{:S(2)}) async-start(bf16[16,40,512]{2,1,0:T(8,128)(2,1)} %bitcast.5), calls=%async_computation | async-start | bytes 1310720 | tf_op jit(solution)/shard_map/all_to_all | solution.py:29
  30.5 16.4 %collective-permute-start = (bf16[16,40,512]{2,1,0:T(8,128)(2,1)S(1)}, bf16[16,40,512]{2,1,0:T(8,128)(2,1)S(1)}, u32[]{:S(2)}, u32[]{:S(2)}) collective-permute-start(bf16[16,40,512]{2,1,0:T(8,128)(2,1)S(1)} %bitcast.85), channel_id=1, source_target_pairs={{0,6},{2,4},{4,2},{6,0},{1,7},{3,5},{5,3},{7,1},{8,14},{10,12},{12... | collective-permute-start | bytes 1966088 | tf_op jit(solution)/shard_map/ppermute | solution.py:19
  46.9 16.8 %copy-start = (bf16[16,40,512]{2,1,0:T(8,128)(2,1)}, bf16[16,40,512]{2,1,0:T(8,128)(2,1)S(1)}, u32[]{:S(2)}) copy-start(bf16[16,40,512]{2,1,0:T(8,128)(2,1)S(1)} %collective-permute-done) | copy-start | bytes 1966084
  64.0 8.0 %collective-permute-start.1 = (bf16[80,2048]{1,0:T(8,128)(2,1)S(1)}, bf16[80,2048]{1,0:T(8,128)(2,1)S(1)}, u32[]{:S(2)}, u32[]{:S(2)}) collective-permute-start(bf16[80,2048]{1,0:T(8,128)(2,1)S(1)} %bitcast.73), channel_id=1, source_target_pairs={{0,2},{2,0},{4,6},{6,4},{1,3},{3,1},{5,7},{7,5},{8,10},{10,8},{12,... | collective-permute-start | bytes 983048 | tf_op jit(solution)/shard_map/ppermute | solution.py:19
  64.9 17.8 %collective-permute-start.5 = (bf16[80,2048]{1,0:T(8,128)(2,1)S(1)}, bf16[80,2048]{1,0:T(8,128)(2,1)S(1)}, u32[]{:S(2)}, u32[]{:S(2)}) collective-permute-start(bf16[80,2048]{1,0:T(8,128)(2,1)S(1)} %bitcast.70), channel_id=1, source_target_pairs={{0,2},{2,0},{4,6},{6,4},{1,3},{3,1},{5,7},{7,5},{8,10},{10,8},{12,... | collective-permute-start | bytes 983048 | tf_op jit(solution)/shard_map/ppermute | solution.py:19
  66.6 16.2 %collective-permute-start.2 = (bf16[80,2048]{1,0:T(8,128)(2,1)S(1)}, bf16[80,2048]{1,0:T(8,128)(2,1)S(1)}, u32[]{:S(2)}, u32[]{:S(2)}) collective-permute-start(bf16[80,2048]{1,0:T(8,128)(2,1)S(1)} %bitcast.74), channel_id=1, source_target_pairs={{0,1},{1,0},{2,3},{3,2},{4,5},{5,4},{6,7},{7,6},{8,9},{9,8},{10,11... | collective-permute-start | bytes 983048 | tf_op jit(solution)/shard_map/ppermute | solution.py:19
  72.0 10.9 %collective-permute-start.3 = (bf16[80,2048]{1,0:T(8,128)(2,1)S(1)}, bf16[80,2048]{1,0:T(8,128)(2,1)S(1)}, u32[]{:S(2)}, u32[]{:S(2)}) collective-permute-start(bf16[80,2048]{1,0:T(8,128)(2,1)S(1)} %collective-permute-done.1.refs_1_), channel_id=1, source_target_pairs={{0,1},{1,0},{2,3},{3,2},{4,5},{5,4},{6,7},{7,6},{8,9},{9,8},{10,11... | collective-permute-start | bytes 983048 | tf_op jit(solution)/shard_map/ppermute | solution.py:19
  72.0 21.1 %collective-permute-start.6 = (bf16[80,2048]{1,0:T(8,128)(2,1)S(1)}, bf16[80,2048]{1,0:T(8,128)(2,1)S(1)}, u32[]{:S(2)}, u32[]{:S(2)}) collective-permute-start(bf16[80,2048]{1,0:T(8,128)(2,1)S(1)} %bitcast.71), channel_id=1, source_target_pairs={{0,1},{1,0},{2,3},{3,2},{4,5},{5,4},{6,7},{7,6},{8,9},{9,8},{10,11... | collective-permute-start | bytes 983048 | tf_op jit(solution)/shard_map/ppermute | solution.py:19
  72.5 49.1 %all-to-all-start.1 = ((bf16[16,40,512]{2,1,0:T(8,128)(2,1)}), bf16[16,40,512]{2,1,0:T(8,128)(2,1)}, u32[]{:S(2)}, u32[]{:S(2)}) async-start(bf16[16,40,512]{2,1,0:T(8,128)(2,1)} %copy-done), calls=%async_computation.1 | async-start | bytes 1310720 | tf_op jit(solution)/shard_map/all_to_all | solution.py:29
  82.7 10.4 %collective-permute-start.7 = (bf16[80,2048]{1,0:T(8,128)(2,1)S(1)}, bf16[80,2048]{1,0:T(8,128)(2,1)S(1)}, u32[]{:S(2)}, u32[]{:S(2)}) collective-permute-start(bf16[80,2048]{1,0:T(8,128)(2,1)S(1)} %collective-permute-done.5.refs_1_), channel_id=1, source_target_pairs={{0,1},{1,0},{2,3},{3,2},{4,5},{5,4},{6,7},{7,6},{8,9},{9,8},{10,11... | collective-permute-start | bytes 983048 | tf_op jit(solution)/shard_map/ppermute | solution.py:19
  92.2 13.3 %collective-permute-start.4 = (bf16[80,2048]{1,0:T(8,128)(2,1)S(1)}, bf16[80,2048]{1,0:T(8,128)(2,1)S(1)}, u32[]{:S(2)}, u32[]{:S(2)}) collective-permute-start(bf16[80,2048]{1,0:T(8,128)(2,1)S(1)} %get-tuple-element.27), channel_id=1, source_target_pairs={{0,1},{1,0},{2,3},{3,2},{4,5},{5,4},{6,7},{7,6},{8,9},{9,8},{10,11... | collective-permute-start | bytes 983048 | tf_op jit(solution)/shard_map/ppermute | solution.py:19
  92.8 10.2 %collective-permute-start.9 = (bf16[80,2048]{1,0:T(8,128)(2,1)S(1)}, bf16[80,2048]{1,0:T(8,128)(2,1)S(1)}, u32[]{:S(2)}, u32[]{:S(2)}) collective-permute-start(bf16[80,2048]{1,0:T(8,128)(2,1)S(1)} %get-tuple-element.31), channel_id=1, source_target_pairs={{0,1},{1,0},{2,3},{3,2},{4,5},{5,4},{6,7},{7,6},{8,9},{9,8},{10,11... | collective-permute-start | bytes 983048 | tf_op jit(solution)/shard_map/ppermute | solution.py:19
  102.4 3.2 %collective-permute-start.8 = (bf16[80,2048]{1,0:T(8,128)(2,1)S(1)}, bf16[80,2048]{1,0:T(8,128)(2,1)S(1)}, u32[]{:S(2)}, u32[]{:S(2)}) collective-permute-start(bf16[80,2048]{1,0:T(8,128)(2,1)S(1)} %get-tuple-element.29), channel_id=1, source_target_pairs={{0,1},{1,0},{2,3},{3,2},{4,5},{5,4},{6,7},{7,6},{8,9},{9,8},{10,11... | collective-permute-start | bytes 983048 | tf_op jit(solution)/shard_map/ppermute | solution.py:19
  102.7 1.9 collective-permute-start.11
  103.1 10.7 %collective-permute-start.10 = (bf16[80,2048]{1,0:T(8,128)(2,1)S(1)}, bf16[80,2048]{1,0:T(8,128)(2,1)S(1)}, u32[]{:S(2)}, u32[]{:S(2)}) collective-permute-start(bf16[80,2048]{1,0:T(8,128)(2,1)S(1)} %add_convert_fusion.3), channel_id=1, source_target_pairs={{0,2},{2,0},{4,6},{6,4},{1,3},{3,1},{5,7},{7,5},{8,10},{10,8},{12,... | collective-permute-start | bytes 983048 | tf_op jit(solution)/shard_map/ppermute | solution.py:19
  104.7 15.4 %collective-permute-start.12 = (bf16[80,2048]{1,0:T(8,128)(2,1)S(1)}, bf16[80,2048]{1,0:T(8,128)(2,1)S(1)}, u32[]{:S(2)}, u32[]{:S(2)}) collective-permute-start(bf16[80,2048]{1,0:T(8,128)(2,1)S(1)} %add_convert_fusion.2), channel_id=1, source_target_pairs={{0,2},{2,0},{4,6},{6,4},{1,3},{3,1},{5,7},{7,5},{8,10},{10,8},{12,... | collective-permute-start | bytes 983048 | tf_op jit(solution)/shard_map/ppermute | solution.py:19
  123.6 16.1 %collective-permute-start.13 = (bf16[160,2048]{1,0:T(8,128)(2,1)S(1)}, bf16[160,2048]{1,0:T(8,128)(2,1)S(1)}, u32[]{:S(2)}, u32[]{:S(2)}) collective-permute-start(bf16[160,2048]{1,0:T(8,128)(2,1)S(1)} %bitcast.67), channel_id=1, source_target_pairs={{0,2},{2,0},{4,6},{6,4},{1,3},{3,1},{5,7},{7,5},{8,10},{10,8},{12,... | collective-permute-start | bytes 1966088 | tf_op jit(solution)/shard_map/ppermute | solution.py:19
  124.1 27.6 %collective-permute-start.14 = (bf16[160,2048]{1,0:T(8,128)(2,1)S(1)}, bf16[160,2048]{1,0:T(8,128)(2,1)}, u32[]{:S(2)}, u32[]{:S(2)}) collective-permute-start(bf16[160,2048]{1,0:T(8,128)(2,1)S(1)} %bitcast.68), channel_id=1, source_target_pairs={{0,1},{1,0},{2,3},{3,2},{4,5},{5,4},{6,7},{7,6},{8,9},{9,8},{10,11... | collective-permute-start | bytes 1966088 | tf_op jit(solution)/shard_map/ppermute | solution.py:19
  139.6 12.1 %collective-permute-start.15 = (bf16[160,2048]{1,0:T(8,128)(2,1)S(1)}, bf16[160,2048]{1,0:T(8,128)(2,1)}, u32[]{:S(2)}, u32[]{:S(2)}) collective-permute-start(bf16[160,2048]{1,0:T(8,128)(2,1)S(1)} %collective-permute-done.13.refs_1_), channel_id=1, source_target_pairs={{0,1},{1,0},{2,3},{3,2},{4,5},{5,4},{6,7},{7,6},{8,9},{9,8},{10,11... | collective-permute-start | bytes 1966088 | tf_op jit(solution)/shard_map/ppermute | solution.py:19
  139.6 47.7 %all-to-all-start.2 = ((bf16[16,40,512]{2,1,0:T(8,128)(2,1)}), bf16[16,40,512]{2,1,0:T(8,128)(2,1)S(1)}, u32[]{:S(2)}, u32[]{:S(2)}) async-start(bf16[16,40,512]{2,1,0:T(8,128)(2,1)} %bitcast.12), calls=%async_computation.2 | async-start | bytes 1310720 | tf_op jit(solution)/shard_map/all_to_all | solution.py:29
  163.9 2.2 collective-permute-start.17
  164.2 2.8 %collective-permute-start.16 = (bf16[160,2048]{1,0:T(8,128)(2,1)S(1)}, bf16[160,2048]{1,0:T(8,128)(2,1)S(1)}, u32[]{:S(2)}, u32[]{:S(2)}) collective-permute-start(bf16[160,2048]{1,0:T(8,128)(2,1)S(1)} %get-tuple-element.38), channel_id=1, source_target_pairs={{0,1},{1,0},{2,3},{3,2},{4,5},{5,4},{6,7},{7,6},{8,9},{9,8},{10,11... | collective-permute-start | bytes 1966088 | tf_op jit(solution)/shard_map/ppermute | solution.py:19
  166.3 17.2 %collective-permute-start.18 = (bf16[160,2048]{1,0:T(8,128)(2,1)S(1)}, bf16[160,2048]{1,0:T(8,128)(2,1)S(1)}, u32[]{:S(2)}, u32[]{:S(2)}) collective-permute-start(bf16[160,2048]{1,0:T(8,128)(2,1)S(1)} %add_convert_fusion), channel_id=1, source_target_pairs={{0,2},{2,0},{4,6},{6,4},{1,3},{3,1},{5,7},{7,5},{8,10},{10,8},{12,... | collective-permute-start | bytes 1966088 | tf_op jit(solution)/shard_map/ppermute | solution.py:19
  185.1 12.1 %copy-start.1 = (f32[128,2]{0,1:T(2,128)S(1)}, f32[128,2]{0,1:T(2,128)}, u32[]{:S(2)}) copy-start(f32[128,2]{0,1:T(2,128)} %param.10) | copy-start | bytes 3076
  187.3 42.5 %all-to-all-start.3 = ((bf16[16,40,512]{2,1,0:T(8,128)(2,1)}), bf16[16,40,512]{2,1,0:T(8,128)(2,1)S(1)}, u32[]{:S(2)}, u32[]{:S(2)}) async-start(bf16[16,40,512]{2,1,0:T(8,128)(2,1)} %bitcast.15), calls=%async_computation.3 | async-start | bytes 1310720 | tf_op jit(solution)/shard_map/all_to_all | solution.py:29
  229.8 11.5 %collective-permute-start.19 = (bf16[16,40,512]{2,1,0:T(8,128)(2,1)S(1)}, bf16[16,40,512]{2,1,0:T(8,128)(2,1)S(1)}, u32[]{:S(2)}, u32[]{:S(2)}) collective-permute-start(bf16[16,40,512]{2,1,0:T(8,128)(2,1)S(1)} %all-to-all-done.3), channel_id=1, source_target_pairs={{0,6},{2,4},{4,2},{6,0},{1,7},{3,5},{5,3},{7,1},{8,14},{10,12},{12... | collective-permute-start | bytes 1966088 | tf_op jit(solution)/shard_map/ppermute | solution.py:19

commit v5 on v4

--- a/solution.py
+++ b/solution.py
@@ -8,9 +8,10 @@
 
 
 ROW = 4
-TILE = 128
+DEPTH = 512
+GATED = 32
 FFN_LIMIT = 50
-COLUMNS = 512
+COLUMNS = 1024
 SPLIT = 4
 
 
@@ -35,9 +36,9 @@
 
 def expert_kernel(*refs):
     ins, (w_gate, w_up, w_down), outs = refs[:4], refs[4:7], refs[7:11]
-    rows, hidden, down, sem = refs[11:]
+    rows, sums, hidden, down, sem = refs[11:]
     step, steps = pl.program_id(0), pl.num_programs(0)
-    count, tile = ins[0].shape[0], w_gate.shape[1]
+    count, (depth, units) = ins[0].shape[0], w_gate.shape
     load = pltpu.make_async_copy(w_down, down, sem)
 
     @pl.when(step == 0)
@@ -45,44 +46,54 @@
         load.start()
         for i, source in enumerate(ins):
             rows[i * count : (i + 1) * count] = source[...]
-
-    both = jnp.dot(
-        rows[...],
+        sums[...] = jnp.zeros_like(sums)
+
+    sums[...] += jnp.dot(
+        rows[:, pl.ds(pl.multiple_of(step * depth, depth), depth)],
         jnp.concatenate([w_gate[...], w_up[...]], axis=1),
         preferred_element_type=jnp.float32,
     )
-    gate, up = both[:, :tile], both[:, tile:]
-    hidden[step] = (gate / (1.0 + jnp.exp(-gate)) * up).astype(jnp.bfloat16)
 
     @pl.when(step == steps - 1)
     def _():
+        def gated(i, carry):
+            some = pl.ds(pl.multiple_of(i * GATED, GATED), GATED)
+            gate, up = sums[some, :units], sums[some, units:]
+            hidden[some] = (gate / (1.0 + jnp.exp(-gate)) * up).astype(jnp.bfloat16)
+            return carry
+
+        lax.fori_loop(0, hidden.shape[0] // GATED, gated, 0)
         load.wait()
-        units = jnp.concatenate([hidden[i] for i in range(hidden.shape[0])], axis=1)
-        for first in range(0, down.shape[1], COLUMNS):
+
+        def lowered(i, carry):
+            some = pl.ds(pl.multiple_of(i * COLUMNS, COLUMNS), COLUMNS)
             part = jnp.dot(
-                units, down[:, first : first + COLUMNS], preferred_element_type=jnp.float32
+                hidden[...], down[:, some], preferred_element_type=jnp.float32
             ).astype(jnp.bfloat16)
-            for i, target in enumerate(outs):
-                target[:, first : first + COLUMNS] = part[i * count : (i + 1) * count]
+            for j, target in enumerate(outs):
+                target[:, some] = part[j * count : (j + 1) * count]
+            return carry
+
+        lax.fori_loop(0, down.shape[1] // COLUMNS, lowered, 0)
 
 
 def expert(blocks, w_gate, w_up, w_down):
     count, model_width = blocks[0].shape
     units = w_gate.shape[1]
-    steps = units // TILE
     total = len(blocks) * count
     whole = pl.BlockSpec((count, model_width), lambda i: (0, 0))
-    columns = pl.BlockSpec((model_width, TILE), lambda i: (0, i))
+    deep = pl.BlockSpec((DEPTH, units), lambda i: (i, 0))
     out = jax.ShapeDtypeStruct((count, model_width), jnp.bfloat16)
     return pl.pallas_call(
         expert_kernel,
-        grid=(steps,),
-        in_specs=[whole] * 4 + [columns, columns, pl.BlockSpec(memory_space=pl.ANY)],
+        grid=(model_width // DEPTH,),
+        in_specs=[whole] * 4 + [deep, deep, pl.BlockSpec(memory_space=pl.ANY)],
         out_specs=[whole] * 4,
         out_shape=[out] * 4,
         scratch_shapes=[
             pltpu.VMEM((total, model_width), jnp.bfloat16),
-            pltpu.VMEM((steps, total, TILE), jnp.bfloat16),
+            pltpu.VMEM((total, 2 * units), jnp.float32),
+            pltpu.VMEM((total, units), jnp.bfloat16),
             pltpu.VMEM((units, model_width), jnp.bfloat16),
             pltpu.SemaphoreType.DMA,
         ],
@@ -201,7 +212,7 @@
     near_out = merge(own, theirs, order, nz)
     far, near_out = lax.optimization_barrier((far, near_out))
     near_back = along_z(near_out)
-    own, theirs = through_row(far, weights, capacity, 1)
+    own, theirs = through_row(far, weights, capacity, 2)
     far_out = merge(own, theirs, order, nz)
     near_back, far_out = lax.optimization_barrier((near_back, far_out))
     far_back = along_z(far_out)

time: 246 us -> 242 us (0.984)
  waiting for transfers between devices: 128 us -> 114 us
  starting transfers between devices: 67.1 us -> 73.3 us
    ppermute x20 -> x26, waiting for transfers between devices: 76.6 us -> 64.5 us  [swap(): return lax.ppermute(block, axis, [(i, i ^ mask) for i in range(count)])]
    ppermute x20 -> x26, starting transfers between devices: 11 us -> 14.9 us  [swap(): return lax.ppermute(block, axis, [(i, i ^ mask) for i in range(count)])]
    pallas_call x3 -> x4, Pallas kernels: 30.7 us -> 31.8 us  [expert(): pl.pallas_call(expert_kernel, grid=(model_width // DEPTH,), in_specs=[who...]
  transfers between devices with their start and end apart: 24 -> 30, of which waited for: 12 -> 12; matrix products, arithmetic and copies ran while one was open for 2% -> 3% of each run, Pallas kernels for 14% -> 15%
where the time goes in v5:
time: 242 us; the launch traced here: 239 us
  waiting for transfers between devices  114 us (47%)
  starting transfers between devices  73.3 us (30%)
  Pallas kernels  35 us (14%)
  matrix products  7.55 us (3%)
  local copies, waits for them, and re-layouts  4.97 us (2%)
  other arithmetic  4.43 us (2%)
    ppermute x26, waiting for transfers between devices, swap(): return lax.ppermute(block, axis, [(i, i ^ mask) for i in range(count)])  64.5 us
    all_to_all x4, starting transfers between devices, along_z(): return lax.all_to_all(packed, 'z', split_axis=0, concat_axis=0, tiled=True)  58.4 us
    all_to_all x4, waiting for transfers between devices, along_z(): return lax.all_to_all(packed, 'z', split_axis=0, concat_axis=0, tiled=True)  49.2 us
    pallas_call x4, Pallas kernels, expert(): pl.pallas_call(expert_kernel, grid=(model_width // DEPTH,), in_specs=[who...  31.8 us
    ppermute x26, starting transfers between devices, swap(): return lax.ppermute(block, axis, [(i, i ^ mask) for i in range(count)])  14.9 us
    dot_general x4, matrix products, local(): jnp.dot(select, back.reshape(-1, width), preferred_element_type=jnp.float32)  5.36 us
  transfers between devices with their start and end apart: 30, of which 12 were waited for; matrix products, arithmetic and copies ran while one was open for 3% of the time, Pallas kernels for 15%

profile of v5, /device:TPU:34, one launch (start us, length us, event | category | flops | bytes accessed | tf_op | source)
XLA Modules:
  0.0 239.3 jit_solution(5840355224155856001)
XLA Ops:
  0.0 1.2 fusion.6
  1.3 0.8 slice_bitcast_fusion.3
  2.2 0.8 compare_select_fusion.1
  3.0 1.2 fusion.8
  4.3 1.5 convolution_convert_fusion.1
  5.8 24.0 %all-to-all-start = ((bf16[16,40,512]{2,1,0:T(8,128)(2,1)}), bf16[16,40,512]{2,1,0:T(8,128)(2,1)S(1)}, u32[]{:S(2)}, u32[]{:S(2)}) async-start(bf16[16,40,512]{2,1,0:T(8,128)(2,1)} %bitcast.5), calls=%async_computation | async-start | bytes 1310720 | tf_op jit(solution)/shard_map/all_to_all | solution.py:30
  29.8 0.7 convolution_convert_fusion
  30.5 1.8 collective-permute-start
  32.7 14.1 %collective-permute-done = bf16[16,40,512]{2,1,0:T(8,128)(2,1)S(1)} collective-permute-done((bf16[16,40,512]{2,1,0:T(8,128)(2,1)S(1)}, bf16[16,40,512]{2,1,0:T(8,128)(2,1)S(1)}, u32[]{:S(2)}, u32[]{:S(2)}) %collective-permute-start) | collective-permute-done | bytes 655392 | tf_op jit(solution)/shard_map/ppermute | solution.py:20
  46.9 16.6 %all-to-all-done = bf16[16,40,512]{2,1,0:T(8,128)(2,1)S(1)} async-done(((bf16[16,40,512]{2,1,0:T(8,128)(2,1)}), bf16[16,40,512]{2,1,0:T(8,128)(2,1)S(1)}, u32[]{:S(2)}, u32[]{:S(2)}) %all-to-all-start) | async-done | bytes 655392 | tf_op jit(solution)/shard_map/all_to_all | solution.py:30
  64.0 0.5 collective-permute-start.1
  64.9 1.7 collective-permute-start.5
  66.6 5.4 %collective-permute-done.1.refs_1_ = bf16[80,2048]{1,0:T(8,128)(2,1)S(1)} collective-permute-done((bf16[80,2048]{1,0:T(8,128)(2,1)S(1)}, bf16[80,2048]{1,0:T(8,128)(2,1)S(1)}, u32[]{:S(2)}, u32[]{:S(2)}) %collective-permute-start.1) | collective-permute-done | bytes 327712 | tf_op jit(solution)/shard_map/ppermute | solution.py:20
  72.0 0.5 collective-permute-start.6
  72.5 10.2 %all-to-all-start.1 = ((bf16[16,40,512]{2,1,0:T(8,128)(2,1)}), bf16[16,40,512]{2,1,0:T(8,128)(2,1)}, u32[]{:S(2)}, u32[]{:S(2)}) async-start(bf16[16,40,512]{2,1,0:T(8,128)(2,1)} %copy-done), calls=%async_computation.1 | async-start | bytes 1310720 | tf_op jit(solution)/shard_map/all_to_all | solution.py:30
  82.9 8.0 %shard_map.73 = (bf16[80,2048]{1,0:T(8,128)(2,1)S(1)}, bf16[80,2048]{1,0:T(8,128)(2,1)S(1)}, bf16[80,2048]{1,0:T(8,128)(2,1)S(1)}, bf16[80,2048]{1,0:T(8,128)(2,1)S(1)}) custom-call(bf16[80,2048]{1,0:T(8,128)(2,1)S(1)} %bitcast.78, bf16[80,2048]{1,0:T(8,128)(2,1)S(1)} %collective-permute-done.1.refs_1_, bf16[80,2048]{1,0:T(8,128)(2,1)S(1)} %collective-permute-done.2.refs_2_, ...), custom_call_target="tpu_custom_call" | custom-call | flops 3523215360 | bytes 13631488 | tf_op jit(solution)/shard_map/pallas_call | solution.py:87
  90.9 0.6 collective-permute-start.4
  91.8 7.9 %shard_map.74 = (bf16[80,2048]{1,0:T(8,128)(2,1)S(1)}, bf16[80,2048]{1,0:T(8,128)(2,1)S(1)}, bf16[80,2048]{1,0:T(8,128)(2,1)S(1)}, bf16[80,2048]{1,0:T(8,128)(2,1)S(1)}) custom-call(bf16[80,2048]{1,0:T(8,128)(2,1)S(1)} %bitcast.72, bf16[80,2048]{1,0:T(8,128)(2,1)S(1)} %collective-permute-done.5.refs_1_, bf16[80,2048]{1,0:T(8,128)(2,1)S(1)} %collective-permute-done.6.refs_2_, ...), custom_call_target="tpu_custom_call" | custom-call | flops 3523215360 | bytes 13631488 | tf_op jit(solution)/shard_map/pallas_call | solution.py:87
  100.5 0.5 collective-permute-start.10
  101.0 1.0 collective-permute-done.11
  102.1 0.8 collective-permute-start.12
  103.0 8.2 %collective-permute-done.10.refs_2_ = bf16[80,2048]{1,0:T(8,128)(2,1)S(1)} collective-permute-done((bf16[80,2048]{1,0:T(8,128)(2,1)S(1)}, bf16[80,2048]{1,0:T(8,128)(2,1)S(1)}, u32[]{:S(2)}, u32[]{:S(2)}) %collective-permute-start.10) | collective-permute-done | bytes 327712 | tf_op jit(solution)/shard_map/ppermute | solution.py:20
  111.2 6.2 %collective-permute-done.12.refs_3_ = bf16[80,2048]{1,0:T(8,128)(2,1)S(1)} collective-permute-done((bf16[80,2048]{1,0:T(8,128)(2,1)S(1)}, bf16[80,2048]{1,0:T(8,128)(2,1)S(1)}, u32[]{:S(2)}, u32[]{:S(2)}) %collective-permute-start.12) | collective-permute-done | bytes 327712 | tf_op jit(solution)/shard_map/ppermute | solution.py:20
  117.4 1.6 shard_map.75
  119.0 1.3 copy.26
  120.7 0.5 collective-permute-start.13
  121.5 1.8 collective-permute-start.17
  123.3 8.1 %collective-permute-done.13.refs_1_ = bf16[80,2048]{1,0:T(8,128)(2,1)S(1)} collective-permute-done((bf16[80,2048]{1,0:T(8,128)(2,1)S(1)}, bf16[80,2048]{1,0:T(8,128)(2,1)S(1)}, u32[]{:S(2)}, u32[]{:S(2)}) %collective-permute-start.13) | collective-permute-done | bytes 327712 | tf_op jit(solution)/shard_map/ppermute | solution.py:20
  131.4 0.5 collective-permute-start.18
  131.9 12.0 %all-to-all-start.2 = ((bf16[16,40,512]{2,1,0:T(8,128)(2,1)}), bf16[16,40,512]{2,1,0:T(8,128)(2,1)}, u32[]{:S(2)}, u32[]{:S(2)}) async-start(bf16[16,40,512]{2,1,0:T(8,128)(2,1)} %bitcast.12), calls=%async_computation.2 | async-start | bytes 1310720 | tf_op jit(solution)/shard_map/all_to_all | solution.py:30
  144.1 8.0 %shard_map.76 = (bf16[80,2048]{1,0:T(8,128)(2,1)S(1)}, bf16[80,2048]{1,0:T(8,128)(2,1)S(1)}, bf16[80,2048]{1,0:T(8,128)(2,1)S(1)}, bf16[80,2048]{1,0:T(8,128)(2,1)S(1)}) custom-call(bf16[80,2048]{1,0:T(8,128)(2,1)S(1)} %bitcast.81, bf16[80,2048]{1,0:T(8,128)(2,1)S(1)} %collective-permute-done.13.refs_1_, ...), custom_call_target="tpu_custom_call" | custom-call | flops 3523215360 | bytes 13631488 | tf_op jit(solution)/shard_map/pallas_call | solution.py:87
  152.1 0.6 collective-permute-start.16
  153.0 8.0 %shard_map.77 = (bf16[80,2048]{1,0:T(8,128)(2,1)S(1)}, bf16[80,2048]{1,0:T(8,128)(2,1)S(1)}, bf16[80,2048]{1,0:T(8,128)(2,1)S(1)}, bf16[80,2048]{1,0:T(8,128)(2,1)S(1)}) custom-call(bf16[80,2048]{1,0:T(8,128)(2,1)S(1)} %bitcast.75, bf16[80,2048]{1,0:T(8,128)(2,1)S(1)} %collective-permute-done.17.refs_1_, ...), custom_call_target="tpu_custom_call" | custom-call | flops 3523215360 | bytes 13631488 | tf_op jit(solution)/shard_map/pallas_call | solution.py:87
  161.7 0.5 collective-permute-start.22
  162.2 1.0 collective-permute-done.23
  163.3 0.8 collective-permute-start.24
  164.3 8.2 %collective-permute-done.22.refs_2_ = bf16[80,2048]{1,0:T(8,128)(2,1)S(1)} collective-permute-done((bf16[80,2048]{1,0:T(8,128)(2,1)S(1)}, bf16[80,2048]{1,0:T(8,128)(2,1)S(1)}, u32[]{:S(2)}, u32[]{:S(2)}) %collective-permute-start.22) | collective-permute-done | bytes 327712 | tf_op jit(solution)/shard_map/ppermute | solution.py:20
  172.4 6.2 %collective-permute-done.24.refs_3_ = bf16[80,2048]{1,0:T(8,128)(2,1)S(1)} collective-permute-done((bf16[80,2048]{1,0:T(8,128)(2,1)S(1)}, bf16[80,2048]{1,0:T(8,128)(2,1)S(1)}, u32[]{:S(2)}, u32[]{:S(2)}) %collective-permute-start.24) | collective-permute-done | bytes 327712 | tf_op jit(solution)/shard_map/ppermute | solution.py:20
  178.6 1.6 shard_map.78
  180.2 12.2 %all-to-all-start.3 = ((bf16[16,40,512]{2,1,0:T(8,128)(2,1)}), bf16[16,40,512]{2,1,0:T(8,128)(2,1)S(1)}, u32[]{:S(2)}, u32[]{:S(2)}) async-start(bf16[16,40,512]{2,1,0:T(8,128)(2,1)} %bitcast.16), calls=%async_computation.3 | async-start | bytes 1310720 | tf_op jit(solution)/shard_map/all_to_all | solution.py:30
  192.4 32.7 %all-to-all-done.3 = bf16[16,40,512]{2,1,0:T(8,128)(2,1)S(1)} async-done(((bf16[16,40,512]{2,1,0:T(8,128)(2,1)}), bf16[16,40,512]{2,1,0:T(8,128)(2,1)S(1)}, u32[]{:S(2)}, u32[]{:S(2)}) %all-to-all-start.3) | async-done | bytes 655392 | tf_op jit(solution)/shard_map/all_to_all | solution.py:30
  225.0 1.6 collective-permute-start.25
  226.7 1.9 fusion.10
  228.6 1.9 fusion.9
  230.5 6.1 %collective-permute-done.25 = bf16[16,40,512]{2,1,0:T(8,128)(2,1)S(1)} collective-permute-done((bf16[16,40,512]{2,1,0:T(8,128)(2,1)S(1)}, bf16[16,40,512]{2,1,0:T(8,128)(2,1)S(1)}, u32[]{:S(2)}, u32[]{:S(2)}) %collective-permute-start.25) | collective-permute-done | bytes 655392 | tf_op jit(solution)/shard_map/ppermute | solution.py:20
  236.5 0.8 fusion.2
  237.3 0.8 fusion.5
  238.3 1.0 copy.29
  (71 shorter events, 5.4 us)
Async XLA Ops:
  5.8 57.6 %all-to-all-start = ((bf16[16,40,512]{2,1,0:T(8,128)(2,1)}), bf16[16,40,512]{2,1,0:T(8,128)(2,1)S(1)}, u32[]{:S(2)}, u32[]{:S(2)}) async-start(bf16[16,40,512]{2,1,0:T(8,128)(2,1)} %bitcast.5), calls=%async_computation | async-start | bytes 1310720 | tf_op jit(solution)/shard_map/all_to_all | solution.py:30
  30.5 16.4 %collective-permute-start = (bf16[16,40,512]{2,1,0:T(8,128)(2,1)S(1)}, bf16[16,40,512]{2,1,0:T(8,128)(2,1)S(1)}, u32[]{:S(2)}, u32[]{:S(2)}) collective-permute-start(bf16[16,40,512]{2,1,0:T(8,128)(2,1)S(1)} %bitcast.90), channel_id=1, source_target_pairs={{0,6},{2,4},{4,2},{6,0},{1,7},{3,5},{5,3},{7,1},{8,14},{10,12},{12... | collective-permute-start | bytes 1966088 | tf_op jit(solution)/shard_map/ppermute | solution.py:20
  46.9 16.8 %copy-start = (bf16[16,40,512]{2,1,0:T(8,128)(2,1)}, bf16[16,40,512]{2,1,0:T(8,128)(2,1)S(1)}, u32[]{:S(2)}) copy-start(bf16[16,40,512]{2,1,0:T(8,128)(2,1)S(1)} %collective-permute-done) | copy-start | bytes 1966084
  64.0 8.0 %collective-permute-start.1 = (bf16[80,2048]{1,0:T(8,128)(2,1)S(1)}, bf16[80,2048]{1,0:T(8,128)(2,1)S(1)}, u32[]{:S(2)}, u32[]{:S(2)}) collective-permute-start(bf16[80,2048]{1,0:T(8,128)(2,1)S(1)} %bitcast.76), channel_id=1, source_target_pairs={{0,2},{2,0},{4,6},{6,4},{1,3},{3,1},{5,7},{7,5},{8,10},{10,8},{12,... | collective-permute-start | bytes 983048 | tf_op jit(solution)/shard_map/ppermute | solution.py:20
  64.9 17.8 %collective-permute-start.5 = (bf16[80,2048]{1,0:T(8,128)(2,1)S(1)}, bf16[80,2048]{1,0:T(8,128)(2,1)S(1)}, u32[]{:S(2)}, u32[]{:S(2)}) collective-permute-start(bf16[80,2048]{1,0:T(8,128)(2,1)S(1)} %bitcast.70), channel_id=1, source_target_pairs={{0,2},{2,0},{4,6},{6,4},{1,3},{3,1},{5,7},{7,5},{8,10},{10,8},{12,... | collective-permute-start | bytes 983048 | tf_op jit(solution)/shard_map/ppermute | solution.py:20
  66.6 16.2 %collective-permute-start.2 = (bf16[80,2048]{1,0:T(8,128)(2,1)S(1)}, bf16[80,2048]{1,0:T(8,128)(2,1)S(1)}, u32[]{:S(2)}, u32[]{:S(2)}) collective-permute-start(bf16[80,2048]{1,0:T(8,128)(2,1)S(1)} %bitcast.77), channel_id=1, source_target_pairs={{0,1},{1,0},{2,3},{3,2},{4,5},{5,4},{6,7},{7,6},{8,9},{9,8},{10,11... | collective-permute-start | bytes 983048 | tf_op jit(solution)/shard_map/ppermute | solution.py:20
  72.0 10.9 %collective-permute-start.3 = (bf16[80,2048]{1,0:T(8,128)(2,1)S(1)}, bf16[80,2048]{1,0:T(8,128)(2,1)S(1)}, u32[]{:S(2)}, u32[]{:S(2)}) collective-permute-start(bf16[80,2048]{1,0:T(8,128)(2,1)S(1)} %collective-permute-done.1.refs_1_), channel_id=1, source_target_pairs={{0,1},{1,0},{2,3},{3,2},{4,5},{5,4},{6,7},{7,6},{8,9},{9,8},{10,11... | collective-permute-start | bytes 983048 | tf_op jit(solution)/shard_map/ppermute | solution.py:20
  72.0 19.8 %collective-permute-start.6 = (bf16[80,2048]{1,0:T(8,128)(2,1)S(1)}, bf16[80,2048]{1,0:T(8,128)(2,1)S(1)}, u32[]{:S(2)}, u32[]{:S(2)}) collective-permute-start(bf16[80,2048]{1,0:T(8,128)(2,1)S(1)} %bitcast.71), channel_id=1, source_target_pairs={{0,1},{1,0},{2,3},{3,2},{4,5},{5,4},{6,7},{7,6},{8,9},{9,8},{10,11... | collective-permute-start | bytes 983048 | tf_op jit(solution)/shard_map/ppermute | solution.py:20
  72.5 46.5 %all-to-all-start.1 = ((bf16[16,40,512]{2,1,0:T(8,128)(2,1)}), bf16[16,40,512]{2,1,0:T(8,128)(2,1)}, u32[]{:S(2)}, u32[]{:S(2)}) async-start(bf16[16,40,512]{2,1,0:T(8,128)(2,1)} %copy-done), calls=%async_computation.1 | async-start | bytes 1310720 | tf_op jit(solution)/shard_map/all_to_all | solution.py:30
  82.7 9.1 %collective-permute-start.7 = (bf16[80,2048]{1,0:T(8,128)(2,1)S(1)}, bf16[80,2048]{1,0:T(8,128)(2,1)S(1)}, u32[]{:S(2)}, u32[]{:S(2)}) collective-permute-start(bf16[80,2048]{1,0:T(8,128)(2,1)S(1)} %collective-permute-done.5.refs_1_), channel_id=1, source_target_pairs={{0,1},{1,0},{2,3},{3,2},{4,5},{5,4},{6,7},{7,6},{8,9},{9,8},{10,11... | collective-permute-start | bytes 983048 | tf_op jit(solution)/shard_map/ppermute | solution.py:20
  90.9 12.0 %collective-permute-start.4 = (bf16[80,2048]{1,0:T(8,128)(2,1)S(1)}, bf16[80,2048]{1,0:T(8,128)(2,1)S(1)}, u32[]{:S(2)}, u32[]{:S(2)}) collective-permute-start(bf16[80,2048]{1,0:T(8,128)(2,1)S(1)} %get-tuple-element.31), channel_id=1, source_target_pairs={{0,1},{1,0},{2,3},{3,2},{4,5},{5,4},{6,7},{7,6},{8,9},{9,8},{10,11... | collective-permute-start | bytes 983048 | tf_op jit(solution)/shard_map/ppermute | solution.py:20
  91.5 8.9 %collective-permute-start.9 = (bf16[80,2048]{1,0:T(8,128)(2,1)S(1)}, bf16[80,2048]{1,0:T(8,128)(2,1)S(1)}, u32[]{:S(2)}, u32[]{:S(2)}) collective-permute-start(bf16[80,2048]{1,0:T(8,128)(2,1)S(1)} %get-tuple-element.35), channel_id=1, source_target_pairs={{0,1},{1,0},{2,3},{3,2},{4,5},{5,4},{6,7},{7,6},{8,9},{9,8},{10,11... | collective-permute-start | bytes 983048 | tf_op jit(solution)/shard_map/ppermute | solution.py:20
  99.8 3.2 %collective-permute-start.8 = (bf16[80,2048]{1,0:T(8,128)(2,1)S(1)}, bf16[80,2048]{1,0:T(8,128)(2,1)S(1)}, u32[]{:S(2)}, u32[]{:S(2)}) collective-permute-start(bf16[80,2048]{1,0:T(8,128)(2,1)S(1)} %get-tuple-element.33), channel_id=1, source_target_pairs={{0,1},{1,0},{2,3},{3,2},{4,5},{5,4},{6,7},{7,6},{8,9},{9,8},{10,11... | collective-permute-start | bytes 983048 | tf_op jit(solution)/shard_map/ppermute | solution.py:20
  100.1 1.9 collective-permute-start.11
  100.5 10.7 %collective-permute-start.10 = (bf16[80,2048]{1,0:T(8,128)(2,1)S(1)}, bf16[80,2048]{1,0:T(8,128)(2,1)S(1)}, u32[]{:S(2)}, u32[]{:S(2)}) collective-permute-start(bf16[80,2048]{1,0:T(8,128)(2,1)S(1)} %add_convert_fusion.5), channel_id=1, source_target_pairs={{0,2},{2,0},{4,6},{6,4},{1,3},{3,1},{5,7},{7,5},{8,10},{10,8},{12,... | collective-permute-start | bytes 983048 | tf_op jit(solution)/shard_map/ppermute | solution.py:20
  102.1 15.4 %collective-permute-start.12 = (bf16[80,2048]{1,0:T(8,128)(2,1)S(1)}, bf16[80,2048]{1,0:T(8,128)(2,1)S(1)}, u32[]{:S(2)}, u32[]{:S(2)}) collective-permute-start(bf16[80,2048]{1,0:T(8,128)(2,1)S(1)} %add_convert_fusion.4), channel_id=1, source_target_pairs={{0,2},{2,0},{4,6},{6,4},{1,3},{3,1},{5,7},{7,5},{8,10},{10,8},{12,... | collective-permute-start | bytes 983048 | tf_op jit(solution)/shard_map/ppermute | solution.py:20
  120.7 10.7 %collective-permute-start.13 = (bf16[80,2048]{1,0:T(8,128)(2,1)S(1)}, bf16[80,2048]{1,0:T(8,128)(2,1)S(1)}, u32[]{:S(2)}, u32[]{:S(2)}) collective-permute-start(bf16[80,2048]{1,0:T(8,128)(2,1)S(1)} %bitcast.79), channel_id=1, source_target_pairs={{0,2},{2,0},{4,6},{6,4},{1,3},{3,1},{5,7},{7,5},{8,10},{10,8},{12,... | collective-permute-start | bytes 983048 | tf_op jit(solution)/shard_map/ppermute | solution.py:20
  121.5 22.4 %collective-permute-start.17 = (bf16[80,2048]{1,0:T(8,128)(2,1)S(1)}, bf16[80,2048]{1,0:T(8,128)(2,1)S(1)}, u32[]{:S(2)}, u32[]{:S(2)}) collective-permute-start(bf16[80,2048]{1,0:T(8,128)(2,1)S(1)} %bitcast.73), channel_id=1, source_target_pairs={{0,2},{2,0},{4,6},{6,4},{1,3},{3,1},{5,7},{7,5},{8,10},{10,8},{12,... | collective-permute-start | bytes 983048 | tf_op jit(solution)/shard_map/ppermute | solution.py:20
  123.3 20.8 %collective-permute-start.14 = (bf16[80,2048]{1,0:T(8,128)(2,1)S(1)}, bf16[80,2048]{1,0:T(8,128)(2,1)S(1)}, u32[]{:S(2)}, u32[]{:S(2)}) collective-permute-start(bf16[80,2048]{1,0:T(8,128)(2,1)S(1)} %bitcast.80), channel_id=1, source_target_pairs={{0,1},{1,0},{2,3},{3,2},{4,5},{5,4},{6,7},{7,6},{8,9},{9,8},{10,11... | collective-permute-start | bytes 983048 | tf_op jit(solution)/shard_map/ppermute | solution.py:20
  131.4 12.7 %collective-permute-start.15 = (bf16[80,2048]{1,0:T(8,128)(2,1)S(1)}, bf16[80,2048]{1,0:T(8,128)(2,1)S(1)}, u32[]{:S(2)}, u32[]{:S(2)}) collective-permute-start(bf16[80,2048]{1,0:T(8,128)(2,1)S(1)} %collective-permute-done.13.refs_1_), channel_id=1, source_target_pairs={{0,1},{1,0},{2,3},{3,2},{4,5},{5,4},{6,7},{7,6},{8,9},{9,8},{10,11... | collective-permute-start | bytes 983048 | tf_op jit(solution)/shard_map/ppermute | solution.py:20
  131.4 21.7 %collective-permute-start.18 = (bf16[80,2048]{1,0:T(8,128)(2,1)S(1)}, bf16[80,2048]{1,0:T(8,128)(2,1)S(1)}, u32[]{:S(2)}, u32[]{:S(2)}) collective-permute-start(bf16[80,2048]{1,0:T(8,128)(2,1)S(1)} %bitcast.74), channel_id=1, source_target_pairs={{0,1},{1,0},{2,3},{3,2},{4,5},{5,4},{6,7},{7,6},{8,9},{9,8},{10,11... | collective-permute-start | bytes 983048 | tf_op jit(solution)/shard_map/ppermute | solution.py:20
  131.9 48.3 %all-to-all-start.2 = ((bf16[16,40,512]{2,1,0:T(8,128)(2,1)}), bf16[16,40,512]{2,1,0:T(8,128)(2,1)}, u32[]{:S(2)}, u32[]{:S(2)}) async-start(bf16[16,40,512]{2,1,0:T(8,128)(2,1)} %bitcast.12), calls=%async_computation.2 | async-start | bytes 1310720 | tf_op jit(solution)/shard_map/all_to_all | solution.py:30
  143.9 9.1 %collective-permute-start.19 = (bf16[80,2048]{1,0:T(8,128)(2,1)S(1)}, bf16[80,2048]{1,0:T(8,128)(2,1)S(1)}, u32[]{:S(2)}, u32[]{:S(2)}) collective-permute-start(bf16[80,2048]{1,0:T(8,128)(2,1)S(1)} %collective-permute-done.17.refs_1_), channel_id=1, source_target_pairs={{0,1},{1,0},{2,3},{3,2},{4,5},{5,4},{6,7},{7,6},{8,9},{9,8},{10,11... | collective-permute-start | bytes 983048 | tf_op jit(solution)/shard_map/ppermute | solution.py:20
  152.1 12.0 %collective-permute-start.16 = (bf16[80,2048]{1,0:T(8,128)(2,1)S(1)}, bf16[80,2048]{1,0:T(8,128)(2,1)S(1)}, u32[]{:S(2)}, u32[]{:S(2)}) collective-permute-start(bf16[80,2048]{1,0:T(8,128)(2,1)S(1)} %get-tuple-element.42), channel_id=1, source_target_pairs={{0,1},{1,0},{2,3},{3,2},{4,5},{5,4},{6,7},{7,6},{8,9},{9,8},{10,11... | collective-permute-start | bytes 983048 | tf_op jit(solution)/shard_map/ppermute | solution.py:20
  152.7 9.0 %collective-permute-start.21 = (bf16[80,2048]{1,0:T(8,128)(2,1)S(1)}, bf16[80,2048]{1,0:T(8,128)(2,1)S(1)}, u32[]{:S(2)}, u32[]{:S(2)}) collective-permute-start(bf16[80,2048]{1,0:T(8,128)(2,1)S(1)} %get-tuple-element.46), channel_id=1, source_target_pairs={{0,1},{1,0},{2,3},{3,2},{4,5},{5,4},{6,7},{7,6},{8,9},{9,8},{10,11... | collective-permute-start | bytes 983048 | tf_op jit(solution)/shard_map/ppermute | solution.py:20
  161.0 3.2 %collective-permute-start.20 = (bf16[80,2048]{1,0:T(8,128)(2,1)S(1)}, bf16[80,2048]{1,0:T(8,128)(2,1)S(1)}, u32[]{:S(2)}, u32[]{:S(2)}) collective-permute-start(bf16[80,2048]{1,0:T(8,128)(2,1)S(1)} %get-tuple-element.44), channel_id=1, source_target_pairs={{0,1},{1,0},{2,3},{3,2},{4,5},{5,4},{6,7},{7,6},{8,9},{9,8},{10,11... | collective-permute-start | bytes 983048 | tf_op jit(solution)/shard_map/ppermute | solution.py:20
  161.3 2.0 collective-permute-start.23
  161.7 10.7 %collective-permute-start.22 = (bf16[80,2048]{1,0:T(8,128)(2,1)S(1)}, bf16[80,2048]{1,0:T(8,128)(2,1)S(1)}, u32[]{:S(2)}, u32[]{:S(2)}) collective-permute-start(bf16[80,2048]{1,0:T(8,128)(2,1)S(1)} %add_convert_fusion.1), channel_id=1, source_target_pairs={{0,2},{2,0},{4,6},{6,4},{1,3},{3,1},{5,7},{7,5},{8,10},{10,8},{12,... | collective-permute-start | bytes 983048 | tf_op jit(solution)/shard_map/ppermute | solution.py:20
  163.3 15.3 %collective-permute-start.24 = (bf16[80,2048]{1,0:T(8,128)(2,1)S(1)}, bf16[80,2048]{1,0:T(8,128)(2,1)S(1)}, u32[]{:S(2)}, u32[]{:S(2)}) collective-permute-start(bf16[80,2048]{1,0:T(8,128)(2,1)S(1)} %add_convert_fusion), channel_id=1, source_target_pairs={{0,2},{2,0},{4,6},{6,4},{1,3},{3,1},{5,7},{7,5},{8,10},{10,8},{12,... | collective-permute-start | bytes 983048 | tf_op jit(solution)/shard_map/ppermute | solution.py:20
  180.2 12.2 %copy-start.1 = (f32[128,2]{0,1:T(2,128)S(1)}, f32[128,2]{0,1:T(2,128)}, u32[]{:S(2)}) copy-start(f32[128,2]{0,1:T(2,128)} %param.10) | copy-start | bytes 3076
  180.2 44.8 %all-to-all-start.3 = ((bf16[16,40,512]{2,1,0:T(8,128)(2,1)}), bf16[16,40,512]{2,1,0:T(8,128)(2,1)S(1)}, u32[]{:S(2)}, u32[]{:S(2)}) async-start(bf16[16,40,512]{2,1,0:T(8,128)(2,1)} %bitcast.16), calls=%async_computation.3 | async-start | bytes 1310720 | tf_op jit(solution)/shard_map/all_to_all | solution.py:30
  225.0 11.5 %collective-permute-start.25 = (bf16[16,40,512]{2,1,0:T(8,128)(2,1)S(1)}, bf16[16,40,512]{2,1,0:T(8,128)(2,1)S(1)}, u32[]{:S(2)}, u32[]{:S(2)}) collective-permute-start(bf16[16,40,512]{2,1,0:T(8,128)(2,1)S(1)} %all-to-all-done.3), channel_id=1, source_target_pairs={{0,6},{2,4},{4,2},{6,0},{1,7},{3,5},{5,3},{7,1},{8,14},{10,12},{12... | collective-permute-start | bytes 1966088 | tf_op jit(solution)/shard_map/ppermute | solution.py:20

commit v6 on v5

--- a/solution.py
+++ b/solution.py
@@ -139,6 +139,34 @@
     return packed.reshape(nz, -1, width)
 
 
+def finish_kernel(mixed, back, *refs):
+    selects, scales, out = refs[: len(refs) // 2], refs[len(refs) // 2 : -1], refs[-1]
+    total = mixed[...]
+    for select, scale in zip(selects, scales):
+        picked = jnp.dot(select[...], back[...], preferred_element_type=jnp.float32)
+        total = total + picked * scale[...]
+    count, width = out.shape[0], total.shape[1]
+    for q in range(SPLIT):
+        out[:, q * width : (q + 1) * width] = total[q * count : (q + 1) * count].astype(out.dtype)
+
+
+def finish(mixed, back, selects, scales):
+    stacked, width = mixed.shape
+    vmem = pl.BlockSpec(memory_space=pltpu.VMEM)
+    return pl.pallas_call(
+        finish_kernel,
+        out_shape=jax.ShapeDtypeStruct((stacked // SPLIT, width * SPLIT), jnp.bfloat16),
+        in_specs=[vmem] * (2 + 2 * len(selects)),
+        out_specs=vmem,
+        compiler_params=pltpu.CompilerParams(vmem_limit_bytes=16 * 2**20),
+        cost_estimate=pl.CostEstimate(
+            flops=2 * len(selects) * stacked * back.shape[0] * width,
+            bytes_accessed=8 * stacked * width,
+            transcendentals=0,
+        ),
+    )(mixed, back, *selects, *scales)
+
+
 def through_row(packed, weights, capacity, pieces):
     rows = unpack(packed, capacity)
     size = rows.shape[0] // pieces
@@ -219,18 +247,20 @@
     far_back = swap(far_back, "x", 3)
 
     mixed = jnp.zeros((SPLIT * tok_count, width), jnp.float32)
+    selects, scales = [], []
     for k in range(top_count):
-        picked = jnp.zeros((SPLIT * tok_count, width), jnp.float32)
-        for part, back in ((0, near_back), (1, far_back)):
-            select = chosen(part, k).T.astype(jnp.bfloat16)
-            picked = picked + jnp.dot(
-                select, back.reshape(-1, width), preferred_element_type=jnp.float32
-            )
-        mixed = mixed + picked * jnp.tile(route_weights[:, k], SPLIT)[:, None]
-    mixed = mixed.astype(jnp.bfloat16)
-    return jnp.concatenate(
-        [mixed[q * tok_count : (q + 1) * tok_count] for q in range(SPLIT)], axis=1
-    )
+        scale = jnp.tile(route_weights[:, k], SPLIT)[:, None]
+        picked = jnp.dot(
+            chosen(0, k).T.astype(jnp.bfloat16),
+            near_back.reshape(-1, width),
+            preferred_element_type=jnp.float32,
+        )
+        mixed = mixed + picked * scale
+        place = jnp.tile(jnp.where(parts[k] == 1, places[k], -1), SPLIT)
+        select = (line_piece[None, :] == piece[:, None]) & (line_place[None, :] == place[:, None])
+        selects.append(select.astype(jnp.bfloat16))
+        scales.append(scale)
+    return finish(mixed, far_back.reshape(-1, width), selects, scales)
 
 
 def solution(mesh):

time: 242 us -> 241 us (level)
    dot_general x4 -> x2, matrix products: 5.36 us -> 3.9 us  [local(): jnp.dot(chosen(0, k).T.astype(jnp.bfloat16), near_back.reshape(-1, width)...]
where the time goes in v6:
time: 241 us; the launch traced here: 238 us
  waiting for transfers between devices  112 us (46%)
  starting transfers between devices  74.5 us (31%)
  Pallas kernels  36.8 us (15%)
  matrix products  6.09 us (3%)
  other arithmetic  4.19 us (2%)
  local copies, waits for them, and re-layouts  4.17 us (2%)
    ppermute x26, waiting for transfers between devices, swap(): return lax.ppermute(block, axis, [(i, i ^ mask) for i in range(count)])  63.2 us
    all_to_all x4, starting transfers between devices, along_z(): return lax.all_to_all(packed, 'z', split_axis=0, concat_axis=0, tiled=True)  58.4 us
    all_to_all x4, waiting for transfers between devices, along_z(): return lax.all_to_all(packed, 'z', split_axis=0, concat_axis=0, tiled=True)  49 us
    pallas_call x4, Pallas kernels, expert(): pl.pallas_call(expert_kernel, grid=(model_width // DEPTH,), in_specs=[who...  31.8 us
    ppermute x26, starting transfers between devices, swap(): return lax.ppermute(block, axis, [(i, i ^ mask) for i in range(count)])  16.2 us
  transfers between devices with their start and end apart: 30, of which 12 were waited for; matrix products, arithmetic and copies ran while one was open for 3% of the time, Pallas kernels for 15%

profile of v6, /device:TPU:34, one launch (start us, length us, event | category | flops | bytes accessed | tf_op | source)
XLA Modules:
  0.0 238.4 jit_solution(10661952205378271134)
XLA Ops:
  0.0 0.8 slice_bitcast_fusion.3
  0.8 1.2 fusion.8
  2.0 1.2 fusion.10
  3.6 1.5 convolution_convert_fusion.1
  5.1 24.0 %all-to-all-start = ((bf16[16,40,512]{2,1,0:T(8,128)(2,1)}), bf16[16,40,512]{2,1,0:T(8,128)(2,1)S(1)}, u32[]{:S(2)}, u32[]{:S(2)}) async-start(bf16[16,40,512]{2,1,0:T(8,128)(2,1)} %bitcast.5), calls=%async_computation | async-start | bytes 1310720 | tf_op jit(solution)/shard_map/all_to_all | solution.py:30
  29.1 0.7 convolution_convert_fusion
  29.8 1.7 collective-permute-start
  32.0 14.1 %collective-permute-done = bf16[16,40,512]{2,1,0:T(8,128)(2,1)S(1)} collective-permute-done((bf16[16,40,512]{2,1,0:T(8,128)(2,1)S(1)}, bf16[16,40,512]{2,1,0:T(8,128)(2,1)S(1)}, u32[]{:S(2)}, u32[]{:S(2)}) %collective-permute-start) | collective-permute-done | bytes 655392 | tf_op jit(solution)/shard_map/ppermute | solution.py:20
  46.2 16.6 %all-to-all-done = bf16[16,40,512]{2,1,0:T(8,128)(2,1)S(1)} async-done(((bf16[16,40,512]{2,1,0:T(8,128)(2,1)}), bf16[16,40,512]{2,1,0:T(8,128)(2,1)S(1)}, u32[]{:S(2)}, u32[]{:S(2)}) %all-to-all-start) | async-done | bytes 655392 | tf_op jit(solution)/shard_map/all_to_all | solution.py:30
  63.3 0.5 collective-permute-start.5
  64.2 1.7 collective-permute-start.1
  65.9 5.4 %collective-permute-done.5.refs_1_ = bf16[80,2048]{1,0:T(8,128)(2,1)S(1)} collective-permute-done((bf16[80,2048]{1,0:T(8,128)(2,1)S(1)}, bf16[80,2048]{1,0:T(8,128)(2,1)S(1)}, u32[]{:S(2)}, u32[]{:S(2)}) %collective-permute-start.5) | collective-permute-done | bytes 327712 | tf_op jit(solution)/shard_map/ppermute | solution.py:20
  71.3 0.5 collective-permute-start.2
  71.8 10.2 %all-to-all-start.1 = ((bf16[16,40,512]{2,1,0:T(8,128)(2,1)}), bf16[16,40,512]{2,1,0:T(8,128)(2,1)}, u32[]{:S(2)}, u32[]{:S(2)}) async-start(bf16[16,40,512]{2,1,0:T(8,128)(2,1)} %copy-done), calls=%async_computation.1 | async-start | bytes 1310720 | tf_op jit(solution)/shard_map/all_to_all | solution.py:30
  82.2 8.0 %shard_map.74 = (bf16[80,2048]{1,0:T(8,128)(2,1)S(1)}, bf16[80,2048]{1,0:T(8,128)(2,1)S(1)}, bf16[80,2048]{1,0:T(8,128)(2,1)S(1)}, bf16[80,2048]{1,0:T(8,128)(2,1)S(1)}) custom-call(bf16[80,2048]{1,0:T(8,128)(2,1)S(1)} %bitcast.79, bf16[80,2048]{1,0:T(8,128)(2,1)S(1)} %collective-permute-done.5.refs_1_, bf16[80,2048]{1,0:T(8,128)(2,1)S(1)} %collective-permute-done.6.refs_2_, ...), custom_call_target="tpu_custom_call" | custom-call | flops 3523215360 | bytes 13631488 | tf_op jit(solution)/shard_map/pallas_call | solution.py:87
  90.2 0.6 collective-permute-start.11
  90.7 8.0 %shard_map.73 = (bf16[80,2048]{1,0:T(8,128)(2,1)S(1)}, bf16[80,2048]{1,0:T(8,128)(2,1)S(1)}, bf16[80,2048]{1,0:T(8,128)(2,1)S(1)}, bf16[80,2048]{1,0:T(8,128)(2,1)S(1)}) custom-call(bf16[80,2048]{1,0:T(8,128)(2,1)S(1)} %bitcast.73, bf16[80,2048]{1,0:T(8,128)(2,1)S(1)} %collective-permute-done.1.refs_1_, bf16[80,2048]{1,0:T(8,128)(2,1)S(1)} %collective-permute-done.2.refs_2_, ...), custom_call_target="tpu_custom_call" | custom-call | flops 3523215360 | bytes 13631488 | tf_op jit(solution)/shard_map/pallas_call | solution.py:87
  98.7 0.4 collective-permute-start.9
  99.1 0.5 collective-permute-start.8
  99.8 0.5 collective-permute-start.12
  100.7 1.4 collective-permute-start.10
  102.3 8.2 %collective-permute-done.12.refs_3_ = bf16[80,2048]{1,0:T(8,128)(2,1)S(1)} collective-permute-done((bf16[80,2048]{1,0:T(8,128)(2,1)S(1)}, bf16[80,2048]{1,0:T(8,128)(2,1)S(1)}, u32[]{:S(2)}, u32[]{:S(2)}) %collective-permute-start.12) | collective-permute-done | bytes 327712 | tf_op jit(solution)/shard_map/ppermute | solution.py:20
  110.5 6.4 %collective-permute-done.10.refs_2_ = bf16[80,2048]{1,0:T(8,128)(2,1)S(1)} collective-permute-done((bf16[80,2048]{1,0:T(8,128)(2,1)S(1)}, bf16[80,2048]{1,0:T(8,128)(2,1)S(1)}, u32[]{:S(2)}, u32[]{:S(2)}) %collective-permute-start.10) | collective-permute-done | bytes 327712 | tf_op jit(solution)/shard_map/ppermute | solution.py:20
  116.9 1.6 shard_map.75
  118.5 1.3 copy.27
  120.1 0.5 collective-permute-start.17
  121.0 1.7 collective-permute-start.13
  122.8 8.1 %collective-permute-done.17.refs_1_ = bf16[80,2048]{1,0:T(8,128)(2,1)S(1)} collective-permute-done((bf16[80,2048]{1,0:T(8,128)(2,1)S(1)}, bf16[80,2048]{1,0:T(8,128)(2,1)S(1)}, u32[]{:S(2)}, u32[]{:S(2)}) %collective-permute-start.17) | collective-permute-done | bytes 327712 | tf_op jit(solution)/shard_map/ppermute | solution.py:20
  130.9 0.5 collective-permute-start.14
  131.4 12.0 %all-to-all-start.2 = ((bf16[16,40,512]{2,1,0:T(8,128)(2,1)}), bf16[16,40,512]{2,1,0:T(8,128)(2,1)}, u32[]{:S(2)}, u32[]{:S(2)}) async-start(bf16[16,40,512]{2,1,0:T(8,128)(2,1)} %bitcast.12), calls=%async_computation.2 | async-start | bytes 1310720 | tf_op jit(solution)/shard_map/all_to_all | solution.py:30
  143.6 8.0 %shard_map.77 = (bf16[80,2048]{1,0:T(8,128)(2,1)S(1)}, bf16[80,2048]{1,0:T(8,128)(2,1)S(1)}, bf16[80,2048]{1,0:T(8,128)(2,1)S(1)}, bf16[80,2048]{1,0:T(8,128)(2,1)S(1)}) custom-call(bf16[80,2048]{1,0:T(8,128)(2,1)S(1)} %bitcast.82, bf16[80,2048]{1,0:T(8,128)(2,1)S(1)} %collective-permute-done.17.refs_1_, ...), custom_call_target="tpu_custom_call" | custom-call | flops 3523215360 | bytes 13631488 | tf_op jit(solution)/shard_map/pallas_call | solution.py:87
  151.6 0.6 collective-permute-start.23
  152.1 7.9 %shard_map.76 = (bf16[80,2048]{1,0:T(8,128)(2,1)S(1)}, bf16[80,2048]{1,0:T(8,128)(2,1)S(1)}, bf16[80,2048]{1,0:T(8,128)(2,1)S(1)}, bf16[80,2048]{1,0:T(8,128)(2,1)S(1)}) custom-call(bf16[80,2048]{1,0:T(8,128)(2,1)S(1)} %bitcast.76, bf16[80,2048]{1,0:T(8,128)(2,1)S(1)} %collective-permute-done.13.refs_1_, ...), custom_call_target="tpu_custom_call" | custom-call | flops 3523215360 | bytes 13631488 | tf_op jit(solution)/shard_map/pallas_call | solution.py:87
  160.1 0.4 collective-permute-start.21
  160.5 0.5 collective-permute-start.20
  161.2 0.5 collective-permute-start.24
  162.2 1.4 collective-permute-start.22
  163.7 8.2 %collective-permute-done.24.refs_3_ = bf16[80,2048]{1,0:T(8,128)(2,1)S(1)} collective-permute-done((bf16[80,2048]{1,0:T(8,128)(2,1)S(1)}, bf16[80,2048]{1,0:T(8,128)(2,1)S(1)}, u32[]{:S(2)}, u32[]{:S(2)}) %collective-permute-start.24) | collective-permute-done | bytes 327712 | tf_op jit(solution)/shard_map/ppermute | solution.py:20
  171.9 6.4 %collective-permute-done.22.refs_2_ = bf16[80,2048]{1,0:T(8,128)(2,1)S(1)} collective-permute-done((bf16[80,2048]{1,0:T(8,128)(2,1)S(1)}, bf16[80,2048]{1,0:T(8,128)(2,1)S(1)}, u32[]{:S(2)}, u32[]{:S(2)}) %collective-permute-start.22) | collective-permute-done | bytes 327712 | tf_op jit(solution)/shard_map/ppermute | solution.py:20
  178.3 1.6 shard_map.78
  179.9 12.2 %all-to-all-start.3 = ((bf16[16,40,512]{2,1,0:T(8,128)(2,1)}), bf16[16,40,512]{2,1,0:T(8,128)(2,1)S(1)}, u32[]{:S(2)}, u32[]{:S(2)}) async-start(bf16[16,40,512]{2,1,0:T(8,128)(2,1)} %bitcast.16), calls=%async_computation.3 | async-start | bytes 1310720 | tf_op jit(solution)/shard_map/all_to_all | solution.py:30
  192.1 0.5 fusion.2
  192.7 32.4 %all-to-all-done.3 = bf16[16,40,512]{2,1,0:T(8,128)(2,1)S(1)} async-done(((bf16[16,40,512]{2,1,0:T(8,128)(2,1)}), bf16[16,40,512]{2,1,0:T(8,128)(2,1)S(1)}, u32[]{:S(2)}, u32[]{:S(2)}) %all-to-all-start.3) | async-done | bytes 655392 | tf_op jit(solution)/shard_map/all_to_all | solution.py:30
  225.1 1.6 collective-permute-start.25
  227.0 1.9 convolution_multiply_fusion.1
  229.0 1.9 fusion.mixed
  230.9 5.7 %collective-permute-done.25 = bf16[16,40,512]{2,1,0:T(8,128)(2,1)S(1)} collective-permute-done((bf16[16,40,512]{2,1,0:T(8,128)(2,1)S(1)}, bf16[16,40,512]{2,1,0:T(8,128)(2,1)S(1)}, u32[]{:S(2)}, u32[]{:S(2)}) %collective-permute-start.25) | collective-permute-done | bytes 655392 | tf_op jit(solution)/shard_map/ppermute | solution.py:20
  236.6 1.8 shard_map.79
  (75 shorter events, 4.7 us)
Async XLA Ops:
  0.8 2.7 %copy-start.1 = (s32[128,2]{0,1:T(2,128)S(1)}, s32[128,2]{0,1:T(2,128)}, u32[]{:S(2)}) copy-start(s32[128,2]{0,1:T(2,128)} %param.9) | copy-start | bytes 3076
  5.1 57.6 %all-to-all-start = ((bf16[16,40,512]{2,1,0:T(8,128)(2,1)}), bf16[16,40,512]{2,1,0:T(8,128)(2,1)S(1)}, u32[]{:S(2)}, u32[]{:S(2)}) async-start(bf16[16,40,512]{2,1,0:T(8,128)(2,1)} %bitcast.5), calls=%async_computation | async-start | bytes 1310720 | tf_op jit(solution)/shard_map/all_to_all | solution.py:30
  29.8 16.4 %collective-permute-start = (bf16[16,40,512]{2,1,0:T(8,128)(2,1)S(1)}, bf16[16,40,512]{2,1,0:T(8,128)(2,1)S(1)}, u32[]{:S(2)}, u32[]{:S(2)}) collective-permute-start(bf16[16,40,512]{2,1,0:T(8,128)(2,1)S(1)} %bitcast.91), channel_id=1, source_target_pairs={{0,6},{2,4},{4,2},{6,0},{1,7},{3,5},{5,3},{7,1},{8,14},{10,12},{12... | collective-permute-start | bytes 1966088 | tf_op jit(solution)/shard_map/ppermute | solution.py:20
  46.2 16.8 %copy-start = (bf16[16,40,512]{2,1,0:T(8,128)(2,1)}, bf16[16,40,512]{2,1,0:T(8,128)(2,1)S(1)}, u32[]{:S(2)}) copy-start(bf16[16,40,512]{2,1,0:T(8,128)(2,1)S(1)} %collective-permute-done) | copy-start | bytes 1966084
  63.3 8.0 %collective-permute-start.5 = (bf16[80,2048]{1,0:T(8,128)(2,1)S(1)}, bf16[80,2048]{1,0:T(8,128)(2,1)S(1)}, u32[]{:S(2)}, u32[]{:S(2)}) collective-permute-start(bf16[80,2048]{1,0:T(8,128)(2,1)S(1)} %bitcast.77), channel_id=1, source_target_pairs={{0,2},{2,0},{4,6},{6,4},{1,3},{3,1},{5,7},{7,5},{8,10},{10,8},{12,... | collective-permute-start | bytes 983048 | tf_op jit(solution)/shard_map/ppermute | solution.py:20
  64.2 17.8 %collective-permute-start.1 = (bf16[80,2048]{1,0:T(8,128)(2,1)S(1)}, bf16[80,2048]{1,0:T(8,128)(2,1)S(1)}, u32[]{:S(2)}, u32[]{:S(2)}) collective-permute-start(bf16[80,2048]{1,0:T(8,128)(2,1)S(1)} %bitcast.71), channel_id=1, source_target_pairs={{0,2},{2,0},{4,6},{6,4},{1,3},{3,1},{5,7},{7,5},{8,10},{10,8},{12,... | collective-permute-start | bytes 983048 | tf_op jit(solution)/shard_map/ppermute | solution.py:20
  65.9 16.2 %collective-permute-start.6 = (bf16[80,2048]{1,0:T(8,128)(2,1)S(1)}, bf16[80,2048]{1,0:T(8,128)(2,1)S(1)}, u32[]{:S(2)}, u32[]{:S(2)}) collective-permute-start(bf16[80,2048]{1,0:T(8,128)(2,1)S(1)} %bitcast.78), channel_id=1, source_target_pairs={{0,1},{1,0},{2,3},{3,2},{4,5},{5,4},{6,7},{7,6},{8,9},{9,8},{10,11... | collective-permute-start | bytes 983048 | tf_op jit(solution)/shard_map/ppermute | solution.py:20
  71.3 10.9 %collective-permute-start.7 = (bf16[80,2048]{1,0:T(8,128)(2,1)S(1)}, bf16[80,2048]{1,0:T(8,128)(2,1)S(1)}, u32[]{:S(2)}, u32[]{:S(2)}) collective-permute-start(bf16[80,2048]{1,0:T(8,128)(2,1)S(1)} %collective-permute-done.5.refs_1_), channel_id=1, source_target_pairs={{0,1},{1,0},{2,3},{3,2},{4,5},{5,4},{6,7},{7,6},{8,9},{9,8},{10,11... | collective-permute-start | bytes 983048 | tf_op jit(solution)/shard_map/ppermute | solution.py:20
  71.3 19.4 %collective-permute-start.2 = (bf16[80,2048]{1,0:T(8,128)(2,1)S(1)}, bf16[80,2048]{1,0:T(8,128)(2,1)S(1)}, u32[]{:S(2)}, u32[]{:S(2)}) collective-permute-start(bf16[80,2048]{1,0:T(8,128)(2,1)S(1)} %bitcast.72), channel_id=1, source_target_pairs={{0,1},{1,0},{2,3},{3,2},{4,5},{5,4},{6,7},{7,6},{8,9},{9,8},{10,11... | collective-permute-start | bytes 983048 | tf_op jit(solution)/shard_map/ppermute | solution.py:20
  71.8 46.7 %all-to-all-start.1 = ((bf16[16,40,512]{2,1,0:T(8,128)(2,1)}), bf16[16,40,512]{2,1,0:T(8,128)(2,1)}, u32[]{:S(2)}, u32[]{:S(2)}) async-start(bf16[16,40,512]{2,1,0:T(8,128)(2,1)} %copy-done), calls=%async_computation.1 | async-start | bytes 1310720 | tf_op jit(solution)/shard_map/all_to_all | solution.py:30
  82.0 8.7 %collective-permute-start.3 = (bf16[80,2048]{1,0:T(8,128)(2,1)S(1)}, bf16[80,2048]{1,0:T(8,128)(2,1)S(1)}, u32[]{:S(2)}, u32[]{:S(2)}) collective-permute-start(bf16[80,2048]{1,0:T(8,128)(2,1)S(1)} %collective-permute-done.1.refs_1_), channel_id=1, source_target_pairs={{0,1},{1,0},{2,3},{3,2},{4,5},{5,4},{6,7},{7,6},{8,9},{9,8},{10,11... | collective-permute-start | bytes 983048 | tf_op jit(solution)/shard_map/ppermute | solution.py:20
  90.2 9.5 %collective-permute-start.11 = (bf16[80,2048]{1,0:T(8,128)(2,1)S(1)}, bf16[80,2048]{1,0:T(8,128)(2,1)S(1)}, u32[]{:S(2)}, u32[]{:S(2)}) collective-permute-start(bf16[80,2048]{1,0:T(8,128)(2,1)S(1)} %get-tuple-element.37), channel_id=1, source_target_pairs={{0,1},{1,0},{2,3},{3,2},{4,5},{5,4},{6,7},{7,6},{8,9},{9,8},{10,11... | collective-permute-start | bytes 983048 | tf_op jit(solution)/shard_map/ppermute | solution.py:20
  98.7 1.9 collective-permute-start.9
  99.1 3.1 %collective-permute-start.8 = (bf16[80,2048]{1,0:T(8,128)(2,1)S(1)}, bf16[80,2048]{1,0:T(8,128)(2,1)S(1)}, u32[]{:S(2)}, u32[]{:S(2)}) collective-permute-start(bf16[80,2048]{1,0:T(8,128)(2,1)S(1)} %get-tuple-element.33), channel_id=1, source_target_pairs={{0,1},{1,0},{2,3},{3,2},{4,5},{5,4},{6,7},{7,6},{8,9},{9,8},{10,11... | collective-permute-start | bytes 983048 | tf_op jit(solution)/shard_map/ppermute | solution.py:20
  99.5 2.7 %collective-permute-start.4 = (bf16[80,2048]{1,0:T(8,128)(2,1)S(1)}, bf16[80,2048]{1,0:T(8,128)(2,1)S(1)}, u32[]{:S(2)}, u32[]{:S(2)}) collective-permute-start(bf16[80,2048]{1,0:T(8,128)(2,1)S(1)} %get-tuple-element.31), channel_id=1, source_target_pairs={{0,1},{1,0},{2,3},{3,2},{4,5},{5,4},{6,7},{7,6},{8,9},{9,8},{10,11... | collective-permute-start | bytes 983048 | tf_op jit(solution)/shard_map/ppermute | solution.py:20
  99.8 10.7 %collective-permute-start.12 = (bf16[80,2048]{1,0:T(8,128)(2,1)S(1)}, bf16[80,2048]{1,0:T(8,128)(2,1)S(1)}, u32[]{:S(2)}, u32[]{:S(2)}) collective-permute-start(bf16[80,2048]{1,0:T(8,128)(2,1)S(1)} %add_convert_fusion.4), channel_id=1, source_target_pairs={{0,2},{2,0},{4,6},{6,4},{1,3},{3,1},{5,7},{7,5},{8,10},{10,8},{12,... | collective-permute-start | bytes 983048 | tf_op jit(solution)/shard_map/ppermute | solution.py:20
  100.7 16.2 %collective-permute-start.10 = (bf16[80,2048]{1,0:T(8,128)(2,1)S(1)}, bf16[80,2048]{1,0:T(8,128)(2,1)S(1)}, u32[]{:S(2)}, u32[]{:S(2)}) collective-permute-start(bf16[80,2048]{1,0:T(8,128)(2,1)S(1)} %add_convert_fusion.5), channel_id=1, source_target_pairs={{0,2},{2,0},{4,6},{6,4},{1,3},{3,1},{5,7},{7,5},{8,10},{10,8},{12,... | collective-permute-start | bytes 983048 | tf_op jit(solution)/shard_map/ppermute | solution.py:20
  120.1 10.7 %collective-permute-start.17 = (bf16[80,2048]{1,0:T(8,128)(2,1)S(1)}, bf16[80,2048]{1,0:T(8,128)(2,1)S(1)}, u32[]{:S(2)}, u32[]{:S(2)}) collective-permute-start(bf16[80,2048]{1,0:T(8,128)(2,1)S(1)} %bitcast.80), channel_id=1, source_target_pairs={{0,2},{2,0},{4,6},{6,4},{1,3},{3,1},{5,7},{7,5},{8,10},{10,8},{12,... | collective-permute-start | bytes 983048 | tf_op jit(solution)/shard_map/ppermute | solution.py:20
  121.0 22.4 %collective-permute-start.13 = (bf16[80,2048]{1,0:T(8,128)(2,1)S(1)}, bf16[80,2048]{1,0:T(8,128)(2,1)S(1)}, u32[]{:S(2)}, u32[]{:S(2)}) collective-permute-start(bf16[80,2048]{1,0:T(8,128)(2,1)S(1)} %bitcast.74), channel_id=1, source_target_pairs={{0,2},{2,0},{4,6},{6,4},{1,3},{3,1},{5,7},{7,5},{8,10},{10,8},{12,... | collective-permute-start | bytes 983048 | tf_op jit(solution)/shard_map/ppermute | solution.py:20
  122.7 20.8 %collective-permute-start.18 = (bf16[80,2048]{1,0:T(8,128)(2,1)S(1)}, bf16[80,2048]{1,0:T(8,128)(2,1)S(1)}, u32[]{:S(2)}, u32[]{:S(2)}) collective-permute-start(bf16[80,2048]{1,0:T(8,128)(2,1)S(1)} %bitcast.81), channel_id=1, source_target_pairs={{0,1},{1,0},{2,3},{3,2},{4,5},{5,4},{6,7},{7,6},{8,9},{9,8},{10,11... | collective-permute-start | bytes 983048 | tf_op jit(solution)/shard_map/ppermute | solution.py:20
  130.9 12.7 %collective-permute-start.19 = (bf16[80,2048]{1,0:T(8,128)(2,1)S(1)}, bf16[80,2048]{1,0:T(8,128)(2,1)S(1)}, u32[]{:S(2)}, u32[]{:S(2)}) collective-permute-start(bf16[80,2048]{1,0:T(8,128)(2,1)S(1)} %collective-permute-done.17.refs_1_), channel_id=1, source_target_pairs={{0,1},{1,0},{2,3},{3,2},{4,5},{5,4},{6,7},{7,6},{8,9},{9,8},{10,11... | collective-permute-start | bytes 983048 | tf_op jit(solution)/shard_map/ppermute | solution.py:20
  130.9 21.3 %collective-permute-start.14 = (bf16[80,2048]{1,0:T(8,128)(2,1)S(1)}, bf16[80,2048]{1,0:T(8,128)(2,1)S(1)}, u32[]{:S(2)}, u32[]{:S(2)}) collective-permute-start(bf16[80,2048]{1,0:T(8,128)(2,1)S(1)} %bitcast.75), channel_id=1, source_target_pairs={{0,1},{1,0},{2,3},{3,2},{4,5},{5,4},{6,7},{7,6},{8,9},{9,8},{10,11... | collective-permute-start | bytes 983048 | tf_op jit(solution)/shard_map/ppermute | solution.py:20
  131.4 48.5 %all-to-all-start.2 = ((bf16[16,40,512]{2,1,0:T(8,128)(2,1)}), bf16[16,40,512]{2,1,0:T(8,128)(2,1)}, u32[]{:S(2)}, u32[]{:S(2)}) async-start(bf16[16,40,512]{2,1,0:T(8,128)(2,1)} %bitcast.12), calls=%async_computation.2 | async-start | bytes 1310720 | tf_op jit(solution)/shard_map/all_to_all | solution.py:30
  143.4 8.7 %collective-permute-start.15 = (bf16[80,2048]{1,0:T(8,128)(2,1)S(1)}, bf16[80,2048]{1,0:T(8,128)(2,1)S(1)}, u32[]{:S(2)}, u32[]{:S(2)}) collective-permute-start(bf16[80,2048]{1,0:T(8,128)(2,1)S(1)} %collective-permute-done.13.refs_1_), channel_id=1, source_target_pairs={{0,1},{1,0},{2,3},{3,2},{4,5},{5,4},{6,7},{7,6},{8,9},{9,8},{10,11... | collective-permute-start | bytes 983048 | tf_op jit(solution)/shard_map/ppermute | solution.py:20
  151.6 9.5 %collective-permute-start.23 = (bf16[80,2048]{1,0:T(8,128)(2,1)S(1)}, bf16[80,2048]{1,0:T(8,128)(2,1)S(1)}, u32[]{:S(2)}, u32[]{:S(2)}) collective-permute-start(bf16[80,2048]{1,0:T(8,128)(2,1)S(1)} %get-tuple-element.48), channel_id=1, source_target_pairs={{0,1},{1,0},{2,3},{3,2},{4,5},{5,4},{6,7},{7,6},{8,9},{9,8},{10,11... | collective-permute-start | bytes 983048 | tf_op jit(solution)/shard_map/ppermute | solution.py:20
  160.1 2.0 collective-permute-start.21
  160.5 3.1 %collective-permute-start.20 = (bf16[80,2048]{1,0:T(8,128)(2,1)S(1)}, bf16[80,2048]{1,0:T(8,128)(2,1)S(1)}, u32[]{:S(2)}, u32[]{:S(2)}) collective-permute-start(bf16[80,2048]{1,0:T(8,128)(2,1)S(1)} %get-tuple-element.44), channel_id=1, source_target_pairs={{0,1},{1,0},{2,3},{3,2},{4,5},{5,4},{6,7},{7,6},{8,9},{9,8},{10,11... | collective-permute-start | bytes 983048 | tf_op jit(solution)/shard_map/ppermute | solution.py:20
  161.0 2.7 %collective-permute-start.16 = (bf16[80,2048]{1,0:T(8,128)(2,1)S(1)}, bf16[80,2048]{1,0:T(8,128)(2,1)S(1)}, u32[]{:S(2)}, u32[]{:S(2)}) collective-permute-start(bf16[80,2048]{1,0:T(8,128)(2,1)S(1)} %get-tuple-element.42), channel_id=1, source_target_pairs={{0,1},{1,0},{2,3},{3,2},{4,5},{5,4},{6,7},{7,6},{8,9},{9,8},{10,11... | collective-permute-start | bytes 983048 | tf_op jit(solution)/shard_map/ppermute | solution.py:20
  161.2 10.7 %collective-permute-start.24 = (bf16[80,2048]{1,0:T(8,128)(2,1)S(1)}, bf16[80,2048]{1,0:T(8,128)(2,1)S(1)}, u32[]{:S(2)}, u32[]{:S(2)}) collective-permute-start(bf16[80,2048]{1,0:T(8,128)(2,1)S(1)} %add_convert_fusion), channel_id=1, source_target_pairs={{0,2},{2,0},{4,6},{6,4},{1,3},{3,1},{5,7},{7,5},{8,10},{10,8},{12,... | collective-permute-start | bytes 983048 | tf_op jit(solution)/shard_map/ppermute | solution.py:20
  162.2 16.2 %collective-permute-start.22 = (bf16[80,2048]{1,0:T(8,128)(2,1)S(1)}, bf16[80,2048]{1,0:T(8,128)(2,1)S(1)}, u32[]{:S(2)}, u32[]{:S(2)}) collective-permute-start(bf16[80,2048]{1,0:T(8,128)(2,1)S(1)} %add_convert_fusion.1), channel_id=1, source_target_pairs={{0,2},{2,0},{4,6},{6,4},{1,3},{3,1},{5,7},{7,5},{8,10},{10,8},{12,... | collective-permute-start | bytes 983048 | tf_op jit(solution)/shard_map/ppermute | solution.py:20
  179.9 12.2 %copy-start.2 = (f32[128,2]{0,1:T(2,128)S(1)}, f32[128,2]{0,1:T(2,128)}, u32[]{:S(2)}) copy-start(f32[128,2]{0,1:T(2,128)} %param.10) | copy-start | bytes 3076
  179.9 45.2 %all-to-all-start.3 = ((bf16[16,40,512]{2,1,0:T(8,128)(2,1)}), bf16[16,40,512]{2,1,0:T(8,128)(2,1)S(1)}, u32[]{:S(2)}, u32[]{:S(2)}) async-start(bf16[16,40,512]{2,1,0:T(8,128)(2,1)} %bitcast.16), calls=%async_computation.3 | async-start | bytes 1310720 | tf_op jit(solution)/shard_map/all_to_all | solution.py:30
  225.1 11.5 %collective-permute-start.25 = (bf16[16,40,512]{2,1,0:T(8,128)(2,1)S(1)}, bf16[16,40,512]{2,1,0:T(8,128)(2,1)S(1)}, u32[]{:S(2)}, u32[]{:S(2)}) collective-permute-start(bf16[16,40,512]{2,1,0:T(8,128)(2,1)S(1)} %all-to-all-done.3), channel_id=1, source_target_pairs={{0,6},{2,4},{4,2},{6,0},{1,7},{3,5},{5,3},{7,1},{8,14},{10,12},{12... | collective-permute-start | bytes 1966088 | tf_op jit(solution)/shard_map/ppermute | solution.py:20
